TPU v7x, 32 devices: a whole 2x2x4 slice. The times are simulated.
32 devices in a mesh: dp: 4 (over y, x), kv: 4 (over z), tp: 2 (over core).
Axes of the slice: x: 2, y: 2, z: 4, core: 2. Of those that a mesh axis runs over, the one named last changes fastest.
Arguments:
- tokens: bfloat16 [192, 2048], P(('dp', 'tp'), 'kv'), may hold values from -8 to 8
- mix_gain: float32 [2048], replicated, may hold values from 0.1 to 1.9
- w_gate: bfloat16 [2048, 4096], P(None, 'kv'), may hold values from -0.125 to 0.125
- w_value: bfloat16 [2048, 4096], P(None, 'kv'), may hold values from -0.125 to 0.125
- w_maps: bfloat16 [2048, 16384], P(None, 'kv'), may hold values from -0.125 to 0.125
- w_step: bfloat16 [2048, 64], replicated, may hold values from -0.125 to 0.125
- conv_value: float32 [4, 4096], P(None, 'kv'), may hold values from -0.5 to 0.5
- conv_maps: float32 [4, 16384], P(None, 'kv'), may hold values from -0.5 to 0.5
- past_value: bfloat16 [192, 3, 4096], P(('dp', 'tp'), None, 'kv'), may hold values from -6 to 6
- past_maps: bfloat16 [192, 3, 16384], P(('dp', 'tp'), None, 'kv'), may hold values from -6 to 6
- step_bias: float32 [64], P('kv'), may hold values from -3 to 0
- decay_log: float32 [64], P('kv'), may hold values from 0 to 2.77
- skip_gain: float32 [64], P('kv'), may hold values from 0.1 to 1.9
- head_gain: float32 [4096], P('kv'), may hold values from 0.1 to 1.9
- state: float32 [192, 64, 64, 128], P(('dp', 'tp'), 'kv'), may hold values from -2 to 2
- w_out: bfloat16 [4096, 2048], P('kv'), may hold values from -0.125 to 0.125
- mlp_gain: float32 [2048], replicated, may hold values from 0.1 to 1.9
- w_up: bfloat16 [2048, 8192], P(None, 'kv'), may hold values from -0.125 to 0.125
- w_down: bfloat16 [8192, 2048], P('kv'), may hold values from -0.09375 to 0.09375
Outputs:
- layer_out: bfloat16 [192, 2048], P(('dp', 'tp'), 'kv')
- state_next: float32 [192, 64, 64, 128], P(('dp', 'tp'), 'kv')
- value_tail: bfloat16 [192, 3, 4096], P(('dp', 'tp'), None, 'kv')
- maps_tail: bfloat16 [192, 3, 16384], P(('dp', 'tp'), None, 'kv')
All inputs are finite; a program needn't handle non-finite values.
Results may differ from a plain program's by a relative error of at most 0.0081.
Values may be sent and summed in bfloat16 or wider, within the bound.
No kernel may reach another device: no remote copies, remote signals or barrier semaphores. Data moves between devices by JAX's collectives and lax.ppermute only.
A program may use at most 128 MiB of HBM per device.

v0:
```python
import jax
import jax.numpy as jnp
from jax import lax
from jax.sharding import PartitionSpec as P

HEAD_DIM = 64
STATE = 128


NORM_EPS = 1e-05


def rms_rows(matrix, gain_vec):
    widened = matrix.astype(jnp.float32)
    inv_scale = lax.rsqrt(jnp.mean(widened * widened, axis=-1, keepdims=True) + NORM_EPS)
    return (widened * inv_scale * gain_vec).astype(jnp.bfloat16)


def short_conv(past_rows, newest, kernel):
    window = jnp.concatenate([past_rows, newest[:, None, :]], axis=1)
    summed = jnp.sum(window.astype(jnp.float32) * kernel[None], axis=1)
    return (jax.nn.silu(summed), window[:, 1:, :])


def local(
    tokens,
    mix_gain,
    w_gate,
    w_value,
    w_maps,
    w_step,
    conv_value,
    conv_maps,
    past_value,
    past_maps,
    step_bias,
    decay_log,
    skip_gain,
    head_gain,
    state,
    w_out,
    mlp_gain,
    w_up,
    w_down,
):
    whole_rows = lax.all_gather(tokens, "kv", axis=1, tiled=True)
    batch_rows = whole_rows.shape[0]
    heads_here = state.shape[1]
    head_start = lax.axis_index("kv") * heads_here
    normed = rms_rows(whole_rows, mix_gain)
    gate_pre = jnp.dot(normed, w_gate, preferred_element_type=jnp.float32)
    step_cols = lax.dynamic_slice_in_dim(w_step, head_start, heads_here, 1)
    step_pre = jnp.dot(normed, step_cols, preferred_element_type=jnp.float32)
    value_new = jnp.dot(normed, w_value, preferred_element_type=jnp.float32).astype(jnp.bfloat16)
    maps_new = jnp.dot(normed, w_maps, preferred_element_type=jnp.float32).astype(jnp.bfloat16)
    value_act, value_tail = short_conv(past_value, value_new, conv_value)
    maps_act, maps_tail = short_conv(past_maps, maps_new, conv_maps)
    maps_act = lax.optimization_barrier(maps_act.astype(jnp.bfloat16))
    grouped = maps_act.astype(jnp.float32).reshape(batch_rows, -1, 2, STATE)
    per_group = heads_here // grouped.shape[1]
    in_map = jnp.repeat(grouped[:, :, 0], per_group, axis=1)
    out_map = jnp.repeat(grouped[:, :, 1], per_group, axis=1)
    head_values = value_act.reshape(batch_rows, heads_here, HEAD_DIM)
    step_size = jax.nn.softplus(step_pre + step_bias)
    decay_rate = jnp.exp(-step_size * jnp.exp(decay_log))
    written = (step_size[:, :, None] * head_values)[:, :, :, None] * in_map[:, :, None, :]
    state_next = decay_rate[:, :, None, None] * state + written
    read_out = (
        jnp.sum(state_next * out_map[:, :, None, :], axis=-1)
        + skip_gain[None, :, None] * head_values
    )
    gated_heads = read_out * jax.nn.silu(gate_pre.reshape(batch_rows, heads_here, HEAD_DIM))
    inv_scale = lax.rsqrt(jnp.mean(gated_heads * gated_heads, axis=-1, keepdims=True) + NORM_EPS)
    heads_out = gated_heads * inv_scale * head_gain.reshape(heads_here, HEAD_DIM)
    heads_out = heads_out.reshape(batch_rows, heads_here * HEAD_DIM).astype(jnp.bfloat16)
    partial_value = jnp.dot(heads_out, w_out, preferred_element_type=jnp.float32)
    own_part = lax.psum_scatter(partial_value, "kv", scatter_dimension=1, tiled=True)
    own_hidden = lax.optimization_barrier(
        (tokens.astype(jnp.float32) + own_part).astype(jnp.bfloat16)
    )
    hidden = lax.all_gather(own_hidden, "kv", axis=1, tiled=True)
    normed_mlp = rms_rows(hidden, mlp_gain)
    squared = jnp.square(jax.nn.relu(jnp.dot(normed_mlp, w_up, preferred_element_type=jnp.float32)))
    squared = squared.astype(jnp.bfloat16)
    partial_mlp = jnp.dot(squared, w_down, preferred_element_type=jnp.float32)
    mlp_part = lax.psum_scatter(partial_mlp, "kv", scatter_dimension=1, tiled=True)
    layer_out = (own_hidden.astype(jnp.float32) + mlp_part).astype(jnp.bfloat16)
    return (layer_out, state_next, value_tail, maps_tail)


def solution(mesh):
    in_specs = (
        P(("dp", "tp"), "kv"),
        P(),
        P(None, "kv"),
        P(None, "kv"),
        P(None, "kv"),
        P(),
        P(None, "kv"),
        P(None, "kv"),
        P(("dp", "tp"), None, "kv"),
        P(("dp", "tp"), None, "kv"),
        P("kv"),
        P("kv"),
        P("kv"),
        P("kv"),
        P(("dp", "tp"), "kv", None, None),
        P("kv", None),
        P(),
        P(None, "kv"),
        P("kv", None),
    )
    out_specs = (
        P(("dp", "tp"), "kv"),
        P(("dp", "tp"), "kv", None, None),
        P(("dp", "tp"), None, "kv"),
        P(("dp", "tp"), None, "kv"),
    )
    return jax.shard_map(local, mesh=mesh, in_specs=in_specs, out_specs=out_specs, check_vma=False)
```

profile of v0, /device:TPU:0, one launch (start us, length us, event | category | flops | bytes accessed | tf_op | source)
XLA Modules:
  0.0 126.5 jit_solution(10900179025579592787)
XLA Ops:
  7.2 15.4 %all_gather.6 = bf16[24,2048]{1,0:T(8,128)(2,1)S(1)} all-gather(bf16[24,512]{1,0:T(8,128)(2,1)} %param.19), channel_id=1, replica_groups=mesh['dp'=4,'kv'=4,'tp'=2] {'kv'}, dimensions={1}, use_global_device_ids=true | all-gather | bytes 122880 | tf_op jit(solution)/shard_map/all_gather | solution.py:46
  22.6 0.1 fusion.6
  22.8 0.7 exp.34
  23.5 1.0 multiply_exponential_fusion
  24.5 2.9 %fusion.3 = bf16[24,1,1024]{2,0,1:T(8,128)(2,1)S(1)} fusion(bf16[2048,1024]{1,0:T(8,128)(2,1)} %param.22, bf16[24,2048]{1,0:T(8,128)(2,1)S(1)} %all_gather.6, f32[2048]{0:T(1024)} %param.20, f32[24]{0:T(128)S(1)} %add_rsqrt_fusion.2), kind=kOutput, calls=%fused_computation.9 | convolution fusion | flops 100884480 | bytes 4350048 | tf_op jit(solution)/shard_map/dot_general | solution.py:54
  27.4 1.0 multiply_reduce_fusion.2
  28.5 8.2 %fusion = bf16[24,1,4096]{2,0,1:T(8,128)(2,1)S(1)} fusion(bf16[2048,4096]{1,0:T(8,128)(2,1)} %param.23, bf16[24,2048]{1,0:T(8,128)(2,1)S(1)} %all_gather.6, f32[2048]{0:T(1024)} %param.20, f32[24]{0:T(128)S(1)} %add_rsqrt_fusion.2), kind=kOutput, calls=%fused_computation.3 | convolution fusion | flops 402948096 | bytes 17080416 | tf_op jit(solution)/shard_map/dot_general | solution.py:55
  36.8 0.2 multiply_reduce_fusion.1
  37.1 0.4 reshape.76
  37.5 0.3 fusion.35
  37.8 2.9 %fusion.30 = f32[24,1024]{1,0:T(8,128)S(1)} fusion(bf16[2048,1024]{1,0:T(8,128)(2,1)} %param.21, bf16[24,2048]{1,0:T(8,128)(2,1)S(1)} %all_gather.6, f32[2048]{0:T(1024)S(1)} %copy-done.4, f32[24]{0:T(128)S(1)} %add_rsqrt_fusion.2), kind=kOutput, calls=%fused_computation.54 | convolution fusion | flops 100859904 | bytes 4399200 | tf_op jit(solution)/shard_map/dot_general | solution.py:51
  40.8 0.1 broadcast_multiply_fusion
  41.0 11.1 %multiply_reduce_fusion = (f32[24,16,64]{2,1,0:T(8,128)S(1)}, f32[24,16,64,128]{3,2,1,0:T(8,128)}) fusion(f32[24,16,128]{2,1,0:T(8,128)S(1)} %bitcast.13, f32[24,16,128]{2,1,0:T(8,128)S(1)} %bitcast.12, f32[24,16,64]{2,1,0:T(8,128)S(1)} %broadcast_multiply_fusion, f32[24,16,64,128]{3,2,1,0:T(8,128)} %param.33, f32[24,16]{1,0:T(8,128)S(1)} %copy.25), kind=kLoop, calls=%fused_computation | loop fusion | flops 15704064 | bytes 25757184 | tf_op jit(solution)/shard_map/reduce_sum | solution.py:69
  52.2 0.2 multiply_reduce_fusion.3
  52.8 3.5 %fusion.21 = f32[24,2048]{1,0:T(8,128)} fusion(bf16[1024,2048]{1,0:T(8,128)(2,1)} %param.34, f32[24,1024]{1,0:T(8,128)S(1)} %mul.217, f32[24,1024]{1,0:T(8,128)S(1)} %fusion.30, f32[24,1024]{1,0:T(8,128)S(1)} %reduce_sum.63, f32[24,1024]{1,0:T(8,128)S(1)} %multiply_reduce_fusion.2, f32[1024]{0:T(1024)S(1)} %copy-done.8, f32[1024]{0:T(1024)S(1)} %mul.205), kind=kOutput, calls=%fused_computation.40 | convolution fusion | flops 101007360 | bytes 4792320 | tf_op jit(solution)/shard_map/dot_general | solution.py:76
  56.4 0.7 fusion.12
  57.1 20.1 %reduce-scatter.3.cloned.1.call-done = f32[24,512]{1,0:T(8,128)} async-done(((f32[24,2048]{1,0:T(8,128)}), f32[24,512]{1,0:T(8,128)}) %reduce-scatter.3.cloned.1.call-update) | async-done | bytes 49168 | tf_op jit(solution)/shard_map/reduce_scatter | solution.py:77
  77.2 0.8 add_convert_fusion.1
  78.0 13.2 %all_gather.7 = bf16[24,2048]{1,0:T(8,128)(2,1)S(1)} all-gather(bf16[24,512]{1,0:T(8,128)(2,1)S(1)} %add_convert_fusion.1), channel_id=1, replica_groups=mesh['dp'=4,'kv'=4,'tp'=2] {'kv'}, dimensions={1}, use_global_device_ids=true | all-gather | bytes 122880 | tf_op jit(solution)/shard_map/all_gather | solution.py:81
  91.3 0.1 fusion.9
  91.4 8.8 %fusion.4 = f32[24,2048]{1,0:T(8,128)} fusion(bf16[2048,2048]{1,0:T(8,128)(2,1)} %param.37, bf16[2048,2048]{1,0:T(8,128)(2,1)} %param.36, bf16[24,2048]{1,0:T(8,128)(2,1)S(1)} %all_gather.7, f32[2048]{0:T(1024)S(1)} %copy-done.7, f32[24]{0:T(128)S(1)} %add_rsqrt_fusion.1), kind=kOutput, calls=%fused_computation.14 | convolution fusion | flops 402997248 | bytes 17080416 | tf_op jit(solution)/shard_map/dot_general | solution.py:85
  100.3 0.9 fusion.5
  101.2 17.1 %reduce-scatter.5.cloned.1.call-done = f32[24,512]{1,0:T(8,128)} async-done(((f32[24,2048]{1,0:T(8,128)}), f32[24,512]{1,0:T(8,128)}) %reduce-scatter.5.cloned.1.call-update) | async-done | bytes 49168 | tf_op jit(solution)/shard_map/reduce_scatter | solution.py:86
  118.2 1.4 %add_convert_fusion = bf16[24,512]{1,0:T(8,128)(2,1)} fusion(f32[24,512]{1,0:T(8,128)} %reduce-scatter.5.cloned.1.call-done, bf16[24,512]{1,0:T(8,128)(2,1)S(1)} %add_convert_fusion.1), kind=kLoop, calls=%fused_computation.41 | loop fusion | flops 36864 | bytes 98304 | tf_op jit(solution)/shard_map/convert_element_type | solution.py:87
  (37 shorter events, 1.1 us)
Async XLA Ops:
  7.2 16.3 %copy-start = (bf16[2048,64]{0,1:T(8,128)(2,1)S(1)}, bf16[2048,64]{0,1:T(8,128)(2,1)}, u32[]{:S(2)}) copy-start(bf16[2048,64]{0,1:T(8,128)(2,1)} %param.24) | copy-start | bytes 786436
  7.2 70.0 %reduce-scatter.3.cloned.1.call-start = ((), (), s32[]{:S(2)}) async-start(), calls=%async_computation.2 | async-start | bytes 245760 | tf_op jit(solution)/shard_map/reduce_scatter | solution.py:77
  28.5 8.2 %copy-start.2 = (bf16[24,3,4096]{2,0,1:T(8,128)(2,1)S(1)}, bf16[24,3,4096]{2,0,1:T(8,128)(2,1)}, u32[]{:S(2)}) copy-start(bf16[24,3,4096]{2,0,1:T(8,128)(2,1)} %param.28) | copy-start | bytes 1769476
  28.5 8.2 %copy-start.6 = (f32[4,4096]{1,0:T(4,128)S(1)}, f32[4,4096]{1,0:T(4,128)}, u32[]{:S(2)}) copy-start(f32[4,4096]{1,0:T(4,128)} %param.26) | copy-start | bytes 196612
  28.5 9.2 %copy-start.4 = (f32[2048]{0:T(1024)S(1)}, f32[2048]{0:T(1024)}, u32[]{:S(2)}) copy-start(f32[2048]{0:T(1024)} %param.20) | copy-start | bytes 24580
  40.9 11.2 %copy-start.9 = (f32[16]{0:T(128)S(1)}, f32[16]{0:T(128)}, u32[]{:S(2)}) copy-start(f32[16]{0:T(128)} %param.31) | copy-start | bytes 196
  40.9 11.9 %copy-start.8 = (f32[1024]{0:T(1024)S(1)}, f32[1024]{0:T(1024)}, u32[]{:S(2)}) copy-start(f32[1024]{0:T(1024)} %param.32) | copy-start | bytes 12292
  40.9 15.5 %copy-start.3 = (bf16[24,3,1024]{2,0,1:T(8,128)(2,1)S(1)}, bf16[24,3,1024]{2,0,1:T(8,128)(2,1)}, u32[]{:S(2)}) copy-start(bf16[24,3,1024]{2,0,1:T(8,128)(2,1)} %param.27) | copy-start | bytes 442372
  40.9 36.3 %copy-start.5 = (bf16[24,512]{1,0:T(8,128)(2,1)S(1)}, bf16[24,512]{1,0:T(8,128)(2,1)}, u32[]{:S(2)}) copy-start(bf16[24,512]{1,0:T(8,128)(2,1)} %param.19) | copy-start | bytes 73732
  41.0 50.5 %copy-start.7 = (f32[2048]{0:T(1024)S(1)}, f32[2048]{0:T(1024)}, u32[]{:S(2)}) copy-start(f32[2048]{0:T(1024)} %param.35) | copy-start | bytes 24580
  56.3 61.9 %reduce-scatter.5.cloned.1.call-start = ((), (), s32[]{:S(2)}) async-start(), calls=%async_computation.3 | async-start | bytes 245760 | tf_op jit(solution)/shard_map/reduce_scatter | solution.py:86
  91.4 28.3 %copy-start.1 = (bf16[2048,64]{0,1:T(8,128)(2,1)S(1)}, bf16[2048,64]{0,1:T(8,128)(2,1)}, u32[]{:S(2)}) copy-start(bf16[2048,64]{0,1:T(8,128)(2,1)} %param.24) | copy-start | bytes 786436
Sparse Core Ops, SparseCore 0:
  56.5 20.7 reduce-scatter.2
  100.4 17.7 reduce-scatter.4
where the time goes:
time: 127 us
  waiting for transfers between devices  37.3 us (29%)
  blocking collectives  28.6 us (23%)
  matrix products  27.3 us (21%)
  other arithmetic  16.7 us (13%)
  between operations  14.2 us (11%)
  local copies, waits for them, and re-layouts  2.25 us (2%)
    reduce_scatter x1, waiting for transfers between devices, local(): lax.psum_scatter(partial_value, 'kv', scatter_dimension=1, tiled=True)  20.1 us
    reduce_scatter x1, waiting for transfers between devices, local(): lax.psum_scatter(partial_mlp, 'kv', scatter_dimension=1, tiled=True)  17.1 us
    all_gather x1, blocking collectives, local(): whole_rows = lax.all_gather(tokens, 'kv', axis=1, tiled=True)  15.4 us
    all_gather x1, blocking collectives, local(): hidden = lax.all_gather(own_hidden, 'kv', axis=1, tiled=True)  13.2 us
    reduce_sum x1, other arithmetic, local(): jnp.sum(state_next * out_map[:, :, None, :], axis=-1)  11.1 us
    dot_general x1, matrix products, local(): partial_mlp = jnp.dot(squared, w_down, preferred_element_type=jnp.float32)  8.84 us
    dot_general x1, matrix products, local(): jnp.dot(normed, w_maps, preferred_element_type=jnp.float32)  8.19 us
    dot_general x1, matrix products, local(): jnp.dot(heads_out, w_out, preferred_element_type=jnp.float32)  3.55 us
  transfers between devices with their start and end apart: 2, of which 2 were waited for; matrix products, arithmetic and copies ran while one was open for 1% of the time, Pallas kernels for 0%

commit v1 on v0

--- a/solution.py
+++ b/solution.py
@@ -1,3 +1,5 @@
+import functools
+
 import jax
 import jax.numpy as jnp
 from jax import lax
@@ -22,7 +24,39 @@
     return (jax.nn.silu(summed), window[:, 1:, :])
 
 
+def shifted(block, axis_name, size, step):
+    return lax.ppermute(block, axis_name, [(i, (i + step) % size) for i in range(size)])
+
+
+def gather_columns(block, axis_name, size):
+    me = lax.axis_index(axis_name)
+    width = block.shape[1]
+    whole = jnp.zeros((block.shape[0], width * size), block.dtype)
+    pieces = [block] + [shifted(block, axis_name, size, step) for step in range(1, size)]
+    for step, piece in enumerate(pieces):
+        source = lax.rem(me + size - step, size)
+        whole = lax.dynamic_update_slice_in_dim(whole, piece, source * width, 1)
+    return whole
+
+
+def scatter_sum(partial, axis_name, size):
+    me = lax.axis_index(axis_name)
+    width = partial.shape[1] // size
+    rounded = partial.astype(jnp.bfloat16)
+    total = lax.dynamic_slice_in_dim(partial, me * width, width, 1)
+    for step in range(1, size):
+        target = lax.rem(me + step, size)
+        piece = lax.dynamic_slice_in_dim(rounded, target * width, width, 1)
+        total = total + shifted(piece, axis_name, size, step).astype(jnp.float32)
+    return total
+
+
+def few_peers(size):
+    return size <= 8
+
+
 def local(
+    size,
     tokens,
     mix_gain,
     w_gate,
@@ -43,7 +77,10 @@
     w_up,
     w_down,
 ):
-    whole_rows = lax.all_gather(tokens, "kv", axis=1, tiled=True)
+    if few_peers(size):
+        whole_rows = gather_columns(tokens, "kv", size)
+    else:
+        whole_rows = lax.all_gather(tokens, "kv", axis=1, tiled=True)
     batch_rows = whole_rows.shape[0]
     heads_here = state.shape[1]
     head_start = lax.axis_index("kv") * heads_here
@@ -74,16 +111,25 @@
     heads_out = gated_heads * inv_scale * head_gain.reshape(heads_here, HEAD_DIM)
     heads_out = heads_out.reshape(batch_rows, heads_here * HEAD_DIM).astype(jnp.bfloat16)
     partial_value = jnp.dot(heads_out, w_out, preferred_element_type=jnp.float32)
-    own_part = lax.psum_scatter(partial_value, "kv", scatter_dimension=1, tiled=True)
+    if few_peers(size):
+        own_part = scatter_sum(partial_value, "kv", size)
+    else:
+        own_part = lax.psum_scatter(partial_value, "kv", scatter_dimension=1, tiled=True)
     own_hidden = lax.optimization_barrier(
         (tokens.astype(jnp.float32) + own_part).astype(jnp.bfloat16)
     )
-    hidden = lax.all_gather(own_hidden, "kv", axis=1, tiled=True)
+    if few_peers(size):
+        hidden = gather_columns(own_hidden, "kv", size)
+    else:
+        hidden = lax.all_gather(own_hidden, "kv", axis=1, tiled=True)
     normed_mlp = rms_rows(hidden, mlp_gain)
     squared = jnp.square(jax.nn.relu(jnp.dot(normed_mlp, w_up, preferred_element_type=jnp.float32)))
     squared = squared.astype(jnp.bfloat16)
     partial_mlp = jnp.dot(squared, w_down, preferred_element_type=jnp.float32)
-    mlp_part = lax.psum_scatter(partial_mlp, "kv", scatter_dimension=1, tiled=True)
+    if few_peers(size):
+        mlp_part = scatter_sum(partial_mlp, "kv", size)
+    else:
+        mlp_part = lax.psum_scatter(partial_mlp, "kv", scatter_dimension=1, tiled=True)
     layer_out = (own_hidden.astype(jnp.float32) + mlp_part).astype(jnp.bfloat16)
     return (layer_out, state_next, value_tail, maps_tail)
 
@@ -116,4 +162,5 @@
         P(("dp", "tp"), None, "kv"),
         P(("dp", "tp"), None, "kv"),
     )
-    return jax.shard_map(local, mesh=mesh, in_specs=in_specs, out_specs=out_specs, check_vma=False)
+    step = functools.partial(local, mesh.shape["kv"])
+    return jax.shard_map(step, mesh=mesh, in_specs=in_specs, out_specs=out_specs, check_vma=False)

time: 127 us -> 75.8 us (0.60)
  blocking collectives: 28.6 us -> 0 us
  waiting for transfers between devices: 37.3 us -> 10.9 us
  starting transfers between devices: 0.08 us -> 18.9 us
  between operations: 14.2 us -> 0.86 us
  other arithmetic: 16.7 us -> 15.1 us
  local copies, waits for them, and re-layouts: 2.25 us -> 3.74 us
  matrix products: 27.3 us -> 26 us
    reduce_scatter x2 -> x0, waiting for transfers between devices: 37.2 us -> none  [the longest x1 20.1 us: local(): lax.psum_scatter(partial_value, 'kv', scatter_dimension=1, tiled=True)]
    all_gather x2 -> x0, blocking collectives: 28.6 us -> none  [the longest x1 15.4 us: local(): whole_rows = lax.all_gather(tokens, 'kv', axis=1, tiled=True)]
    ppermute x0 -> x12, starting transfers between devices: none -> 18.9 us  [shifted(): lax.ppermute(block, axis_name, [(i, (i + step) % size) for i in range(siz...]
    ppermute x0 -> x12, waiting for transfers between devices: none -> 10.9 us  [shifted(): lax.ppermute(block, axis_name, [(i, (i + step) % size) for i in range(siz...]
  transfers between devices with their start and end apart: 2 -> 12, of which waited for: 2 -> 8; matrix products, arithmetic and copies ran while one was open for 1% -> 5% of each run, Pallas kernels for 0% -> 0%
where the time goes in v1:
time: 75.8 us; the launch traced here: 75.5 us
  matrix products  26 us (34%)
  starting transfers between devices  18.9 us (25%)
  other arithmetic  15.1 us (20%)
  waiting for transfers between devices  10.9 us (14%)
  local copies, waits for them, and re-layouts  3.74 us (5%)
  between operations  0.86 us (1%)
    ppermute x12, starting transfers between devices, shifted(): lax.ppermute(block, axis_name, [(i, (i + step) % size) for i in range(siz...  18.9 us
    reduce_sum x1, other arithmetic, local(): jnp.sum(state_next * out_map[:, :, None, :], axis=-1)  11 us
    ppermute x12, waiting for transfers between devices, shifted(): lax.ppermute(block, axis_name, [(i, (i + step) % size) for i in range(siz...  10.9 us
    dot_general x1, matrix products, local(): jnp.dot(normed, w_maps, preferred_element_type=jnp.float32)  8.19 us
    dot_general x1, matrix products, local(): partial_mlp = jnp.dot(squared, w_down, preferred_element_type=jnp.float32)  8.19 us
    dot_general x1, matrix products, local(): jnp.dot(normed, w_value, preferred_element_type=jnp.float32)  2.91 us
    dot_general x1, matrix products, local(): gate_pre = jnp.dot(normed, w_gate, preferred_element_type=jnp.float32)  2.89 us
    dot_general x1, matrix products, local(): jnp.dot(heads_out, w_out, preferred_element_type=jnp.float32)  2.86 us
  transfers between devices with their start and end apart: 12, of which 8 were waited for; matrix products, arithmetic and copies ran while one was open for 5% of the time, Pallas kernels for 0%

profile of v1, /device:TPU:0, one launch (start us, length us, event | category | flops | bytes accessed | tf_op | source)
XLA Modules:
  0.0 75.5 jit_solution(14073067170065230739)
XLA Ops:
  0.6 3.1 %collective-permute-start = (bf16[24,512]{1,0:T(8,128)(2,1)}, bf16[24,512]{1,0:T(8,128)(2,1)S(1)}, u32[]{:S(2)}, u32[]{:S(2)}) collective-permute-start(bf16[24,512]{1,0:T(8,128)(2,1)} %param.19), channel_id=1, source_target_pairs={{0,2},{2,4},{4,6},{6,0},{1,3},{3,5},{5,7},{7,1},{8,10},{10,12},{12... | collective-permute-start | bytes 73736 | tf_op jit(solution)/shard_map/ppermute | solution.py:28
  3.8 2.6 %collective-permute-start.1 = (bf16[24,512]{1,0:T(8,128)(2,1)}, bf16[24,512]{1,0:T(8,128)(2,1)S(1)}, u32[]{:S(2)}, u32[]{:S(2)}) collective-permute-start(bf16[24,512]{1,0:T(8,128)(2,1)} %param.19), channel_id=1, source_target_pairs={{0,4},{2,6},{4,0},{6,2},{1,5},{3,7},{5,1},{7,3},{8,12},{10,14},{12... | collective-permute-start | bytes 73736 | tf_op jit(solution)/shard_map/ppermute | solution.py:28
  6.3 1.3 %collective-permute-start.2 = (bf16[24,512]{1,0:T(8,128)(2,1)}, bf16[24,512]{1,0:T(8,128)(2,1)S(1)}, u32[]{:S(2)}, u32[]{:S(2)}) collective-permute-start(bf16[24,512]{1,0:T(8,128)(2,1)} %param.19), channel_id=1, source_target_pairs={{0,6},{2,0},{4,2},{6,4},{1,7},{3,1},{5,3},{7,5},{8,14},{10,8},{12,... | collective-permute-start | bytes 73736 | tf_op jit(solution)/shard_map/ppermute | solution.py:28
  7.7 0.8 %constant_dynamic-update-slice_fusion.7 = bf16[24,2048]{1,0:T(8,128)(2,1)S(1)} fusion(bf16[24,2048]{1,0:T(8,128)(2,1)S(1)} %broadcast.87.clone, bf16[24,512]{1,0:T(8,128)(2,1)} %param.19, s32[]{:T(128)S(6)} %select_n.16), kind=kLoop, calls=%fused_computation.63 | loop fusion | bytes 49156 | tf_op jit(solution)/shard_map/dynamic_update_slice | solution.py:38
  10.5 2.9 %fusion.3 = bf16[24,1,1024]{2,0,1:T(8,128)(2,1)S(1)} fusion(bf16[2048,1024]{1,0:T(8,128)(2,1)} %param.22, bf16[24,2048]{1,0:T(8,128)(2,1)S(1)} %constant_dynamic-update-slice_fusion.4, f32[2048]{0:T(1024)} %param.20, f32[24]{0:T(128)S(1)} %add_rsqrt_fusion.2), kind=kOutput, calls=%fused_computation.9 | convolution fusion | flops 100884480 | bytes 4350048 | tf_op jit(solution)/shard_map/dot_general | solution.py:91
  13.4 1.0 %multiply_reduce_fusion.2 = f32[24,1024]{1,0:T(8,128)S(1)} fusion(bf16[24,1,1024]{2,0,1:T(8,128)(2,1)S(1)} %fusion.3, bf16[24,3,1024]{2,0,1:T(8,128)(2,1)} %param.27, f32[4,1024]{1,0:T(4,128)} %param.25), kind=kLoop, calls=%fused_computation.17 | loop fusion | flops 368640 | bytes 311296 | tf_op jit(solution)/shard_map/reduce_sum | solution.py:23
  14.5 1.0 %multiply_exponential_fusion = (f32[24,16]{0,1:T(8,128)S(1)}, f32[24,16]{0,1:T(8,128)S(1)}) fusion(f32[16]{0:T(128)S(1)} %exp.34, f32[16]{0:T(128)} %param.29, bf16[2048,64]{0,1:T(8,128)(2,1)S(1)} %copy-done, s32[]{:T(128)S(6)} %select_n.37, bf16[24,2048]{1,0:T(8,128)(2,1)S(1)} %constant_dynamic-update-slice_fusion.4, f32[2048]{0:T(1024)} %param.20, ...), kind=kOutput, calls=%fused_computation.48 | convolution fusion | flops 1772928 | bytes 176196 | tf_op jit(solution)/shard_map/dot_general | solution.py:90
  15.6 8.2 %fusion = bf16[24,1,4096]{2,0,1:T(8,128)(2,1)S(1)} fusion(bf16[2048,4096]{1,0:T(8,128)(2,1)} %param.23, bf16[24,2048]{1,0:T(8,128)(2,1)S(1)} %constant_dynamic-update-slice_fusion.4, f32[2048]{0:T(1024)} %param.20, f32[24]{0:T(128)S(1)} %add_rsqrt_fusion.2), kind=kOutput, calls=%fused_computation.3 | convolution fusion | flops 402948096 | bytes 17080416 | tf_op jit(solution)/shard_map/dot_general | solution.py:92
  24.9 2.9 %fusion.30 = f32[24,1024]{1,0:T(8,128)S(1)} fusion(bf16[2048,1024]{1,0:T(8,128)(2,1)} %param.21, bf16[24,2048]{1,0:T(8,128)(2,1)S(1)} %constant_dynamic-update-slice_fusion.4, f32[2048]{0:T(1024)S(1)} %copy-done.4, f32[24]{0:T(128)S(1)} %add_rsqrt_fusion.2), kind=kOutput, calls=%fused_computation.68 | convolution fusion | flops 100859904 | bytes 4399200 | tf_op jit(solution)/shard_map/dot_general | solution.py:88
  28.0 11.0 %multiply_reduce_fusion = (f32[24,16,64]{2,1,0:T(8,128)S(1)}, f32[24,16,64,128]{3,2,1,0:T(8,128)}) fusion(f32[24,16,128]{2,1,0:T(8,128)S(1)} %bitcast.13, f32[24,16,128]{2,1,0:T(8,128)S(1)} %bitcast.12, f32[24,16,64]{2,1,0:T(8,128)S(1)} %broadcast_multiply_fusion, f32[24,16,64,128]{3,2,1,0:T(8,128)} %param.33, f32[24,16]{1,0:T(8,128)S(1)} %copy.25), kind=kLoop, calls=%fused_computation | loop fusion | flops 15704064 | bytes 25757184 | tf_op jit(solution)/shard_map/reduce_sum | solution.py:106
  39.6 2.9 %fusion.36 = (bf16[24,2048]{1,0:T(8,128)(2,1)S(1)}, f32[24,2048]{1,0:T(8,128)S(1)}) fusion(bf16[1024,2048]{1,0:T(8,128)(2,1)} %param.34, f32[24,1024]{1,0:T(8,128)S(1)} %mul.247, f32[24,1024]{1,0:T(8,128)S(1)} %fusion.30, f32[24,1024]{1,0:T(8,128)S(1)} %reduce_sum.63, f32[24,1024]{1,0:T(8,128)S(1)} %multiply_reduce_fusion.2, f32[1024]{0:T(1024)S(1)} %copy-done.8, ...), kind=kOutput, calls=%fused_computation.70 | convolution fusion | flops 101056512 | bytes 4890624 | tf_op jit(solution)/shard_map/dot_general | solution.py:113
  42.9 3.4 %collective-permute-start.4 = (bf16[24,512]{1,0:T(8,128)(2,1)S(1)}, bf16[24,512]{1,0:T(8,128)(2,1)S(1)}, u32[]{:S(2)}, u32[]{:S(2)}) collective-permute-start(bf16[24,512]{1,0:T(8,128)(2,1)S(1)} %get-tuple-element.13), channel_id=1, source_target_pairs={{0,4},{2,6},{4,0},{6,2},{1,5},{3,7},{5,1},{7,3},{8,12},{10,14},{12... | collective-permute-start | bytes 73736 | tf_op jit(solution)/shard_map/ppermute | solution.py:28
  46.4 0.9 %fusion.5 = bf16[24,3,4096]{2,0,1:T(8,128)(2,1)} fusion(bf16[24,3,4096]{2,0,1:T(8,128)(2,1)S(1)} %copy-done.2, bf16[24,1,4096]{2,0,1:T(8,128)(2,1)S(1)} %fusion), kind=kLoop, calls=%fused_computation.15 | loop fusion | flops 294912 | bytes 1376256 | tf_op jit(solution)/shard_map/concatenate | solution.py:22
  47.3 1.0 %collective-permute-done.3 = bf16[24,512]{1,0:T(8,128)(2,1)S(1)} collective-permute-done((bf16[24,512]{1,0:T(8,128)(2,1)S(1)}, bf16[24,512]{1,0:T(8,128)(2,1)S(1)}, u32[]{:S(2)}, u32[]{:S(2)}) %collective-permute-start.3) | collective-permute-done | bytes 24608 | tf_op jit(solution)/shard_map/ppermute | solution.py:28
  48.6 1.5 %collective-permute-done.5 = bf16[24,512]{1,0:T(8,128)(2,1)S(1)} collective-permute-done((bf16[24,512]{1,0:T(8,128)(2,1)S(1)}, bf16[24,512]{1,0:T(8,128)(2,1)S(1)}, u32[]{:S(2)}, u32[]{:S(2)}) %collective-permute-start.5) | collective-permute-done | bytes 24608 | tf_op jit(solution)/shard_map/ppermute | solution.py:28
  50.9 2.0 %collective-permute-start.7 = (bf16[24,512]{1,0:T(8,128)(2,1)S(1)}, bf16[24,512]{1,0:T(8,128)(2,1)S(1)}, u32[]{:S(2)}, u32[]{:S(2)}) collective-permute-start(bf16[24,512]{1,0:T(8,128)(2,1)S(1)} %add_convert_fusion.1), channel_id=1, source_target_pairs={{0,4},{2,6},{4,0},{6,2},{1,5},{3,7},{5,1},{7,3},{8,12},{10,14},{12... | collective-permute-start | bytes 73736 | tf_op jit(solution)/shard_map/ppermute | solution.py:28
  52.9 1.1 %collective-permute-start.8 = (bf16[24,512]{1,0:T(8,128)(2,1)S(1)}, bf16[24,512]{1,0:T(8,128)(2,1)S(1)}, u32[]{:S(2)}, u32[]{:S(2)}) collective-permute-start(bf16[24,512]{1,0:T(8,128)(2,1)S(1)} %add_convert_fusion.1), channel_id=1, source_target_pairs={{0,6},{2,0},{4,2},{6,4},{1,7},{3,1},{5,3},{7,5},{8,14},{10,8},{12,... | collective-permute-start | bytes 73736 | tf_op jit(solution)/shard_map/ppermute | solution.py:28
  54.1 1.8 %collective-permute-done.6 = bf16[24,512]{1,0:T(8,128)(2,1)S(1)} collective-permute-done((bf16[24,512]{1,0:T(8,128)(2,1)S(1)}, bf16[24,512]{1,0:T(8,128)(2,1)S(1)}, u32[]{:S(2)}, u32[]{:S(2)}) %collective-permute-start.6) | collective-permute-done | bytes 24608 | tf_op jit(solution)/shard_map/ppermute | solution.py:28
  55.9 0.9 %collective-permute-done.8 = bf16[24,512]{1,0:T(8,128)(2,1)S(1)} collective-permute-done((bf16[24,512]{1,0:T(8,128)(2,1)S(1)}, bf16[24,512]{1,0:T(8,128)(2,1)S(1)}, u32[]{:S(2)}, u32[]{:S(2)}) %collective-permute-start.8) | collective-permute-done | bytes 24608 | tf_op jit(solution)/shard_map/ppermute | solution.py:28
  56.9 8.2 %fusion.37 = (bf16[24,2048]{1,0:T(8,128)(2,1)S(1)}, f32[24,2048]{1,0:T(8,128)S(1)}) fusion(bf16[2048,2048]{1,0:T(8,128)(2,1)} %param.37, bf16[2048,2048]{1,0:T(8,128)(2,1)} %param.36, bf16[24,2048]{1,0:T(8,128)(2,1)S(1)} %constant_dynamic-update-slice_fusion, f32[2048]{0:T(1024)S(1)} %copy-done.7, f32[24]{0:T(128)S(1)} %add_rsqrt_fusion.1), kind=kOutput, calls=%fused_computation.71 | convolution fusion | flops 403046400 | bytes 17178720 | tf_op jit(solution)/shard_map/dot_general | solution.py:128
  65.1 1.0 %collective-permute-start.10 = (bf16[24,512]{1,0:T(8,128)(2,1)S(1)}, bf16[24,512]{1,0:T(8,128)(2,1)S(1)}, u32[]{:S(2)}, u32[]{:S(2)}) collective-permute-start(bf16[24,512]{1,0:T(8,128)(2,1)S(1)} %get-tuple-element.10), channel_id=1, source_target_pairs={{0,4},{2,6},{4,0},{6,2},{1,5},{3,7},{5,1},{7,3},{8,12},{10,14},{12... | collective-permute-start | bytes 73736 | tf_op jit(solution)/shard_map/ppermute | solution.py:28
  66.1 3.1 %collective-permute-start.11 = (bf16[24,512]{1,0:T(8,128)(2,1)S(1)}, bf16[24,512]{1,0:T(8,128)(2,1)S(1)}, u32[]{:S(2)}, u32[]{:S(2)}) collective-permute-start(bf16[24,512]{1,0:T(8,128)(2,1)S(1)} %get-tuple-element.9), channel_id=1, source_target_pairs={{0,6},{2,0},{4,2},{6,4},{1,7},{3,1},{5,3},{7,5},{8,14},{10,8},{12,... | collective-permute-start | bytes 73736 | tf_op jit(solution)/shard_map/ppermute | solution.py:28
  69.9 0.8 %collective-permute-done.11 = bf16[24,512]{1,0:T(8,128)(2,1)S(1)} collective-permute-done((bf16[24,512]{1,0:T(8,128)(2,1)S(1)}, bf16[24,512]{1,0:T(8,128)(2,1)S(1)}, u32[]{:S(2)}, u32[]{:S(2)}) %collective-permute-start.11) | collective-permute-done | bytes 24608 | tf_op jit(solution)/shard_map/ppermute | solution.py:28
  70.7 4.1 %collective-permute-done.9 = bf16[24,512]{1,0:T(8,128)(2,1)S(1)} collective-permute-done((bf16[24,512]{1,0:T(8,128)(2,1)S(1)}, bf16[24,512]{1,0:T(8,128)(2,1)S(1)}, u32[]{:S(2)}, u32[]{:S(2)}) %collective-permute-start.9) | collective-permute-done | bytes 24608 | tf_op jit(solution)/shard_map/ppermute | solution.py:28
  (65 shorter events, 7.2 us)
Async XLA Ops:
  0.6 13.9 %copy-start = (bf16[2048,64]{0,1:T(8,128)(2,1)S(1)}, bf16[2048,64]{0,1:T(8,128)(2,1)}, u32[]{:S(2)}) copy-start(bf16[2048,64]{0,1:T(8,128)(2,1)} %param.24) | copy-start | bytes 786436
  0.6 9.3 %collective-permute-start = (bf16[24,512]{1,0:T(8,128)(2,1)}, bf16[24,512]{1,0:T(8,128)(2,1)S(1)}, u32[]{:S(2)}, u32[]{:S(2)}) collective-permute-start(bf16[24,512]{1,0:T(8,128)(2,1)} %param.19), channel_id=1, source_target_pairs={{0,2},{2,4},{4,6},{6,0},{1,3},{3,5},{5,7},{7,1},{8,10},{10,12},{12... | collective-permute-start | bytes 73736 | tf_op jit(solution)/shard_map/ppermute | solution.py:28
  3.8 6.2 %collective-permute-start.1 = (bf16[24,512]{1,0:T(8,128)(2,1)}, bf16[24,512]{1,0:T(8,128)(2,1)S(1)}, u32[]{:S(2)}, u32[]{:S(2)}) collective-permute-start(bf16[24,512]{1,0:T(8,128)(2,1)} %param.19), channel_id=1, source_target_pairs={{0,4},{2,6},{4,0},{6,2},{1,5},{3,7},{5,1},{7,3},{8,12},{10,14},{12... | collective-permute-start | bytes 73736 | tf_op jit(solution)/shard_map/ppermute | solution.py:28
  6.3 4.0 %collective-permute-start.2 = (bf16[24,512]{1,0:T(8,128)(2,1)}, bf16[24,512]{1,0:T(8,128)(2,1)S(1)}, u32[]{:S(2)}, u32[]{:S(2)}) collective-permute-start(bf16[24,512]{1,0:T(8,128)(2,1)} %param.19), channel_id=1, source_target_pairs={{0,6},{2,0},{4,2},{6,4},{1,7},{3,1},{5,3},{7,5},{8,14},{10,8},{12,... | collective-permute-start | bytes 73736 | tf_op jit(solution)/shard_map/ppermute | solution.py:28
  15.6 8.2 %copy-start.2 = (bf16[24,3,4096]{2,0,1:T(8,128)(2,1)S(1)}, bf16[24,3,4096]{2,0,1:T(8,128)(2,1)}, u32[]{:S(2)}) copy-start(bf16[24,3,4096]{2,0,1:T(8,128)(2,1)} %param.28) | copy-start | bytes 1769476
  15.6 8.2 %copy-start.6 = (f32[4,4096]{1,0:T(4,128)S(1)}, f32[4,4096]{1,0:T(4,128)}, u32[]{:S(2)}) copy-start(f32[4,4096]{1,0:T(4,128)} %param.26) | copy-start | bytes 196612
  15.6 9.3 %copy-start.4 = (f32[2048]{0:T(1024)S(1)}, f32[2048]{0:T(1024)}, u32[]{:S(2)}) copy-start(f32[2048]{0:T(1024)} %param.20) | copy-start | bytes 24580
  28.0 11.2 %copy-start.9 = (f32[16]{0:T(128)S(1)}, f32[16]{0:T(128)}, u32[]{:S(2)}) copy-start(f32[16]{0:T(128)} %param.31) | copy-start | bytes 196
  28.0 11.6 %copy-start.8 = (f32[1024]{0:T(1024)S(1)}, f32[1024]{0:T(1024)}, u32[]{:S(2)}) copy-start(f32[1024]{0:T(1024)} %param.32) | copy-start | bytes 12292
  28.0 22.1 %copy-start.5 = (bf16[24,512]{1,0:T(8,128)(2,1)S(1)}, bf16[24,512]{1,0:T(8,128)(2,1)}, u32[]{:S(2)}) copy-start(bf16[24,512]{1,0:T(8,128)(2,1)} %param.19) | copy-start | bytes 73732
  39.0 17.9 %copy-start.7 = (f32[2048]{0:T(1024)S(1)}, f32[2048]{0:T(1024)}, u32[]{:S(2)}) copy-start(f32[2048]{0:T(1024)} %param.35) | copy-start | bytes 24580
  42.5 5.8 %collective-permute-start.3 = (bf16[24,512]{1,0:T(8,128)(2,1)S(1)}, bf16[24,512]{1,0:T(8,128)(2,1)S(1)}, u32[]{:S(2)}, u32[]{:S(2)}) collective-permute-start(bf16[24,512]{1,0:T(8,128)(2,1)S(1)} %get-tuple-element.11), channel_id=1, source_target_pairs={{0,2},{2,4},{4,6},{6,0},{1,3},{3,5},{5,7},{7,1},{8,10},{10,12},{12... | collective-permute-start | bytes 73736 | tf_op jit(solution)/shard_map/ppermute | solution.py:28
  42.9 5.8 %collective-permute-start.4 = (bf16[24,512]{1,0:T(8,128)(2,1)S(1)}, bf16[24,512]{1,0:T(8,128)(2,1)S(1)}, u32[]{:S(2)}, u32[]{:S(2)}) collective-permute-start(bf16[24,512]{1,0:T(8,128)(2,1)S(1)} %get-tuple-element.13), channel_id=1, source_target_pairs={{0,4},{2,6},{4,0},{6,2},{1,5},{3,7},{5,1},{7,3},{8,12},{10,14},{12... | collective-permute-start | bytes 73736 | tf_op jit(solution)/shard_map/ppermute | solution.py:28
  46.3 3.8 %collective-permute-start.5 = (bf16[24,512]{1,0:T(8,128)(2,1)S(1)}, bf16[24,512]{1,0:T(8,128)(2,1)S(1)}, u32[]{:S(2)}, u32[]{:S(2)}) collective-permute-start(bf16[24,512]{1,0:T(8,128)(2,1)S(1)} %get-tuple-element.12), channel_id=1, source_target_pairs={{0,6},{2,0},{4,2},{6,4},{1,7},{3,1},{5,3},{7,5},{8,14},{10,8},{12,... | collective-permute-start | bytes 73736 | tf_op jit(solution)/shard_map/ppermute | solution.py:28
  50.1 5.7 %collective-permute-start.6 = (bf16[24,512]{1,0:T(8,128)(2,1)S(1)}, bf16[24,512]{1,0:T(8,128)(2,1)S(1)}, u32[]{:S(2)}, u32[]{:S(2)}) collective-permute-start(bf16[24,512]{1,0:T(8,128)(2,1)S(1)} %add_convert_fusion.1), channel_id=1, source_target_pairs={{0,2},{2,4},{4,6},{6,0},{1,3},{3,5},{5,7},{7,1},{8,10},{10,12},{12... | collective-permute-start | bytes 73736 | tf_op jit(solution)/shard_map/ppermute | solution.py:28
  50.9 5.0 %collective-permute-start.7 = (bf16[24,512]{1,0:T(8,128)(2,1)S(1)}, bf16[24,512]{1,0:T(8,128)(2,1)S(1)}, u32[]{:S(2)}, u32[]{:S(2)}) collective-permute-start(bf16[24,512]{1,0:T(8,128)(2,1)S(1)} %add_convert_fusion.1), channel_id=1, source_target_pairs={{0,4},{2,6},{4,0},{6,2},{1,5},{3,7},{5,1},{7,3},{8,12},{10,14},{12... | collective-permute-start | bytes 73736 | tf_op jit(solution)/shard_map/ppermute | solution.py:28
  52.9 3.8 %collective-permute-start.8 = (bf16[24,512]{1,0:T(8,128)(2,1)S(1)}, bf16[24,512]{1,0:T(8,128)(2,1)S(1)}, u32[]{:S(2)}, u32[]{:S(2)}) collective-permute-start(bf16[24,512]{1,0:T(8,128)(2,1)S(1)} %add_convert_fusion.1), channel_id=1, source_target_pairs={{0,6},{2,0},{4,2},{6,4},{1,7},{3,1},{5,3},{7,5},{8,14},{10,8},{12,... | collective-permute-start | bytes 73736 | tf_op jit(solution)/shard_map/ppermute | solution.py:28
  56.9 18.6 %copy-start.1 = (bf16[2048,64]{0,1:T(8,128)(2,1)S(1)}, bf16[2048,64]{0,1:T(8,128)(2,1)}, u32[]{:S(2)}) copy-start(bf16[2048,64]{0,1:T(8,128)(2,1)} %param.24) | copy-start | bytes 786436
  56.9 12.3 %copy-start.3 = (bf16[24,3,1024]{2,0,1:T(8,128)(2,1)S(1)}, bf16[24,3,1024]{2,0,1:T(8,128)(2,1)}, u32[]{:S(2)}) copy-start(bf16[24,3,1024]{2,0,1:T(8,128)(2,1)} %param.27) | copy-start | bytes 442372
  65.1 4.8 %collective-permute-start.10 = (bf16[24,512]{1,0:T(8,128)(2,1)S(1)}, bf16[24,512]{1,0:T(8,128)(2,1)S(1)}, u32[]{:S(2)}, u32[]{:S(2)}) collective-permute-start(bf16[24,512]{1,0:T(8,128)(2,1)S(1)} %get-tuple-element.10), channel_id=1, source_target_pairs={{0,4},{2,6},{4,0},{6,2},{1,5},{3,7},{5,1},{7,3},{8,12},{10,14},{12... | collective-permute-start | bytes 73736 | tf_op jit(solution)/shard_map/ppermute | solution.py:28
  66.1 4.6 %collective-permute-start.11 = (bf16[24,512]{1,0:T(8,128)(2,1)S(1)}, bf16[24,512]{1,0:T(8,128)(2,1)S(1)}, u32[]{:S(2)}, u32[]{:S(2)}) collective-permute-start(bf16[24,512]{1,0:T(8,128)(2,1)S(1)} %get-tuple-element.9), channel_id=1, source_target_pairs={{0,6},{2,0},{4,2},{6,4},{1,7},{3,1},{5,3},{7,5},{8,14},{10,8},{12,... | collective-permute-start | bytes 73736 | tf_op jit(solution)/shard_map/ppermute | solution.py:28
  69.2 5.6 %collective-permute-start.9 = (bf16[24,512]{1,0:T(8,128)(2,1)S(1)}, bf16[24,512]{1,0:T(8,128)(2,1)S(1)}, u32[]{:S(2)}, u32[]{:S(2)}) collective-permute-start(bf16[24,512]{1,0:T(8,128)(2,1)S(1)} %get-tuple-element.8), channel_id=1, source_target_pairs={{0,2},{2,4},{4,6},{6,0},{1,3},{3,5},{5,7},{7,1},{8,10},{10,12},{12... | collective-permute-start | bytes 73736 | tf_op jit(solution)/shard_map/ppermute | solution.py:28

commit v2 on v0

--- a/solution.py
+++ b/solution.py
@@ -1,13 +1,23 @@
+import functools
+
 import jax
 import jax.numpy as jnp
 from jax import lax
+from jax.experimental import pallas as pl
+from jax.experimental.pallas import tpu as pltpu
 from jax.sharding import PartitionSpec as P
 
 HEAD_DIM = 64
 STATE = 128
+LANES = 128
+TILE = 512
 
 
 NORM_EPS = 1e-05
+
+VMEM = pl.BlockSpec(memory_space=pltpu.VMEM)
+SMEM = pl.BlockSpec(memory_space=pltpu.SMEM)
+HBM = pl.BlockSpec(memory_space=pltpu.HBM)
 
 
 def rms_rows(matrix, gain_vec):
@@ -22,7 +32,7 @@
     return (jax.nn.silu(summed), window[:, 1:, :])
 
 
-def local(
+def local_many(
     tokens,
     mix_gain,
     w_gate,
@@ -88,6 +98,380 @@
     return (layer_out, state_next, value_tail, maps_tail)
 
 
+def shifted(block, size, step):
+    return lax.ppermute(block, "kv", [(i, (i + step) % size) for i in range(size)])
+
+
+def in_hbm(array):
+    return pltpu.with_memory_space_constraint(array, pltpu.HBM)
+
+
+def cost(flops, moved):
+    return pl.CostEstimate(flops=int(flops), bytes_accessed=int(moved), transcendentals=0)
+
+
+def silu(x):
+    return x / (1.0 + jnp.exp(-x))
+
+
+def fetch_kernel(parts, *refs):
+    count = (len(refs) - 1) // 2
+    sources, targets, sems = refs[-1 - 2 * count : -1 - count], refs[-1 - count : -1], refs[-1]
+    copies = []
+    for which in range(count):
+        rows = sources[which].shape[0] // parts
+        for part in range(parts):
+            block = pl.ds(part * rows, rows)
+            copies.append(
+                pltpu.make_async_copy(
+                    sources[which].at[block], targets[which].at[block], sems.at[which * parts + part]
+                )
+            )
+    for copy in copies:
+        copy.start()
+    for copy in copies:
+        copy.wait()
+
+
+def fetch(after, arrays, name, flops, parts=4):
+    moved = sum(a.size * a.dtype.itemsize for a in arrays)
+    first = [] if after is None else [after]
+    return pl.pallas_call(
+        functools.partial(fetch_kernel, parts),
+        out_shape=[pltpu.VMEM(a.shape, a.dtype) for a in arrays],
+        in_specs=[pl.BlockSpec(memory_space=pl.ANY)] * len(first) + [HBM] * len(arrays),
+        out_specs=[VMEM] * len(arrays),
+        scratch_shapes=[pltpu.SemaphoreType.DMA((parts * len(arrays),))],
+        compiler_params=pltpu.CompilerParams(vmem_limit_bytes=1 << 20),
+        cost_estimate=cost(flops, 2 * moved),
+        name=name,
+    )(*first, *[in_hbm(a) for a in arrays])
+
+
+def mixer_kernel(size, *refs):
+    me_ref, bias_ref, dlog_ref, skip_ref = refs[:4]
+    chunks = refs[4 : 4 + size]
+    (gain, wstep, conv_v, conv_m, hgain, wmaps, past_v, past_m, wvalue, wgate, state, wout) = refs[
+        4 + size : 16 + size
+    ]
+    (part_o, x_o, state_o, dec_o, in_o, u_o, vtail, mtail) = refs[16 + size : 24 + size]
+    (wvalue_s, wgate_s, wout_s, pastv_s, pastm_s, newv_s, newm_s, out_s, value_s, gate_s, heads_s, sems, ssems) = refs[
+        24 + size :
+    ]
+    rows, width = chunks[0].shape
+    me = me_ref[0]
+    heads = state.shape[1]
+    pairs = heads // 2
+
+    def state_copy(pair):
+        both = pl.ds(2 * pair, 2)
+        return pltpu.make_async_copy(state.at[:, both], state_o.at[:, both], ssems.at[pair])
+
+    loads = [
+        pltpu.make_async_copy(past_m, pastm_s, sems.at[0]),
+        pltpu.make_async_copy(past_v, pastv_s, sems.at[1]),
+        pltpu.make_async_copy(wvalue, wvalue_s, sems.at[2]),
+        pltpu.make_async_copy(wgate, wgate_s, sems.at[3]),
+    ]
+    for copy in loads:
+        copy.start()
+    for pair in range(pairs):
+        state_copy(pair).start()
+    load_out = pltpu.make_async_copy(wout, wout_s, sems.at[4])
+    load_out.start()
+
+    for step in range(size):
+        source = lax.rem(me + size - step, size)
+        x_o[:, pl.ds(pl.multiple_of(source * width, width), width)] = chunks[step][...]
+    x = x_o[...].astype(jnp.float32)
+    inv = lax.rsqrt(jnp.mean(x * x, axis=-1, keepdims=True) + NORM_EPS)
+    normed = (x * inv * gain[...]).astype(jnp.bfloat16)
+
+    step_pre = lax.dot_general(
+        normed, wstep[...], (((1,), (1,)), ((), ())), preferred_element_type=jnp.float32
+    )
+
+    def conv(past, new, taps, block):
+        total = new.astype(jnp.float32) * taps[3:4, block]
+        for t in range(3):
+            total = total + past[t, :, block].astype(jnp.float32) * taps[t : t + 1, block]
+        return silu(total)
+
+    loads[0].wait()
+    tails = [pltpu.make_async_copy(pastm_s.at[pl.ds(1, 2)], mtail.at[pl.ds(0, 2)], sems.at[5])]
+    tails[0].start()
+    for tile in range(wmaps.shape[1] // TILE):
+        block = pl.ds(tile * TILE, TILE)
+        new = jnp.dot(normed, wmaps[:, block], preferred_element_type=jnp.float32).astype(jnp.bfloat16)
+        newm_s[:, block] = new
+        act = conv(pastm_s, new, conv_m, block).astype(jnp.bfloat16).astype(jnp.float32)
+        for half in range(TILE // (2 * STATE)):
+            head = tile * (TILE // (2 * STATE)) + half
+            base = half * 2 * STATE
+            in_o[:, pl.ds(head * STATE, STATE)] = act[:, base : base + STATE]
+            out_s[:, pl.ds(head * STATE, STATE)] = act[:, base + STATE : base + 2 * STATE]
+    tails.append(pltpu.make_async_copy(newm_s, mtail.at[2], sems.at[6]))
+    tails[1].start()
+
+    loads[1].wait()
+    tails.append(pltpu.make_async_copy(pastv_s.at[pl.ds(1, 2)], vtail.at[pl.ds(0, 2)], sems.at[7]))
+    tails[2].start()
+    loads[2].wait()
+    for tile in range(wvalue_s.shape[1] // TILE):
+        block = pl.ds(tile * TILE, TILE)
+        new = jnp.dot(normed, wvalue_s[:, block], preferred_element_type=jnp.float32).astype(jnp.bfloat16)
+        newv_s[:, block] = new
+        value_s[:, block] = conv(pastv_s, new, conv_v, block)
+    tails.append(pltpu.make_async_copy(newv_s, vtail.at[2], sems.at[8]))
+    tails[3].start()
+    loads[3].wait()
+    for tile in range(wgate_s.shape[1] // TILE):
+        block = pl.ds(tile * TILE, TILE)
+        gate_s[:, block] = silu(jnp.dot(normed, wgate_s[:, block], preferred_element_type=jnp.float32))
+
+    lane = lax.broadcasted_iota(jnp.int32, (HEAD_DIM, LANES), 1)
+    low = lax.broadcasted_iota(jnp.int32, (rows, LANES), 1) < HEAD_DIM
+    step_lane = lax.broadcasted_iota(jnp.int32, step_pre.shape, 1)
+
+    def pair_body(pair, carry):
+        state_copy(pair).wait()
+        gathered, decays, sizes, meets = [], [], [], []
+        for which in range(2):
+            head = 2 * pair + which
+            wide = pl.ds(pl.multiple_of(head * STATE, STATE), STATE)
+            column = jnp.sum(
+                jnp.where(step_lane == me * heads + head, step_pre, 0.0), axis=1, keepdims=True
+            )
+            pre = jnp.broadcast_to(column, (rows, LANES)) + bias_ref[head]
+            size_h = jnp.maximum(pre, 0.0) + jnp.log1p(jnp.exp(-jnp.abs(pre)))
+            rate = jnp.exp(jnp.full((rows, LANES), dlog_ref[head]))
+            decay = jnp.exp(-size_h * rate)
+            dec_o[:, wide] = decay
+            out_h = out_s[:, wide]
+            meets.append(jnp.sum(in_o[:, wide] * out_h, axis=1, keepdims=True))
+            decays.append(decay)
+            sizes.append(size_h)
+            total = jnp.zeros((HEAD_DIM, LANES), jnp.float32)
+            for row in range(rows):
+                dots = jnp.sum(state_o[row, head] * out_h[row : row + 1], axis=1, keepdims=True)
+                total = jnp.where(lane == row, dots, total)
+            gathered.append(total)
+        carried = jnp.transpose(jnp.concatenate(gathered, axis=0))[:rows]
+        block = pl.ds(pl.multiple_of(pair * LANES, LANES), LANES)
+        value = value_s[:, block]
+        written = jnp.where(low, sizes[0], sizes[1]) * value
+        u_o[block, :] = jnp.transpose(written)
+        read = jnp.where(low, decays[0], decays[1]) * carried
+        read = read + jnp.where(low, meets[0], meets[1]) * written
+        read = read + jnp.where(low, skip_ref[2 * pair], skip_ref[2 * pair + 1]) * value
+        gated = read * gate_s[:, block]
+        square = gated * gated
+        first = jnp.sum(jnp.where(low, square, 0.0), axis=1, keepdims=True)
+        second = jnp.sum(jnp.where(low, 0.0, square), axis=1, keepdims=True)
+        scale = lax.rsqrt(jnp.where(low, first, second) * (1.0 / HEAD_DIM) + NORM_EPS)
+        heads_s[:, block] = (gated * scale * hgain[:, block]).astype(jnp.bfloat16)
+        return carry
+
+    lax.fori_loop(0, pairs, pair_body, 0)
+
+    load_out.wait()
+    merged = heads_s[...]
+    for tile in range(wout_s.shape[1] // TILE):
+        block = pl.ds(tile * TILE, TILE)
+        part_o[:, block] = jnp.dot(merged, wout_s[:, block], preferred_element_type=jnp.float32).astype(
+            jnp.bfloat16
+        )
+    for copy in tails:
+        copy.wait()
+
+
+def write_kernel(state_ref, dec_ref, in_ref, u_ref, next_ref):
+    rows = state_ref.shape[0]
+    pair = pl.program_id(0)
+    for which in range(2):
+        head = 2 * pair + which
+        wide = pl.ds(pl.multiple_of(head * STATE, STATE), STATE)
+        column = u_ref[pl.ds(pl.multiple_of(head * HEAD_DIM, HEAD_DIM), HEAD_DIM), :]
+        decay, in_map = dec_ref[:, wide], in_ref[:, wide]
+        for row in range(rows):
+            next_ref[row, which] = (
+                state_ref[row, head] * decay[row : row + 1]
+                + column[:, row : row + 1] * in_map[row : row + 1]
+            )
+
+
+def mlp_kernel(size, *refs):
+    me_ref, x_ref = refs[:2]
+    parts = refs[2 : 2 + size]
+    gain, wup, wdown = refs[2 + size : 5 + size]
+    base_o = refs[5 + size]
+    pieces = refs[6 + size : 5 + 2 * size]
+    hidden_s, total_s = refs[5 + 2 * size :]
+    width = base_o.shape[1]
+    me = me_ref[0]
+    total = x_ref[...].astype(jnp.float32)
+    for part in parts:
+        total = total + part[...].astype(jnp.float32)
+    hidden = total.astype(jnp.bfloat16)
+    hidden_s[...] = hidden.astype(jnp.float32)
+    wide = hidden_s[...]
+    inv = lax.rsqrt(jnp.mean(wide * wide, axis=-1, keepdims=True) + NORM_EPS)
+    normed = (wide * inv * gain[...]).astype(jnp.bfloat16)
+    out = None
+    for tile in range(wup.shape[1] // TILE):
+        block = pl.ds(tile * TILE, TILE)
+        up = jnp.maximum(jnp.dot(normed, wup[:, block], preferred_element_type=jnp.float32), 0.0)
+        squared = (up * up).astype(jnp.bfloat16)
+        down = jnp.dot(squared, wdown[block, :], preferred_element_type=jnp.float32)
+        out = down if out is None else out + down
+    total_s[...] = out
+    own = pl.ds(pl.multiple_of(me * width, width), width)
+    base_o[...] = hidden_s[:, own] + total_s[:, own]
+    for step in range(1, size):
+        target = lax.rem(me + step, size)
+        block = pl.ds(pl.multiple_of(target * width, width), width)
+        pieces[step - 1][...] = total_s[:, block].astype(jnp.bfloat16)
+
+
+def local_few(
+    size,
+    tokens,
+    mix_gain,
+    w_gate,
+    w_value,
+    w_maps,
+    w_step,
+    conv_value,
+    conv_maps,
+    past_value,
+    past_maps,
+    step_bias,
+    decay_log,
+    skip_gain,
+    head_gain,
+    state,
+    w_out,
+    mlp_gain,
+    w_up,
+    w_down,
+):
+    f32, bf16 = jnp.float32, jnp.bfloat16
+    rows, width = tokens.shape
+    model = width * size
+    heads = state.shape[1]
+    inner, maps = w_value.shape[1], w_maps.shape[1]
+    me = lax.axis_index("kv").astype(jnp.int32).reshape(1)
+
+    chunks = [tokens] + [shifted(tokens, size, step) for step in range(1, size)]
+    (maps_near,) = fetch(None, [w_maps], "fetch_maps", 1e6)
+    part, whole, held, decay, in_map, written, value_tail, maps_tail = pl.pallas_call(
+        functools.partial(mixer_kernel, size),
+        out_shape=[
+            pltpu.VMEM((rows, model), bf16),
+            pltpu.VMEM((rows, model), bf16),
+            pltpu.VMEM(state.shape, f32),
+            pltpu.VMEM((rows, heads * STATE), f32),
+            pltpu.VMEM((rows, heads * STATE), f32),
+            pltpu.VMEM((inner, rows), f32),
+            jax.ShapeDtypeStruct((3, rows, inner), bf16),
+            jax.ShapeDtypeStruct((3, rows, maps), bf16),
+        ],
+        in_specs=[SMEM] * 4 + [VMEM] * (size + 6) + [HBM] * 6,
+        out_specs=[VMEM] * 6 + [HBM] * 2,
+        scratch_shapes=[
+            pltpu.VMEM(w_value.shape, bf16),
+            pltpu.VMEM(w_gate.shape, bf16),
+            pltpu.VMEM(w_out.shape, bf16),
+            pltpu.VMEM((3, rows, inner), bf16),
+            pltpu.VMEM((3, rows, maps), bf16),
+            pltpu.VMEM((rows, inner), bf16),
+            pltpu.VMEM((rows, maps), bf16),
+            pltpu.VMEM((rows, heads * STATE), f32),
+            pltpu.VMEM((rows, inner), f32),
+            pltpu.VMEM((rows, inner), f32),
+            pltpu.VMEM((rows, inner), bf16),
+            pltpu.SemaphoreType.DMA((9,)),
+            pltpu.SemaphoreType.DMA((heads // 2,)),
+        ],
+        compiler_params=pltpu.CompilerParams(vmem_limit_bytes=20 << 20),
+        cost_estimate=cost(2 * rows * model * (2 * inner + maps), 40e6),
+        name="mixer",
+    )(
+        me,
+        step_bias,
+        decay_log,
+        skip_gain,
+        *chunks,
+        mix_gain.reshape(1, -1),
+        w_step.T,
+        conv_value,
+        conv_maps,
+        head_gain.reshape(1, -1),
+        maps_near,
+        *[
+            in_hbm(a)
+            for a in (
+                past_value.transpose(1, 0, 2),
+                past_maps.transpose(1, 0, 2),
+                w_value,
+                w_gate,
+                state,
+                w_out,
+            )
+        ],
+    )
+
+    parts = [part] + [shifted(part, size, step) for step in range(1, size)]
+    up_near, down_near = fetch(part, [w_up, w_down], "fetch_mlp", 1e6)
+    base, *pieces = pl.pallas_call(
+        functools.partial(mlp_kernel, size),
+        out_shape=[pltpu.VMEM((rows, width), f32)] + [pltpu.VMEM((rows, width), bf16)] * (size - 1),
+        in_specs=[SMEM] + [VMEM] * (size + 4),
+        out_specs=[VMEM] * size,
+        scratch_shapes=[pltpu.VMEM((rows, model), f32), pltpu.VMEM((rows, model), f32)],
+        compiler_params=pltpu.CompilerParams(vmem_limit_bytes=8 << 20),
+        cost_estimate=cost(4 * rows * model * w_up.shape[1], 17e6),
+        name="mlp",
+    )(me, whole, *parts, mlp_gain.reshape(1, -1), up_near, down_near)
+
+    arrived = [shifted(pieces[step - 1], size, step) for step in range(1, size)]
+    held, decay, in_map, written, _ = lax.optimization_barrier((held, decay, in_map, written, base))
+    state_next = pl.pallas_call(
+        write_kernel,
+        out_shape=jax.ShapeDtypeStruct(state.shape, f32),
+        grid=(heads // 2,),
+        in_specs=[VMEM] * 4,
+        out_specs=pl.BlockSpec((rows, 2, HEAD_DIM, STATE), lambda pair: (0, pair, 0, 0)),
+        compiler_params=pltpu.CompilerParams(vmem_limit_bytes=8 << 20),
+        cost_estimate=cost(8e9, 25e6),
+        name="write_state",
+    )(held, decay, in_map, written)
+    total = base
+    for piece in arrived:
+        total = total + piece.astype(f32)
+    return (
+        total.astype(bf16),
+        state_next,
+        value_tail.transpose(1, 0, 2),
+        maps_tail.transpose(1, 0, 2),
+    )
+
+
+def local(size, *arrays):
+    tokens, w_value, w_maps, state, w_up = (arrays[i] for i in (0, 3, 4, 14, 17))
+    heads = state.shape[1]
+    fits = (
+        size <= 8
+        and heads % 2 == 0
+        and state.shape[2:] == (HEAD_DIM, STATE)
+        and w_maps.shape[1] == heads * 2 * STATE
+        and all(extent % TILE == 0 for extent in (w_value.shape[1], w_maps.shape[1], w_up.shape[1]))
+        and tokens.shape[1] % LANES == 0
+        and tokens.shape[0] % 8 == 0
+    )
+    return local_few(size, *arrays) if fits else local_many(*arrays)
+
+
 def solution(mesh):
     in_specs = (
         P(("dp", "tp"), "kv"),
@@ -116,4 +500,5 @@
         P(("dp", "tp"), None, "kv"),
         P(("dp", "tp"), None, "kv"),
     )
-    return jax.shard_map(local, mesh=mesh, in_specs=in_specs, out_specs=out_specs, check_vma=False)
+    step = functools.partial(local, mesh.shape["kv"])
+    return jax.shard_map(step, mesh=mesh, in_specs=in_specs, out_specs=out_specs, check_vma=False)

time: 127 us -> 55.4 us (0.44)
  Pallas kernels: 0 us -> 37.4 us
  waiting for transfers between devices: 37.3 us -> 1.99 us
  blocking collectives: 28.6 us -> 0 us
  matrix products: 27.3 us -> 0 us
  other arithmetic: 16.7 us -> 0.63 us
  starting transfers between devices: 0.08 us -> 14.4 us
  between operations: 14.2 us -> 0.84 us
  local copies, waits for them, and re-layouts: 2.25 us -> 0.04 us
    pallas_call x0 -> x5, Pallas kernels: none -> 37.4 us  [the longest x1 14.8 us: local_few(): pl.pallas_call(functools.partial(mixer_kernel, size), out_shape=[pltpu.VM...]
    reduce_scatter x2 -> x0, waiting for transfers between devices: 37.2 us -> none  [the longest x1 20.1 us: local(): lax.psum_scatter(partial_value, 'kv', scatter_dimension=1, tiled=True)]
    all_gather x2 -> x0, blocking collectives: 28.6 us -> none  [the longest x1 15.4 us: local(): whole_rows = lax.all_gather(tokens, 'kv', axis=1, tiled=True)]
    dot_general x6 -> x0, matrix products: 27.3 us -> none  [the longest x1 8.84 us: local(): partial_mlp = jnp.dot(squared, w_down, preferred_element_type=jnp.float32)]
    ppermute x0 -> x9, starting transfers between devices: none -> 14.4 us  [shifted(): lax.ppermute(block, 'kv', [(i, (i + step) % size) for i in range(size)])]
    reduce_sum x6 -> x0, other arithmetic: 12.7 us -> none  [the longest x1 11.1 us: local(): jnp.sum(state_next * out_map[:, :, None, :], axis=-1)]
    ppermute x0 -> x9, waiting for transfers between devices: none -> 1.99 us  [shifted(): lax.ppermute(block, 'kv', [(i, (i + step) % size) for i in range(size)])]
    convert_element_type x3 -> x1, other arithmetic: 2.33 us -> 0.63 us  [local_few(): total.astype(bf16)]
  transfers between devices with their start and end apart: 2 -> 9, of which waited for: 2 -> 1; matrix products, arithmetic and copies ran while one was open for 1% -> 0% of each run, Pallas kernels for 0% -> 35%
where the time goes in v2:
time: 55.4 us; the launch traced here: 55.2 us
  Pallas kernels  37.4 us (68%)
  starting transfers between devices  14.4 us (26%)
  waiting for transfers between devices  1.99 us (4%)
  between operations  0.84 us (2%)
  other arithmetic  0.63 us (1%)
    pallas_call x1, Pallas kernels, local_few(): pl.pallas_call(functools.partial(mixer_kernel, size), out_shape=[pltpu.VM...  14.8 us
    ppermute x9, starting transfers between devices, shifted(): lax.ppermute(block, 'kv', [(i, (i + step) % size) for i in range(size)])  14.4 us
    pallas_call x2, Pallas kernels, fetch(): pl.pallas_call(functools.partial(fetch_kernel, parts), out_shape=[pltpu.V...  11.8 us
    pallas_call x1, Pallas kernels, local_few(): pl.pallas_call(write_kernel, out_shape=jax.ShapeDtypeStruct(state.shape,...  7.37 us
    pallas_call x1, Pallas kernels, local_few(): pl.pallas_call(functools.partial(mlp_kernel, size), out_shape=[pltpu.VMEM...  3.36 us
    ppermute x9, waiting for transfers between devices, shifted(): lax.ppermute(block, 'kv', [(i, (i + step) % size) for i in range(size)])  1.99 us
  transfers between devices with their start and end apart: 9, of which 1 were waited for; matrix products, arithmetic and copies ran while one was open for 0% of the time, Pallas kernels for 35%

profile of v2, /device:TPU:0, one launch (start us, length us, event | category | flops | bytes accessed | tf_op | source)
XLA Modules:
  0.0 55.2 jit_solution(15974304758798939150)
XLA Ops:
  0.6 4.1 %collective-permute-start.1 = (bf16[24,512]{1,0:T(8,128)(2,1)}, bf16[24,512]{1,0:T(8,128)(2,1)S(1)}, u32[]{:S(2)}, u32[]{:S(2)}) collective-permute-start(bf16[24,512]{1,0:T(8,128)(2,1)} %refs_4_.1), channel_id=1, source_target_pairs={{0,4},{2,6},{4,0},{6,2},{1,5},{3,7},{5,1},{7,3},{8,12},{10,14},{12... | collective-permute-start | bytes 73736 | tf_op jit(solution)/shard_map/ppermute | solution.py:102
  4.8 1.6 %collective-permute-start = (bf16[24,512]{1,0:T(8,128)(2,1)}, bf16[24,512]{1,0:T(8,128)(2,1)S(1)}, u32[]{:S(2)}, u32[]{:S(2)}) collective-permute-start(bf16[24,512]{1,0:T(8,128)(2,1)} %refs_4_.1), channel_id=1, source_target_pairs={{0,2},{2,4},{4,6},{6,0},{1,3},{3,5},{5,7},{7,1},{8,10},{10,12},{12... | collective-permute-start | bytes 73736 | tf_op jit(solution)/shard_map/ppermute | solution.py:102
  6.3 2.2 %collective-permute-start.2 = (bf16[24,512]{1,0:T(8,128)(2,1)}, bf16[24,512]{1,0:T(8,128)(2,1)S(1)}, u32[]{:S(2)}, u32[]{:S(2)}) collective-permute-start(bf16[24,512]{1,0:T(8,128)(2,1)} %refs_4_.1), channel_id=1, source_target_pairs={{0,6},{2,0},{4,2},{6,4},{1,7},{3,1},{5,3},{7,5},{8,14},{10,8},{12,... | collective-permute-start | bytes 73736 | tf_op jit(solution)/shard_map/ppermute | solution.py:102
  8.7 5.9 %fetch_maps.1.refs_13_ = bf16[2048,4096]{1,0:T(8,128)(2,1)S(1)} custom-call(bf16[2048,4096]{1,0:T(8,128)(2,1)} %refs_0_.1), custom_call_target="tpu_custom_call" | custom-call | flops 1000000 | bytes 33554432 | tf_op jit(solution)/shard_map/fetch_maps/pallas_call | solution.py:139
  14.6 0.0 collective-permute-done.1.refs_6_
  14.6 0.0 collective-permute-done.refs_5_
  14.6 0.0 collective-permute-done.2.refs_7_
  14.7 14.8 %mixer.1 = (bf16[24,2048]{1,0:T(8,128)(2,1)S(1)}, bf16[24,2048]{1,0:T(8,128)(2,1)S(1)}, f32[24,16,64,128]{3,2,1,0:T(8,128)S(1)}, f32[24,2048]{1,0:T(8,128)S(1)},...) custom-call(s32[1]{0:T(128)} %bitcast.refs_0_, ...), custom_call_target="tpu_custom_call" | custom-call | flops 603979776 | bytes 40000000 | tf_op jit(solution)/shard_map/mixer/pallas_call | solution.py:367
  29.5 0.0 copy-start.5
  29.5 0.1 collective-permute-start.5
  29.6 1.2 %collective-permute-start.4 = (bf16[24,2048]{1,0:T(8,128)(2,1)S(1)}, bf16[24,2048]{1,0:T(8,128)(2,1)S(1)}, u32[]{:S(2)}, u32[]{:S(2)}) collective-permute-start(bf16[24,2048]{1,0:T(8,128)(2,1)S(1)} %get-tuple-element.23.refs_0_.refs_2_), channel_id=1, source_target_pairs={{0,4},{2,6},{4,0},{6,2},{1,5},{3,7},{5,1},{7,3},{8,12},{10,14},{12... | collective-permute-start | bytes 294920 | tf_op jit(solution)/shard_map/ppermute | solution.py:102
  30.8 0.8 %collective-permute-start.3 = (bf16[24,2048]{1,0:T(8,128)(2,1)S(1)}, bf16[24,2048]{1,0:T(8,128)(2,1)S(1)}, u32[]{:S(2)}, u32[]{:S(2)}) collective-permute-start(bf16[24,2048]{1,0:T(8,128)(2,1)S(1)} %get-tuple-element.23.refs_0_.refs_2_), channel_id=1, source_target_pairs={{0,2},{2,4},{4,6},{6,0},{1,3},{3,5},{5,7},{7,1},{8,10},{10,12},{12... | collective-permute-start | bytes 294920 | tf_op jit(solution)/shard_map/ppermute | solution.py:102
  31.6 5.9 %fetch_mlp.1 = (bf16[2048,2048]{1,0:T(8,128)(2,1)S(1)}, bf16[2048,2048]{1,0:T(8,128)(2,1)S(1)}) custom-call(bf16[24,2048]{1,0:T(8,128)(2,1)S(1)} %get-tuple-element.23.refs_0_.refs_2_, bf16[2048,2048]{1,0:T(8,128)(2,1)} %refs_1_.3, bf16[2048,2048]{1,0:T(8,128)(2,1)} %refs_2_.3), custom_call_target="tpu_custom_call" | custom-call | flops 1000000 | bytes 33554432 | tf_op jit(solution)/shard_map/fetch_mlp/pallas_call | solution.py:139
  37.5 0.0 collective-permute-done.5.refs_5_
  37.5 2.0 %collective-permute-done.4.refs_4_ = bf16[24,2048]{1,0:T(8,128)(2,1)S(1)} collective-permute-done((bf16[24,2048]{1,0:T(8,128)(2,1)S(1)}, bf16[24,2048]{1,0:T(8,128)(2,1)S(1)}, u32[]{:S(2)}, u32[]{:S(2)}) %collective-permute-start.4) | collective-permute-done | bytes 98336 | tf_op jit(solution)/shard_map/ppermute | solution.py:102
  39.5 0.0 collective-permute-done.3.refs_3_
  39.5 3.4 %mlp.1 = (f32[24,512]{1,0:T(8,128)S(1)}, bf16[24,512]{1,0:T(8,128)(2,1)S(1)}, bf16[24,512]{1,0:T(8,128)(2,1)S(1)}, bf16[24,512]{1,0:T(8,128)(2,1)S(1)}) custom-call(s32[1]{0:T(128)} %bitcast.refs_0_, bf16[24,2048]{1,0:T(8,128)(2,1)S(1)} %get-tuple-element.22.refs_1_, bf16[24,2048]{1,0:T(8,128)(2,1)S(1)} %get-tuple-element.23.refs_0_.refs_2_, ...), custom_call_target="tpu_custom_call" | custom-call | flops 402653184 | bytes 17000000 | tf_op jit(solution)/shard_map/mlp/pallas_call | solution.py:426
  42.9 0.1 collective-permute-start.6
  42.9 1.6 %collective-permute-start.7 = (bf16[24,512]{1,0:T(8,128)(2,1)S(1)}, bf16[24,512]{1,0:T(8,128)(2,1)S(1)}, u32[]{:S(2)}, u32[]{:S(2)}) collective-permute-start(bf16[24,512]{1,0:T(8,128)(2,1)S(1)} %get-tuple-element.28), channel_id=1, source_target_pairs={{0,4},{2,6},{4,0},{6,2},{1,5},{3,7},{5,1},{7,3},{8,12},{10,14},{12... | collective-permute-start | bytes 73736 | tf_op jit(solution)/shard_map/ppermute | solution.py:102
  44.6 2.6 %collective-permute-start.8 = (bf16[24,512]{1,0:T(8,128)(2,1)S(1)}, bf16[24,512]{1,0:T(8,128)(2,1)S(1)}, u32[]{:S(2)}, u32[]{:S(2)}) collective-permute-start(bf16[24,512]{1,0:T(8,128)(2,1)S(1)} %get-tuple-element.29), channel_id=1, source_target_pairs={{0,6},{2,0},{4,2},{6,4},{1,7},{3,1},{5,3},{7,5},{8,14},{10,8},{12,... | collective-permute-start | bytes 73736 | tf_op jit(solution)/shard_map/ppermute | solution.py:102
  47.2 7.4 %write_state.1 = f32[24,16,64,128]{3,2,1,0:T(8,128)} custom-call(f32[24,16,64,128]{3,2,1,0:T(8,128)S(1)} %get-tuple-element.34.state_ref, f32[24,2048]{1,0:T(8,128)S(1)} %get-tuple-element.35.dec_ref, f32[24,2048]{1,0:T(8,128)S(1)} %get-tuple-element.36.in_ref, f32[1024,24]{1,0:T(8,128)S(1)} %get-tuple-element.37.u_ref), custom_call_target="tpu_custom_call" | custom-call | flops 8000000000 | bytes 25000000 | tf_op jit(solution)/shard_map/write_state/pallas_call | solution.py:439
  54.6 0.0 collective-permute-done.6
  54.6 0.0 collective-permute-done.7
  54.6 0.6 %add_convert_fusion = bf16[24,512]{1,0:T(8,128)(2,1)} fusion(bf16[24,512]{1,0:T(8,128)(2,1)S(1)} %collective-permute-done.8, bf16[24,512]{1,0:T(8,128)(2,1)S(1)} %collective-permute-done.7, f32[24,512]{1,0:T(8,128)S(1)} %get-tuple-element.26, bf16[24,512]{1,0:T(8,128)(2,1)S(1)} %collective-permute-done.6), kind=kLoop, calls=%fused_computation | loop fusion | flops 86016 | bytes 147456 | tf_op jit(solution)/shard_map/convert_element_type | solution.py:453
  (20 shorter events, 0.0 us)
Async XLA Ops:
  0.6 13.9 %collective-permute-start.1 = (bf16[24,512]{1,0:T(8,128)(2,1)}, bf16[24,512]{1,0:T(8,128)(2,1)S(1)}, u32[]{:S(2)}, u32[]{:S(2)}) collective-permute-start(bf16[24,512]{1,0:T(8,128)(2,1)} %refs_4_.1), channel_id=1, source_target_pairs={{0,4},{2,6},{4,0},{6,2},{1,5},{3,7},{5,1},{7,3},{8,12},{10,14},{12... | collective-permute-start | bytes 73736 | tf_op jit(solution)/shard_map/ppermute | solution.py:102
  4.8 9.8 %collective-permute-start = (bf16[24,512]{1,0:T(8,128)(2,1)}, bf16[24,512]{1,0:T(8,128)(2,1)S(1)}, u32[]{:S(2)}, u32[]{:S(2)}) collective-permute-start(bf16[24,512]{1,0:T(8,128)(2,1)} %refs_4_.1), channel_id=1, source_target_pairs={{0,2},{2,4},{4,6},{6,0},{1,3},{3,5},{5,7},{7,1},{8,10},{10,12},{12... | collective-permute-start | bytes 73736 | tf_op jit(solution)/shard_map/ppermute | solution.py:102
  6.3 8.3 %collective-permute-start.2 = (bf16[24,512]{1,0:T(8,128)(2,1)}, bf16[24,512]{1,0:T(8,128)(2,1)S(1)}, u32[]{:S(2)}, u32[]{:S(2)}) collective-permute-start(bf16[24,512]{1,0:T(8,128)(2,1)} %refs_4_.1), channel_id=1, source_target_pairs={{0,6},{2,0},{4,2},{6,4},{1,7},{3,1},{5,3},{7,5},{8,14},{10,8},{12,... | collective-permute-start | bytes 73736 | tf_op jit(solution)/shard_map/ppermute | solution.py:102
  8.6 6.0 %copy-start = (bf16[2048,64]{0,1:T(8,128)(2,1)S(1)}, bf16[2048,64]{0,1:T(8,128)(2,1)}, u32[]{:S(2)}) copy-start(bf16[2048,64]{0,1:T(8,128)(2,1)} %param.24) | copy-start | bytes 786436
  8.6 6.0 %copy-start.1 = (f32[4,4096]{1,0:T(4,128)S(1)}, f32[4,4096]{1,0:T(4,128)}, u32[]{:S(2)}) copy-start(f32[4,4096]{1,0:T(4,128)} %refs_11_.1) | copy-start | bytes 196612
  8.6 6.0 %copy-start.2 = (bf16[24,512]{1,0:T(8,128)(2,1)S(1)}, bf16[24,512]{1,0:T(8,128)(2,1)}, u32[]{:S(2)}) copy-start(bf16[24,512]{1,0:T(8,128)(2,1)} %refs_4_.1) | copy-start | bytes 73732
  8.6 6.0 %copy-start.3 = (f32[4,1024]{1,0:T(4,128)S(1)}, f32[4,1024]{1,0:T(4,128)}, u32[]{:S(2)}) copy-start(f32[4,1024]{1,0:T(4,128)} %refs_10_.1) | copy-start | bytes 49156
  8.6 6.1 %copy-start.4 = (f32[2048]{0:T(1024)S(1)}, f32[2048]{0:T(1024)}, u32[]{:S(2)}) copy-start(f32[2048]{0:T(1024)} %param.20) | copy-start | bytes 24580
  8.6 6.1 %copy-start.6 = (f32[1024]{0:T(1024)S(1)}, f32[1024]{0:T(1024)}, u32[]{:S(2)}) copy-start(f32[1024]{0:T(1024)} %param.32) | copy-start | bytes 12292
  8.6 6.1 %copy-start.7 = (f32[16]{0:T(128)S(1)}, f32[16]{0:T(128)}, u32[]{:S(2)}) copy-start(f32[16]{0:T(128)} %refs_1_.2) | copy-start | bytes 196
  8.6 6.1 %copy-start.8 = (f32[16]{0:T(128)S(1)}, f32[16]{0:T(128)}, u32[]{:S(2)}) copy-start(f32[16]{0:T(128)} %refs_2_.2) | copy-start | bytes 196
  8.6 6.1 %copy-start.9 = (f32[16]{0:T(128)S(1)}, f32[16]{0:T(128)}, u32[]{:S(2)}) copy-start(f32[16]{0:T(128)} %refs_3_.1) | copy-start | bytes 196
  29.5 10.0 %copy-start.5 = (f32[2048]{0:T(1024)S(1)}, f32[2048]{0:T(1024)}, u32[]{:S(2)}) copy-start(f32[2048]{0:T(1024)} %param.35) | copy-start | bytes 24580
  29.5 8.0 %collective-permute-start.5 = (bf16[24,2048]{1,0:T(8,128)(2,1)S(1)}, bf16[24,2048]{1,0:T(8,128)(2,1)S(1)}, u32[]{:S(2)}, u32[]{:S(2)}) collective-permute-start(bf16[24,2048]{1,0:T(8,128)(2,1)S(1)} %get-tuple-element.23.refs_0_.refs_2_), channel_id=1, source_target_pairs={{0,6},{2,0},{4,2},{6,4},{1,7},{3,1},{5,3},{7,5},{8,14},{10,8},{12,... | collective-permute-start | bytes 294920 | tf_op jit(solution)/shard_map/ppermute | solution.py:102
  29.6 9.9 %collective-permute-start.4 = (bf16[24,2048]{1,0:T(8,128)(2,1)S(1)}, bf16[24,2048]{1,0:T(8,128)(2,1)S(1)}, u32[]{:S(2)}, u32[]{:S(2)}) collective-permute-start(bf16[24,2048]{1,0:T(8,128)(2,1)S(1)} %get-tuple-element.23.refs_0_.refs_2_), channel_id=1, source_target_pairs={{0,4},{2,6},{4,0},{6,2},{1,5},{3,7},{5,1},{7,3},{8,12},{10,14},{12... | collective-permute-start | bytes 294920 | tf_op jit(solution)/shard_map/ppermute | solution.py:102
  30.8 8.7 %collective-permute-start.3 = (bf16[24,2048]{1,0:T(8,128)(2,1)S(1)}, bf16[24,2048]{1,0:T(8,128)(2,1)S(1)}, u32[]{:S(2)}, u32[]{:S(2)}) collective-permute-start(bf16[24,2048]{1,0:T(8,128)(2,1)S(1)} %get-tuple-element.23.refs_0_.refs_2_), channel_id=1, source_target_pairs={{0,2},{2,4},{4,6},{6,0},{1,3},{3,5},{5,7},{7,1},{8,10},{10,12},{12... | collective-permute-start | bytes 294920 | tf_op jit(solution)/shard_map/ppermute | solution.py:102
  42.9 11.7 %collective-permute-start.6 = (bf16[24,512]{1,0:T(8,128)(2,1)S(1)}, bf16[24,512]{1,0:T(8,128)(2,1)S(1)}, u32[]{:S(2)}, u32[]{:S(2)}) collective-permute-start(bf16[24,512]{1,0:T(8,128)(2,1)S(1)} %get-tuple-element.27), channel_id=1, source_target_pairs={{0,2},{2,4},{4,6},{6,0},{1,3},{3,5},{5,7},{7,1},{8,10},{10,12},{12... | collective-permute-start | bytes 73736 | tf_op jit(solution)/shard_map/ppermute | solution.py:102
  42.9 11.6 %collective-permute-start.7 = (bf16[24,512]{1,0:T(8,128)(2,1)S(1)}, bf16[24,512]{1,0:T(8,128)(2,1)S(1)}, u32[]{:S(2)}, u32[]{:S(2)}) collective-permute-start(bf16[24,512]{1,0:T(8,128)(2,1)S(1)} %get-tuple-element.28), channel_id=1, source_target_pairs={{0,4},{2,6},{4,0},{6,2},{1,5},{3,7},{5,1},{7,3},{8,12},{10,14},{12... | collective-permute-start | bytes 73736 | tf_op jit(solution)/shard_map/ppermute | solution.py:102
  44.6 10.0 %collective-permute-start.8 = (bf16[24,512]{1,0:T(8,128)(2,1)S(1)}, bf16[24,512]{1,0:T(8,128)(2,1)S(1)}, u32[]{:S(2)}, u32[]{:S(2)}) collective-permute-start(bf16[24,512]{1,0:T(8,128)(2,1)S(1)} %get-tuple-element.29), channel_id=1, source_target_pairs={{0,6},{2,0},{4,2},{6,4},{1,7},{3,1},{5,3},{7,5},{8,14},{10,8},{12,... | collective-permute-start | bytes 73736 | tf_op jit(solution)/shard_map/ppermute | solution.py:102

commit v3 on v2

v3 whole, which is shorter than its diff:
```python
import functools

import jax
import jax.numpy as jnp
from jax import lax
from jax.experimental import pallas as pl
from jax.experimental.pallas import tpu as pltpu
from jax.sharding import PartitionSpec as P

HEAD_DIM = 64
STATE = 128
LANES = 128
TILE = 1024
SLOTS = 3
GROUP = 4


NORM_EPS = 1e-05

VMEM = pl.BlockSpec(memory_space=pltpu.VMEM)
SMEM = pl.BlockSpec(memory_space=pltpu.SMEM)
HBM = pl.BlockSpec(memory_space=pltpu.HBM)


def rms_rows(matrix, gain_vec):
    widened = matrix.astype(jnp.float32)
    inv_scale = lax.rsqrt(jnp.mean(widened * widened, axis=-1, keepdims=True) + NORM_EPS)
    return (widened * inv_scale * gain_vec).astype(jnp.bfloat16)


def short_conv(past_rows, newest, kernel):
    window = jnp.concatenate([past_rows, newest[:, None, :]], axis=1)
    summed = jnp.sum(window.astype(jnp.float32) * kernel[None], axis=1)
    return (jax.nn.silu(summed), window[:, 1:, :])


def local_many(
    tokens,
    mix_gain,
    w_gate,
    w_value,
    w_maps,
    w_step,
    conv_value,
    conv_maps,
    past_value,
    past_maps,
    step_bias,
    decay_log,
    skip_gain,
    head_gain,
    state,
    w_out,
    mlp_gain,
    w_up,
    w_down,
):
    whole_rows = lax.all_gather(tokens, "kv", axis=1, tiled=True)
    batch_rows = whole_rows.shape[0]
    heads_here = state.shape[1]
    head_start = lax.axis_index("kv") * heads_here
    normed = rms_rows(whole_rows, mix_gain)
    gate_pre = jnp.dot(normed, w_gate, preferred_element_type=jnp.float32)
    step_cols = lax.dynamic_slice_in_dim(w_step, head_start, heads_here, 1)
    step_pre = jnp.dot(normed, step_cols, preferred_element_type=jnp.float32)
    value_new = jnp.dot(normed, w_value, preferred_element_type=jnp.float32).astype(jnp.bfloat16)
    maps_new = jnp.dot(normed, w_maps, preferred_element_type=jnp.float32).astype(jnp.bfloat16)
    value_act, value_tail = short_conv(past_value, value_new, conv_value)
    maps_act, maps_tail = short_conv(past_maps, maps_new, conv_maps)
    maps_act = lax.optimization_barrier(maps_act.astype(jnp.bfloat16))
    grouped = maps_act.astype(jnp.float32).reshape(batch_rows, -1, 2, STATE)
    per_group = heads_here // grouped.shape[1]
    in_map = jnp.repeat(grouped[:, :, 0], per_group, axis=1)
    out_map = jnp.repeat(grouped[:, :, 1], per_group, axis=1)
    head_values = value_act.reshape(batch_rows, heads_here, HEAD_DIM)
    step_size = jax.nn.softplus(step_pre + step_bias)
    decay_rate = jnp.exp(-step_size * jnp.exp(decay_log))
    written = (step_size[:, :, None] * head_values)[:, :, :, None] * in_map[:, :, None, :]
    state_next = decay_rate[:, :, None, None] * state + written
    read_out = (
        jnp.sum(state_next * out_map[:, :, None, :], axis=-1)
        + skip_gain[None, :, None] * head_values
    )
    gated_heads = read_out * jax.nn.silu(gate_pre.reshape(batch_rows, heads_here, HEAD_DIM))
    inv_scale = lax.rsqrt(jnp.mean(gated_heads * gated_heads, axis=-1, keepdims=True) + NORM_EPS)
    heads_out = gated_heads * inv_scale * head_gain.reshape(heads_here, HEAD_DIM)
    heads_out = heads_out.reshape(batch_rows, heads_here * HEAD_DIM).astype(jnp.bfloat16)
    partial_value = jnp.dot(heads_out, w_out, preferred_element_type=jnp.float32)
    own_part = lax.psum_scatter(partial_value, "kv", scatter_dimension=1, tiled=True)
    own_hidden = lax.optimization_barrier(
        (tokens.astype(jnp.float32) + own_part).astype(jnp.bfloat16)
    )
    hidden = lax.all_gather(own_hidden, "kv", axis=1, tiled=True)
    normed_mlp = rms_rows(hidden, mlp_gain)
    squared = jnp.square(jax.nn.relu(jnp.dot(normed_mlp, w_up, preferred_element_type=jnp.float32)))
    squared = squared.astype(jnp.bfloat16)
    partial_mlp = jnp.dot(squared, w_down, preferred_element_type=jnp.float32)
    mlp_part = lax.psum_scatter(partial_mlp, "kv", scatter_dimension=1, tiled=True)
    layer_out = (own_hidden.astype(jnp.float32) + mlp_part).astype(jnp.bfloat16)
    return (layer_out, state_next, value_tail, maps_tail)


def shifted(block, size, step):
    return lax.ppermute(block, "kv", [(i, (i + step) % size) for i in range(size)])


def in_hbm(array):
    return pltpu.with_memory_space_constraint(array, pltpu.HBM)


def cost(flops, moved):
    return pl.CostEstimate(flops=int(flops), bytes_accessed=int(moved), transcendentals=0)


def silu(x):
    return x / (1.0 + jnp.exp(-x))


def row_copies(source, target, sems, first, parts):
    depth = source.shape[0] // parts
    blocks = [pl.ds(part * depth, depth) for part in range(parts)]
    return [
        pltpu.make_async_copy(source.at[block], target.at[block], sems.at[first + part])
        for part, block in enumerate(blocks)
    ]


def fetch_kernel(parts, *refs):
    count = len(parts)
    sources, targets, sems = refs[:count], refs[count:-1], refs[-1]
    copies = []
    for source, target, number in zip(sources, targets, parts):
        copies += row_copies(source, target, sems, len(copies), number)
    for copy in copies:
        copy.start()
    for copy in copies:
        copy.wait()


def fetch(arrays, parts, name):
    moved = sum(a.size * a.dtype.itemsize for a in arrays)
    return pl.pallas_call(
        functools.partial(fetch_kernel, parts),
        out_shape=[pltpu.VMEM(a.shape, a.dtype) for a in arrays],
        in_specs=[HBM] * len(arrays),
        out_specs=[VMEM] * len(arrays),
        scratch_shapes=[pltpu.SemaphoreType.DMA((sum(parts),))],
        compiler_params=pltpu.CompilerParams(vmem_limit_bytes=1 << 20),
        cost_estimate=cost(1e6, 2 * moved),
        name=name,
    )(*[in_hbm(a) for a in arrays])


def mixer_kernel(size, *refs):
    me_ref, bias_ref, dlog_ref, skip_ref = refs[:4]
    chunks = refs[4 : 4 + size]
    (gain, wstep, conv_v, conv_m, hgain, wmaps, pastv_s, pastm_s, wvalue, wgate, state, wout) = refs[
        4 + size : 16 + size
    ]
    (part_o, x_o, state_o, dec_o, in_o, u_o, vtail, mtail) = refs[16 + size : 24 + size]
    (normed_s, wvalue_s, wgate_s, wout_s, newv_s, newm_s, out_s, value_s, gate_s, heads_s, sems, ssems) = refs[
        24 + size :
    ]
    rows, width = chunks[0].shape
    me = me_ref[0]
    heads = state.shape[1]
    pairs = heads // 2

    def state_copy(pair):
        both = pl.ds(2 * pair, 2)
        return pltpu.make_async_copy(state.at[:, both], state_o.at[:, both], ssems.at[pair])

    load_value = row_copies(wvalue, wvalue_s, sems, 0, 2)
    load_gate = row_copies(wgate, wgate_s, sems, 2, 2)
    load_out = row_copies(wout, wout_s, sems, 4, 2)
    later = pairs - 2
    tails = [
        pltpu.make_async_copy(pastm_s.at[pl.ds(1, 2)], mtail.at[pl.ds(0, 2)], sems.at[6]),
        pltpu.make_async_copy(pastv_s.at[pl.ds(1, 2)], vtail.at[pl.ds(0, 2)], sems.at[7]),
        pltpu.make_async_copy(newm_s, mtail.at[2], sems.at[8]),
        pltpu.make_async_copy(newv_s, vtail.at[2], sems.at[9]),
    ]

    for copy in load_value + load_gate:
        copy.start()

    for step in range(size):
        source = lax.rem(me + size - step, size)
        x_o[:, pl.ds(pl.multiple_of(source * width, width), width)] = chunks[step][...]
    x = x_o[...].astype(jnp.float32)
    inv = lax.rsqrt(jnp.mean(x * x, axis=-1, keepdims=True) + NORM_EPS)
    normed = (x * inv * gain[...]).astype(jnp.bfloat16)
    normed_s[...] = normed

    step_pre = lax.dot_general(
        normed, wstep[...], (((1,), (1,)), ((), ())), preferred_element_type=jnp.float32
    )

    def conv(past, new, taps, block):
        total = new.astype(jnp.float32) * taps[3:4, block]
        for t in range(3):
            total = total + past[t, :, block].astype(jnp.float32) * taps[t : t + 1, block]
        return silu(total)

    for copy in tails[:2]:
        copy.start()
    def span(index, extent):
        return pl.ds(pl.multiple_of(index * extent, extent), extent)

    def product(weights, block):
        return jnp.dot(normed_s[...], weights[:, block], preferred_element_type=jnp.float32)

    def maps_product(tile):
        block = span(tile, TILE)
        newm_s[:, block] = product(wmaps, block).astype(jnp.bfloat16)

    def maps_conv(tile):
        block = span(tile, TILE)
        act = conv(pastm_s, newm_s[:, block], conv_m, block).astype(jnp.bfloat16).astype(jnp.float32)
        groups = TILE // (2 * STATE)
        for group in range(groups):
            base = group * 2 * STATE
            target = span(tile * groups + group, STATE)
            in_o[:, target] = act[:, base : base + STATE]
            out_s[:, target] = act[:, base + STATE : base + 2 * STATE]

    def maps_body(tile, carry):
        for part in range(2):

            @pl.when(2 * tile + part < later)
            def _():
                state_copy(2 * tile + part).start()

        maps_product(tile + 1)
        maps_conv(tile)
        return carry

    last = wmaps.shape[1] // TILE - 1
    maps_product(0)
    lax.fori_loop(0, last, maps_body, 0)
    for pair in range(2 * last, later):
        state_copy(pair).start()
    for copy in load_value + load_gate:
        copy.wait()
    maps_conv(last)
    for tile in range(wvalue_s.shape[1] // TILE):
        block = pl.ds(tile * TILE, TILE)
        new = product(wvalue_s, block).astype(jnp.bfloat16)
        newv_s[:, block] = new
        value_s[:, block] = conv(pastv_s, new, conv_v, block)
        gate_s[:, block] = silu(product(wgate_s, block))
    for copy in tails[2:]:
        copy.start()

    row_of = lax.broadcasted_iota(jnp.int32, (rows, STATE), 0)
    part_of = lax.broadcasted_iota(jnp.int32, (rows, GROUP * HEAD_DIM), 1) // HEAD_DIM
    low = lax.broadcasted_iota(jnp.int32, (rows, LANES), 1) < HEAD_DIM
    step_lane = lax.broadcasted_iota(jnp.int32, step_pre.shape, 1)

    def carried_sums(group, outs):
        total = None
        for row in range(0, rows, 2):
            wanted = [
                jnp.concatenate([jnp.where(row_of == row + t, out, 0.0) for t in range(2)], axis=1)
                for out in outs
            ]
            held = [
                state_o[row + t, pl.ds(group * GROUP, GROUP)].reshape(GROUP * HEAD_DIM, STATE)
                for t in range(2)
            ]
            term = lax.dot_general(
                jnp.concatenate(wanted, axis=0).astype(jnp.bfloat16),
                jnp.concatenate(held, axis=1).astype(jnp.bfloat16),
                (((1,), (1,)), ((), ())),
                preferred_element_type=jnp.float32,
            )
            total = term if total is None else total + term
        picked = None
        for which in range(GROUP):
            piece = jnp.where(part_of == which, total[which * rows : (which + 1) * rows], 0.0)
            picked = piece if picked is None else picked + piece
        return picked

    def group_body(group, carry):
        for which in range(GROUP // 2):
            pair = group * (GROUP // 2) + which
            state_copy(pair).wait()

            @pl.when(pair + later < pairs)
            def _():
                state_copy(pair + later).start()

            for part in range(2):

                @pl.when(pair == pairs - later + part)
                def _():
                    load_out[part].start()

        outs, decays, sizes, meets = [], [], [], []
        for which in range(GROUP):
            head = group * GROUP + which
            wide = span(head, STATE)
            column = jnp.sum(
                jnp.where(step_lane == me * heads + head, step_pre, 0.0), axis=1, keepdims=True
            )
            pre = jnp.broadcast_to(column, (rows, LANES)) + bias_ref[head]
            size_h = jnp.maximum(pre, 0.0) + jnp.log1p(jnp.exp(-jnp.abs(pre)))
            rate = jnp.exp(jnp.full((rows, LANES), dlog_ref[head]))
            decay = jnp.exp(-size_h * rate)
            dec_o[:, wide] = decay
            outs.append(out_s[:, wide])
            meets.append(jnp.sum(in_o[:, wide] * outs[-1], axis=1, keepdims=True))
            decays.append(decay)
            sizes.append(size_h)
        carried = carried_sums(group, outs)
        for which in range(GROUP // 2):
            one, two = 2 * which, 2 * which + 1
            block = span(group * (GROUP // 2) + which, LANES)
            value = value_s[:, block]
            written = jnp.where(low, sizes[one], sizes[two]) * value
            u_o[:, block] = written
            read = jnp.where(low, decays[one], decays[two]) * carried[:, which * LANES : (which + 1) * LANES]
            read = read + jnp.where(low, meets[one], meets[two]) * written
            skip = jnp.where(low, skip_ref[group * GROUP + one], skip_ref[group * GROUP + two])
            gated = (read + skip * value) * gate_s[:, block]
            square = gated * gated
            first = jnp.sum(jnp.where(low, square, 0.0), axis=1, keepdims=True)
            second = jnp.sum(jnp.where(low, 0.0, square), axis=1, keepdims=True)
            scale = lax.rsqrt(jnp.where(low, first, second) * (1.0 / HEAD_DIM) + NORM_EPS)
            heads_s[:, block] = (gated * scale * hgain[:, block]).astype(jnp.bfloat16)
        return carry

    lax.fori_loop(0, heads // GROUP, group_body, 0)

    for copy in load_out:
        copy.wait()

    def out_body(tile, carry):
        block = span(tile, TILE)
        part_o[:, block] = jnp.dot(heads_s[...], wout_s[:, block], preferred_element_type=jnp.float32).astype(
            jnp.bfloat16
        )
        return carry

    lax.fori_loop(0, wout_s.shape[1] // TILE, out_body, 0)
    for copy in tails:
        copy.wait()


def write_kernel(parts, state_ref, dec_ref, in_ref, u_ref, wup, next_ref, wup_o, buffers, sems, wsems):
    rows, heads = state_ref.shape[:2]
    slots = buffers.shape[0]
    loads = row_copies(wup, wup_o, wsems, 0, parts)
    for copy in loads:
        copy.start()

    def store(pair):
        slot = lax.rem(pair, slots)
        return pltpu.make_async_copy(buffers.at[slot], next_ref.at[:, pl.ds(2 * pair, 2)], sems.at[slot])

    def pair_body(pair, carry):
        @pl.when(pair >= slots)
        def _():
            store(pair - slots).wait()

        slot = lax.rem(pair, slots)
        turned = jnp.transpose(u_ref[:, pl.ds(pl.multiple_of(pair * LANES, LANES), LANES)])
        for which in range(2):
            head = 2 * pair + which
            wide = pl.ds(pl.multiple_of(head * STATE, STATE), STATE)
            column = turned[which * HEAD_DIM : (which + 1) * HEAD_DIM]
            decay, in_map = dec_ref[:, wide], in_ref[:, wide]
            for row in range(rows):
                buffers[slot, row, which] = (
                    state_ref[row, head] * decay[row : row + 1]
                    + column[:, row : row + 1] * in_map[row : row + 1]
                )
        store(pair).start()
        return carry

    pairs = heads // 2
    lax.fori_loop(0, pairs, pair_body, 0)
    for pair in range(max(pairs - slots, 0), pairs):
        store(pair).wait()
    for copy in loads:
        copy.wait()


def mlp_kernel(size, *refs):
    me_ref, x_ref = refs[:2]
    parts = refs[2 : 2 + size]
    gain, wup, wdown = refs[2 + size : 5 + size]
    base_o = refs[5 + size]
    pieces = refs[6 + size : 5 + 2 * size]
    hidden_s, total_s, normed_s, squared_s, wdown_s, sems = refs[5 + 2 * size :]
    loads = row_copies(wdown, wdown_s, sems, 0, sems.shape[0])
    for copy in loads:
        copy.start()
    width = base_o.shape[1]
    me = me_ref[0]
    total = x_ref[...].astype(jnp.float32)
    for part in parts:
        total = total + part[...].astype(jnp.float32)
    hidden = total.astype(jnp.bfloat16)
    hidden_s[...] = hidden.astype(jnp.float32)
    wide = hidden_s[...]
    inv = lax.rsqrt(jnp.mean(wide * wide, axis=-1, keepdims=True) + NORM_EPS)
    normed = (wide * inv * gain[...]).astype(jnp.bfloat16)
    normed_s[...] = normed

    def up_body(tile, carry):
        block = pl.ds(pl.multiple_of(tile * TILE, TILE), TILE)
        up = jnp.maximum(jnp.dot(normed_s[...], wup[:, block], preferred_element_type=jnp.float32), 0.0)
        squared_s[:, block] = (up * up).astype(jnp.bfloat16)
        return carry

    lax.fori_loop(0, wup.shape[1] // TILE, up_body, 0)
    out = None
    depth = wdown.shape[0] // len(loads)
    for part, copy in enumerate(loads):
        copy.wait()
        block = pl.ds(part * depth, depth)
        down = jnp.dot(squared_s[:, block], wdown_s[block, :], preferred_element_type=jnp.float32)
        out = down if out is None else out + down
    total_s[...] = out
    own = pl.ds(pl.multiple_of(me * width, width), width)
    base_o[...] = hidden_s[:, own] + total_s[:, own]
    for step in range(1, size):
        target = lax.rem(me + step, size)
        block = pl.ds(pl.multiple_of(target * width, width), width)
        pieces[step - 1][...] = total_s[:, block].astype(jnp.bfloat16)


def local_few(
    size,
    tokens,
    mix_gain,
    w_gate,
    w_value,
    w_maps,
    w_step,
    conv_value,
    conv_maps,
    past_value,
    past_maps,
    step_bias,
    decay_log,
    skip_gain,
    head_gain,
    state,
    w_out,
    mlp_gain,
    w_up,
    w_down,
):
    f32, bf16 = jnp.float32, jnp.bfloat16
    rows, width = tokens.shape
    model = width * size
    heads = state.shape[1]
    inner, maps = w_value.shape[1], w_maps.shape[1]
    me = lax.axis_index("kv").astype(jnp.int32).reshape(1)

    chunks = [tokens] + [shifted(tokens, size, step) for step in range(1, size)]
    past_value, past_maps = past_value.transpose(1, 0, 2), past_maps.transpose(1, 0, 2)
    maps_near, value_near, past_near = fetch([w_maps, past_value, past_maps], (8, 1, 1), "fetch_maps")
    part, whole, held, decay, in_map, written, value_tail, maps_tail = pl.pallas_call(
        functools.partial(mixer_kernel, size),
        out_shape=[
            pltpu.VMEM((rows, model), bf16),
            pltpu.VMEM((rows, model), bf16),
            pltpu.VMEM(state.shape, f32),
            pltpu.VMEM((rows, heads * STATE), f32),
            pltpu.VMEM((rows, heads * STATE), f32),
            pltpu.VMEM((rows, inner), f32),
            jax.ShapeDtypeStruct((3, rows, inner), bf16),
            jax.ShapeDtypeStruct((3, rows, maps), bf16),
        ],
        in_specs=[SMEM] * 4 + [VMEM] * (size + 8) + [HBM] * 4,
        out_specs=[VMEM] * 6 + [HBM] * 2,
        scratch_shapes=[
            pltpu.VMEM((rows, model), bf16),
            pltpu.VMEM(w_value.shape, bf16),
            pltpu.VMEM(w_gate.shape, bf16),
            pltpu.VMEM(w_out.shape, bf16),
            pltpu.VMEM((rows, inner), bf16),
            pltpu.VMEM((rows, maps), bf16),
            pltpu.VMEM((rows, heads * STATE), f32),
            pltpu.VMEM((rows, inner), f32),
            pltpu.VMEM((rows, inner), f32),
            pltpu.VMEM((rows, inner), bf16),
            pltpu.SemaphoreType.DMA((10,)),
            pltpu.SemaphoreType.DMA((heads // 2,)),
        ],
        compiler_params=pltpu.CompilerParams(vmem_limit_bytes=20 << 20),
        cost_estimate=cost(2 * rows * model * (2 * inner + maps), 40e6),
        name="mixer",
    )(
        me,
        step_bias,
        decay_log,
        skip_gain,
        *chunks,
        mix_gain.reshape(1, -1),
        w_step.T,
        conv_value,
        conv_maps,
        head_gain.reshape(1, -1),
        maps_near,
        value_near,
        past_near,
        *[in_hbm(a) for a in (w_value, w_gate, state, w_out)],
    )

    parts = [part] + [shifted(part, size, step) for step in range(1, size)]
    state_next, up_near = pl.pallas_call(
        functools.partial(write_kernel, 4),
        out_shape=[jax.ShapeDtypeStruct(state.shape, f32), pltpu.VMEM(w_up.shape, bf16)],
        in_specs=[VMEM] * 4 + [HBM],
        out_specs=[HBM, VMEM],
        scratch_shapes=[
            pltpu.VMEM((SLOTS, rows, 2, HEAD_DIM, STATE), f32),
            pltpu.SemaphoreType.DMA((SLOTS,)),
            pltpu.SemaphoreType.DMA((4,)),
        ],
        compiler_params=pltpu.CompilerParams(vmem_limit_bytes=8 << 20),
        cost_estimate=cost(1e6, 33e6),
        name="write_state",
    )(held, decay, in_map, written, in_hbm(w_up))
    base, *pieces = pl.pallas_call(
        functools.partial(mlp_kernel, size),
        out_shape=[pltpu.VMEM((rows, width), f32)] + [pltpu.VMEM((rows, width), bf16)] * (size - 1),
        in_specs=[SMEM] + [VMEM] * (size + 3) + [HBM],
        out_specs=[VMEM] * size,
        scratch_shapes=[
            pltpu.VMEM((rows, model), f32),
            pltpu.VMEM((rows, model), f32),
            pltpu.VMEM((rows, model), bf16),
            pltpu.VMEM((rows, w_up.shape[1]), bf16),
            pltpu.VMEM(w_down.shape, bf16),
            pltpu.SemaphoreType.DMA((4,)),
        ],
        compiler_params=pltpu.CompilerParams(vmem_limit_bytes=12 << 20),
        cost_estimate=cost(4 * rows * model * w_up.shape[1], 17e6),
        name="mlp",
    )(me, whole, *parts, mlp_gain.reshape(1, -1), up_near, in_hbm(w_down))

    arrived = [shifted(pieces[step - 1], size, step) for step in range(1, size)]
    total = base
    for piece in arrived:
        total = total + piece.astype(f32)
    return (
        total.astype(bf16),
        state_next,
        value_tail.transpose(1, 0, 2),
        maps_tail.transpose(1, 0, 2),
    )


def local(size, *arrays):
    tokens, w_value, w_maps, state, w_up = (arrays[i] for i in (0, 3, 4, 14, 17))
    heads = state.shape[1]
    fits = (
        size <= 8
        and heads % GROUP == 0
        and state.shape[2:] == (HEAD_DIM, STATE)
        and w_maps.shape[1] == heads * 2 * STATE
        and all(extent % TILE == 0 for extent in (w_value.shape[1], w_maps.shape[1], w_up.shape[1]))
        and tokens.shape[1] % LANES == 0
        and tokens.shape[0] % 8 == 0
    )
    return local_few(size, *arrays) if fits else local_many(*arrays)


def solution(mesh):
    in_specs = (
        P(("dp", "tp"), "kv"),
        P(),
        P(None, "kv"),
        P(None, "kv"),
        P(None, "kv"),
        P(),
        P(None, "kv"),
        P(None, "kv"),
        P(("dp", "tp"), None, "kv"),
        P(("dp", "tp"), None, "kv"),
        P("kv"),
        P("kv"),
        P("kv"),
        P("kv"),
        P(("dp", "tp"), "kv", None, None),
        P("kv", None),
        P(),
        P(None, "kv"),
        P("kv", None),
    )
    out_specs = (
        P(("dp", "tp"), "kv"),
        P(("dp", "tp"), "kv", None, None),
        P(("dp", "tp"), None, "kv"),
        P(("dp", "tp"), None, "kv"),
    )
    step = functools.partial(local, mesh.shape["kv"])
    return jax.shard_map(step, mesh=mesh, in_specs=in_specs, out_specs=out_specs, check_vma=False)
```

time: 55.4 us -> 47.6 us (0.86)
  Pallas kernels: 37.4 us -> 28.4 us
  starting transfers between devices: 14.4 us -> 15.9 us
    pallas_call x2 -> x1, Pallas kernels: 11.8 us -> 6.09 us  [fetch(): pl.pallas_call(functools.partial(fetch_kernel, parts), out_shape=[pltpu.V...]
    pallas_call x1, Pallas kernels: 14.8 us -> 10.4 us  [local_few(): pl.pallas_call(functools.partial(mixer_kernel, size), out_shape=[pltpu.VM...]
    ppermute x9, starting transfers between devices: 14.4 us -> 15.9 us  [shifted(): lax.ppermute(block, 'kv', [(i, (i + step) % size) for i in range(size)])]
    pallas_call x1, Pallas kernels: 3.36 us -> 4.07 us  [local_few(): pl.pallas_call(functools.partial(mlp_kernel, size), out_shape=[pltpu.VMEM...]
  transfers between devices with their start and end apart: 9 -> 9, of which waited for: 1 -> 2; matrix products, arithmetic and copies ran while one was open for 0% -> 0% of each run, Pallas kernels for 35% -> 29%
where the time goes in v3:
time: 47.6 us; the launch traced here: 47.4 us
  Pallas kernels  28.4 us (60%)
  starting transfers between devices  15.9 us (33%)
  waiting for transfers between devices  1.54 us (3%)
  between operations  0.84 us (2%)
  other arithmetic  0.62 us (1%)
    ppermute x9, starting transfers between devices, shifted(): lax.ppermute(block, 'kv', [(i, (i + step) % size) for i in range(size)])  15.9 us
    pallas_call x1, Pallas kernels, local_few(): pl.pallas_call(functools.partial(mixer_kernel, size), out_shape=[pltpu.VM...  10.4 us
    pallas_call x1, Pallas kernels, local_few(): pl.pallas_call(functools.partial(write_kernel, 4), out_shape=[jax.ShapeDt...  7.85 us
    pallas_call x1, Pallas kernels, fetch(): pl.pallas_call(functools.partial(fetch_kernel, parts), out_shape=[pltpu.V...  6.09 us
    pallas_call x1, Pallas kernels, local_few(): pl.pallas_call(functools.partial(mlp_kernel, size), out_shape=[pltpu.VMEM...  4.07 us
    ppermute x9, waiting for transfers between devices, shifted(): lax.ppermute(block, 'kv', [(i, (i + step) % size) for i in range(size)])  1.54 us
  transfers between devices with their start and end apart: 9, of which 2 were waited for; matrix products, arithmetic and copies ran while one was open for 0% of the time, Pallas kernels for 29%

profile of v3, /device:TPU:0, one launch (start us, length us, event | category | flops | bytes accessed | tf_op | source)
XLA Modules:
  0.0 47.4 jit_solution(13431245406037374676)
XLA Ops:
  0.6 3.1 %collective-permute-start = (bf16[24,512]{1,0:T(8,128)(2,1)}, bf16[24,512]{1,0:T(8,128)(2,1)S(1)}, u32[]{:S(2)}, u32[]{:S(2)}) collective-permute-start(bf16[24,512]{1,0:T(8,128)(2,1)} %refs_4_.1), channel_id=1, source_target_pairs={{0,2},{2,4},{4,6},{6,0},{1,3},{3,5},{5,7},{7,1},{8,10},{10,12},{12... | collective-permute-start | bytes 73736 | tf_op jit(solution)/shard_map/ppermute | solution.py:104
  3.7 2.6 %collective-permute-start.1 = (bf16[24,512]{1,0:T(8,128)(2,1)}, bf16[24,512]{1,0:T(8,128)(2,1)S(1)}, u32[]{:S(2)}, u32[]{:S(2)}) collective-permute-start(bf16[24,512]{1,0:T(8,128)(2,1)} %refs_4_.1), channel_id=1, source_target_pairs={{0,4},{2,6},{4,0},{6,2},{1,5},{3,7},{5,1},{7,3},{8,12},{10,14},{12... | collective-permute-start | bytes 73736 | tf_op jit(solution)/shard_map/ppermute | solution.py:104
  6.3 1.3 %collective-permute-start.2 = (bf16[24,512]{1,0:T(8,128)(2,1)}, bf16[24,512]{1,0:T(8,128)(2,1)S(1)}, u32[]{:S(2)}, u32[]{:S(2)}) collective-permute-start(bf16[24,512]{1,0:T(8,128)(2,1)} %refs_4_.1), channel_id=1, source_target_pairs={{0,6},{2,0},{4,2},{6,4},{1,7},{3,1},{5,3},{7,5},{8,14},{10,8},{12,... | collective-permute-start | bytes 73736 | tf_op jit(solution)/shard_map/ppermute | solution.py:104
  7.7 0.0 copy-start.4
  7.7 6.1 %fetch_maps.1 = (bf16[2048,4096]{1,0:T(8,128)(2,1)S(1)}, bf16[3,24,1024]{2,1,0:T(8,128)(2,1)S(1)}, bf16[3,24,4096]{2,1,0:T(8,128)(2,1)S(1)}) custom-call(bf16[2048,4096]{1,0:T(8,128)(2,1)} %refs_0_.1, bf16[3,24,1024]{2,1,0:T(8,128)(2,1)} %bitcast.14, bf16[3,24,4096]{2,1,0:T(8,128)(2,1)} %bitcast.13), custom_call_target="tpu_custom_call" | custom-call | flops 1000000 | bytes 35028992 | tf_op jit(solution)/shard_map/fetch_maps/pallas_call | solution.py:142
  13.8 0.0 collective-permute-done.refs_5_
  13.8 0.0 collective-permute-done.1.refs_6_
  13.9 0.0 collective-permute-done.2.refs_7_
  14.0 10.4 %mixer.1 = (bf16[24,2048]{1,0:T(8,128)(2,1)S(1)}, bf16[24,2048]{1,0:T(8,128)(2,1)S(1)}, f32[24,16,64,128]{3,2,1,0:T(8,128)S(1)}, f32[24,2048]{1,0:T(8,128)S(1)},...) custom-call(s32[1]{0:T(128)} %bitcast.refs_0_, ...), custom_call_target="tpu_custom_call" | custom-call | flops 603979776 | bytes 40000000 | tf_op jit(solution)/shard_map/mixer/pallas_call | solution.py:466
  24.4 0.7 %collective-permute-start.3 = (bf16[24,2048]{1,0:T(8,128)(2,1)S(1)}, bf16[24,2048]{1,0:T(8,128)(2,1)S(1)}, u32[]{:S(2)}, u32[]{:S(2)}) collective-permute-start(bf16[24,2048]{1,0:T(8,128)(2,1)S(1)} %get-tuple-element.25.refs_2_), channel_id=1, source_target_pairs={{0,2},{2,4},{4,6},{6,0},{1,3},{3,5},{5,7},{7,1},{8,10},{10,12},{12... | collective-permute-start | bytes 294920 | tf_op jit(solution)/shard_map/ppermute | solution.py:104
  25.1 0.3 collective-permute-start.4
  25.5 2.8 %collective-permute-start.5 = (bf16[24,2048]{1,0:T(8,128)(2,1)S(1)}, bf16[24,2048]{1,0:T(8,128)(2,1)S(1)}, u32[]{:S(2)}, u32[]{:S(2)}) collective-permute-start(bf16[24,2048]{1,0:T(8,128)(2,1)S(1)} %get-tuple-element.25.refs_2_), channel_id=1, source_target_pairs={{0,6},{2,0},{4,2},{6,4},{1,7},{3,1},{5,3},{7,5},{8,14},{10,8},{12,... | collective-permute-start | bytes 294920 | tf_op jit(solution)/shard_map/ppermute | solution.py:104
  28.3 7.9 %write_state.1 = (f32[24,16,64,128]{3,2,1,0:T(8,128)}, bf16[2048,2048]{1,0:T(8,128)(2,1)S(1)}) custom-call(f32[24,16,64,128]{3,2,1,0:T(8,128)S(1)} %get-tuple-element.26.state_ref, f32[24,2048]{1,0:T(8,128)S(1)} %get-tuple-element.27.dec_ref, f32[24,2048]{1,0:T(8,128)S(1)} %get-tuple-element.28.in_ref, f32[24,1024]{1,0:T(8,128)S(1)} %get-tuple-element.29.u_ref, ...), custom_call_target="tpu_custom_call" | custom-call | flops 1000000 | bytes 33000000 | tf_op jit(solution)/shard_map/write_state/pallas_call | solution.py:515
  36.1 0.0 collective-permute-done.3.refs_3_
  36.2 0.0 collective-permute-done.4.refs_4_
  36.2 0.0 collective-permute-done.5.refs_5_
  36.2 4.1 %mlp.1 = (f32[24,512]{1,0:T(8,128)S(1)}, bf16[24,512]{1,0:T(8,128)(2,1)S(1)}, bf16[24,512]{1,0:T(8,128)(2,1)S(1)}, bf16[24,512]{1,0:T(8,128)(2,1)S(1)}) custom-call(s32[1]{0:T(128)} %bitcast.refs_0_, bf16[24,2048]{1,0:T(8,128)(2,1)S(1)} %get-tuple-element.24.refs_1_, bf16[24,2048]{1,0:T(8,128)(2,1)S(1)} %get-tuple-element.25.refs_2_, ...), custom_call_target="tpu_custom_call" | custom-call | flops 402653184 | bytes 17000000 | tf_op jit(solution)/shard_map/mlp/pallas_call | solution.py:529
  40.3 0.6 %collective-permute-start.6 = (bf16[24,512]{1,0:T(8,128)(2,1)S(1)}, bf16[24,512]{1,0:T(8,128)(2,1)S(1)}, u32[]{:S(2)}, u32[]{:S(2)}) collective-permute-start(bf16[24,512]{1,0:T(8,128)(2,1)S(1)} %get-tuple-element.32), channel_id=1, source_target_pairs={{0,2},{2,4},{4,6},{6,0},{1,3},{3,5},{5,7},{7,1},{8,10},{10,12},{12... | collective-permute-start | bytes 73736 | tf_op jit(solution)/shard_map/ppermute | solution.py:104
  40.9 1.5 %collective-permute-start.7 = (bf16[24,512]{1,0:T(8,128)(2,1)S(1)}, bf16[24,512]{1,0:T(8,128)(2,1)S(1)}, u32[]{:S(2)}, u32[]{:S(2)}) collective-permute-start(bf16[24,512]{1,0:T(8,128)(2,1)S(1)} %get-tuple-element.33), channel_id=1, source_target_pairs={{0,4},{2,6},{4,0},{6,2},{1,5},{3,7},{5,1},{7,3},{8,12},{10,14},{12... | collective-permute-start | bytes 73736 | tf_op jit(solution)/shard_map/ppermute | solution.py:104
  42.4 2.8 %collective-permute-start.8 = (bf16[24,512]{1,0:T(8,128)(2,1)S(1)}, bf16[24,512]{1,0:T(8,128)(2,1)S(1)}, u32[]{:S(2)}, u32[]{:S(2)}) collective-permute-start(bf16[24,512]{1,0:T(8,128)(2,1)S(1)} %get-tuple-element.34), channel_id=1, source_target_pairs={{0,6},{2,0},{4,2},{6,4},{1,7},{3,1},{5,3},{7,5},{8,14},{10,8},{12,... | collective-permute-start | bytes 73736 | tf_op jit(solution)/shard_map/ppermute | solution.py:104
  45.3 0.7 %collective-permute-done.6 = bf16[24,512]{1,0:T(8,128)(2,1)S(1)} collective-permute-done((bf16[24,512]{1,0:T(8,128)(2,1)S(1)}, bf16[24,512]{1,0:T(8,128)(2,1)S(1)}, u32[]{:S(2)}, u32[]{:S(2)}) %collective-permute-start.6) | collective-permute-done | bytes 24608 | tf_op jit(solution)/shard_map/ppermute | solution.py:104
  45.9 0.0 collective-permute-done.7
  45.9 0.8 %collective-permute-done.8 = bf16[24,512]{1,0:T(8,128)(2,1)S(1)} collective-permute-done((bf16[24,512]{1,0:T(8,128)(2,1)S(1)}, bf16[24,512]{1,0:T(8,128)(2,1)S(1)}, u32[]{:S(2)}, u32[]{:S(2)}) %collective-permute-start.8) | collective-permute-done | bytes 24608 | tf_op jit(solution)/shard_map/ppermute | solution.py:104
  46.8 0.6 %add_convert_fusion = bf16[24,512]{1,0:T(8,128)(2,1)} fusion(bf16[24,512]{1,0:T(8,128)(2,1)S(1)} %collective-permute-done.8, bf16[24,512]{1,0:T(8,128)(2,1)S(1)} %collective-permute-done.7, f32[24,512]{1,0:T(8,128)S(1)} %get-tuple-element.31, bf16[24,512]{1,0:T(8,128)(2,1)S(1)} %collective-permute-done.6), kind=kLoop, calls=%fused_computation | loop fusion | flops 86016 | bytes 147456 | tf_op jit(solution)/shard_map/convert_element_type | solution.py:552
  (19 shorter events, 0.0 us)
Async XLA Ops:
  0.6 13.2 %collective-permute-start = (bf16[24,512]{1,0:T(8,128)(2,1)}, bf16[24,512]{1,0:T(8,128)(2,1)S(1)}, u32[]{:S(2)}, u32[]{:S(2)}) collective-permute-start(bf16[24,512]{1,0:T(8,128)(2,1)} %refs_4_.1), channel_id=1, source_target_pairs={{0,2},{2,4},{4,6},{6,0},{1,3},{3,5},{5,7},{7,1},{8,10},{10,12},{12... | collective-permute-start | bytes 73736 | tf_op jit(solution)/shard_map/ppermute | solution.py:104
  3.7 10.1 %collective-permute-start.1 = (bf16[24,512]{1,0:T(8,128)(2,1)}, bf16[24,512]{1,0:T(8,128)(2,1)S(1)}, u32[]{:S(2)}, u32[]{:S(2)}) collective-permute-start(bf16[24,512]{1,0:T(8,128)(2,1)} %refs_4_.1), channel_id=1, source_target_pairs={{0,4},{2,6},{4,0},{6,2},{1,5},{3,7},{5,1},{7,3},{8,12},{10,14},{12... | collective-permute-start | bytes 73736 | tf_op jit(solution)/shard_map/ppermute | solution.py:104
  6.3 7.5 %collective-permute-start.2 = (bf16[24,512]{1,0:T(8,128)(2,1)}, bf16[24,512]{1,0:T(8,128)(2,1)S(1)}, u32[]{:S(2)}, u32[]{:S(2)}) collective-permute-start(bf16[24,512]{1,0:T(8,128)(2,1)} %refs_4_.1), channel_id=1, source_target_pairs={{0,6},{2,0},{4,2},{6,4},{1,7},{3,1},{5,3},{7,5},{8,14},{10,8},{12,... | collective-permute-start | bytes 73736 | tf_op jit(solution)/shard_map/ppermute | solution.py:104
  7.7 6.2 %copy-start = (bf16[2048,64]{0,1:T(8,128)(2,1)S(1)}, bf16[2048,64]{0,1:T(8,128)(2,1)}, u32[]{:S(2)}) copy-start(bf16[2048,64]{0,1:T(8,128)(2,1)} %param.24) | copy-start | bytes 786436
  7.7 6.2 %copy-start.1 = (f32[4,4096]{1,0:T(4,128)S(1)}, f32[4,4096]{1,0:T(4,128)}, u32[]{:S(2)}) copy-start(f32[4,4096]{1,0:T(4,128)} %refs_11_.1) | copy-start | bytes 196612
  7.7 6.2 %copy-start.2 = (bf16[24,512]{1,0:T(8,128)(2,1)S(1)}, bf16[24,512]{1,0:T(8,128)(2,1)}, u32[]{:S(2)}) copy-start(bf16[24,512]{1,0:T(8,128)(2,1)} %refs_4_.1) | copy-start | bytes 73732
  7.7 6.2 %copy-start.3 = (f32[4,1024]{1,0:T(4,128)S(1)}, f32[4,1024]{1,0:T(4,128)}, u32[]{:S(2)}) copy-start(f32[4,1024]{1,0:T(4,128)} %refs_10_.1) | copy-start | bytes 49156
  7.7 6.2 %copy-start.4 = (f32[2048]{0:T(1024)S(1)}, f32[2048]{0:T(1024)}, u32[]{:S(2)}) copy-start(f32[2048]{0:T(1024)} %param.20) | copy-start | bytes 24580
  7.7 6.2 %copy-start.6 = (f32[1024]{0:T(1024)S(1)}, f32[1024]{0:T(1024)}, u32[]{:S(2)}) copy-start(f32[1024]{0:T(1024)} %param.32) | copy-start | bytes 12292
  7.7 6.2 %copy-start.7 = (f32[16]{0:T(128)S(1)}, f32[16]{0:T(128)}, u32[]{:S(2)}) copy-start(f32[16]{0:T(128)} %refs_1_.1) | copy-start | bytes 196
  7.7 6.2 %copy-start.8 = (f32[16]{0:T(128)S(1)}, f32[16]{0:T(128)}, u32[]{:S(2)}) copy-start(f32[16]{0:T(128)} %refs_2_.1) | copy-start | bytes 196
  7.7 6.2 %copy-start.9 = (f32[16]{0:T(128)S(1)}, f32[16]{0:T(128)}, u32[]{:S(2)}) copy-start(f32[16]{0:T(128)} %refs_3_.1) | copy-start | bytes 196
  24.4 11.7 %collective-permute-start.3 = (bf16[24,2048]{1,0:T(8,128)(2,1)S(1)}, bf16[24,2048]{1,0:T(8,128)(2,1)S(1)}, u32[]{:S(2)}, u32[]{:S(2)}) collective-permute-start(bf16[24,2048]{1,0:T(8,128)(2,1)S(1)} %get-tuple-element.25.refs_2_), channel_id=1, source_target_pairs={{0,2},{2,4},{4,6},{6,0},{1,3},{3,5},{5,7},{7,1},{8,10},{10,12},{12... | collective-permute-start | bytes 294920 | tf_op jit(solution)/shard_map/ppermute | solution.py:104
  25.1 11.0 %collective-permute-start.4 = (bf16[24,2048]{1,0:T(8,128)(2,1)S(1)}, bf16[24,2048]{1,0:T(8,128)(2,1)S(1)}, u32[]{:S(2)}, u32[]{:S(2)}) collective-permute-start(bf16[24,2048]{1,0:T(8,128)(2,1)S(1)} %get-tuple-element.25.refs_2_), channel_id=1, source_target_pairs={{0,4},{2,6},{4,0},{6,2},{1,5},{3,7},{5,1},{7,3},{8,12},{10,14},{12... | collective-permute-start | bytes 294920 | tf_op jit(solution)/shard_map/ppermute | solution.py:104
  25.5 10.7 %collective-permute-start.5 = (bf16[24,2048]{1,0:T(8,128)(2,1)S(1)}, bf16[24,2048]{1,0:T(8,128)(2,1)S(1)}, u32[]{:S(2)}, u32[]{:S(2)}) collective-permute-start(bf16[24,2048]{1,0:T(8,128)(2,1)S(1)} %get-tuple-element.25.refs_2_), channel_id=1, source_target_pairs={{0,6},{2,0},{4,2},{6,4},{1,7},{3,1},{5,3},{7,5},{8,14},{10,8},{12,... | collective-permute-start | bytes 294920 | tf_op jit(solution)/shard_map/ppermute | solution.py:104
  28.3 7.9 %copy-start.5 = (f32[2048]{0:T(1024)S(1)}, f32[2048]{0:T(1024)}, u32[]{:S(2)}) copy-start(f32[2048]{0:T(1024)} %param.35) | copy-start | bytes 24580
  40.3 5.7 %collective-permute-start.6 = (bf16[24,512]{1,0:T(8,128)(2,1)S(1)}, bf16[24,512]{1,0:T(8,128)(2,1)S(1)}, u32[]{:S(2)}, u32[]{:S(2)}) collective-permute-start(bf16[24,512]{1,0:T(8,128)(2,1)S(1)} %get-tuple-element.32), channel_id=1, source_target_pairs={{0,2},{2,4},{4,6},{6,0},{1,3},{3,5},{5,7},{7,1},{8,10},{10,12},{12... | collective-permute-start | bytes 73736 | tf_op jit(solution)/shard_map/ppermute | solution.py:104
  40.9 5.1 %collective-permute-start.7 = (bf16[24,512]{1,0:T(8,128)(2,1)S(1)}, bf16[24,512]{1,0:T(8,128)(2,1)S(1)}, u32[]{:S(2)}, u32[]{:S(2)}) collective-permute-start(bf16[24,512]{1,0:T(8,128)(2,1)S(1)} %get-tuple-element.33), channel_id=1, source_target_pairs={{0,4},{2,6},{4,0},{6,2},{1,5},{3,7},{5,1},{7,3},{8,12},{10,14},{12... | collective-permute-start | bytes 73736 | tf_op jit(solution)/shard_map/ppermute | solution.py:104
  42.4 4.4 %collective-permute-start.8 = (bf16[24,512]{1,0:T(8,128)(2,1)S(1)}, bf16[24,512]{1,0:T(8,128)(2,1)S(1)}, u32[]{:S(2)}, u32[]{:S(2)}) collective-permute-start(bf16[24,512]{1,0:T(8,128)(2,1)S(1)} %get-tuple-element.34), channel_id=1, source_target_pairs={{0,6},{2,0},{4,2},{6,4},{1,7},{3,1},{5,3},{7,5},{8,14},{10,8},{12,... | collective-permute-start | bytes 73736 | tf_op jit(solution)/shard_map/ppermute | solution.py:104

commit v4 on v3

--- a/solution.py
+++ b/solution.py
@@ -12,13 +12,13 @@
 LANES = 128
 TILE = 1024
 SLOTS = 3
+LATE = 3
 GROUP = 4
 
 
 NORM_EPS = 1e-05
 
 VMEM = pl.BlockSpec(memory_space=pltpu.VMEM)
-SMEM = pl.BlockSpec(memory_space=pltpu.SMEM)
 HBM = pl.BlockSpec(memory_space=pltpu.HBM)
 
 
@@ -100,6 +100,10 @@
     return (layer_out, state_next, value_tail, maps_tail)
 
 
+def swapped(block, size, step):
+    return lax.ppermute(block, "kv", [(i, i ^ step) for i in range(size)])
+
+
 def shifted(block, size, step):
     return lax.ppermute(block, "kv", [(i, (i + step) % size) for i in range(size)])
 
@@ -152,17 +156,18 @@
 
 
 def mixer_kernel(size, *refs):
-    me_ref, bias_ref, dlog_ref, skip_ref = refs[:4]
-    chunks = refs[4 : 4 + size]
+    bias_ref, dlog_ref, skip_ref = refs[:3]
+    refs = refs[3:]
+    chunks = refs[:size]
     (gain, wstep, conv_v, conv_m, hgain, wmaps, pastv_s, pastm_s, wvalue, wgate, state, wout) = refs[
-        4 + size : 16 + size
+        size : 12 + size
     ]
-    (part_o, x_o, state_o, dec_o, in_o, u_o, vtail, mtail) = refs[16 + size : 24 + size]
-    (normed_s, wvalue_s, wgate_s, wout_s, newv_s, newm_s, out_s, value_s, gate_s, heads_s, sems, ssems) = refs[
-        24 + size :
+    (part_o, x_o, state_o, dec_o, in_o, u_o, vtail, mtail) = refs[12 + size : 20 + size]
+    (normed_s, wboth_s, raw_s, wout_s, newv_s, newm_s, out_s, value_s, gate_s, heads_s, sems, ssems) = refs[
+        20 + size :
     ]
     rows, width = chunks[0].shape
-    me = me_ref[0]
+    me = lax.axis_index("kv")
     heads = state.shape[1]
     pairs = heads // 2
 
@@ -170,8 +175,9 @@
         both = pl.ds(2 * pair, 2)
         return pltpu.make_async_copy(state.at[:, both], state_o.at[:, both], ssems.at[pair])
 
-    load_value = row_copies(wvalue, wvalue_s, sems, 0, 2)
-    load_gate = row_copies(wgate, wgate_s, sems, 2, 2)
+    inner = wvalue.shape[1]
+    load_value = row_copies(wvalue, wboth_s.at[:, pl.ds(0, inner)], sems, 0, 2)
+    load_gate = row_copies(wgate, wboth_s.at[:, pl.ds(inner, inner)], sems, 2, 2)
     load_out = row_copies(wout, wout_s, sems, 4, 2)
     later = pairs - 2
     tails = [
@@ -185,7 +191,7 @@
         copy.start()
 
     for step in range(size):
-        source = lax.rem(me + size - step, size)
+        source = lax.bitwise_xor(me, step)
         x_o[:, pl.ds(pl.multiple_of(source * width, width), width)] = chunks[step][...]
     x = x_o[...].astype(jnp.float32)
     inv = lax.rsqrt(jnp.mean(x * x, axis=-1, keepdims=True) + NORM_EPS)
@@ -209,10 +215,6 @@
 
     def product(weights, block):
         return jnp.dot(normed_s[...], weights[:, block], preferred_element_type=jnp.float32)
-
-    def maps_product(tile):
-        block = span(tile, TILE)
-        newm_s[:, block] = product(wmaps, block).astype(jnp.bfloat16)
 
     def maps_conv(tile):
         block = span(tile, TILE)
@@ -225,37 +227,51 @@
             out_s[:, target] = act[:, base + STATE : base + 2 * STATE]
 
     def maps_body(tile, carry):
-        for part in range(2):
-
-            @pl.when(2 * tile + part < later)
-            def _():
-                state_copy(2 * tile + part).start()
-
-        maps_product(tile + 1)
-        maps_conv(tile)
-        return carry
-
-    last = wmaps.shape[1] // TILE - 1
-    maps_product(0)
-    lax.fori_loop(0, last, maps_body, 0)
-    for pair in range(2 * last, later):
+        @pl.when(tile < later)
+        def _():
+            state_copy(tile).start()
+
+        maps_conv(jnp.maximum(tile - 1, 0))
+        block = span(tile, TILE)
+        newm_s[:, block] = product(wmaps, block).astype(jnp.bfloat16)
+        return carry
+
+    tiles = wmaps.shape[1] // TILE
+    newm_s[:, :TILE] = jnp.zeros((rows, TILE), jnp.bfloat16)
+    lax.fori_loop(0, tiles, maps_body, 0)
+    for pair in range(tiles, later):
         state_copy(pair).start()
+    tails[2].start()
     for copy in load_value + load_gate:
         copy.wait()
-    maps_conv(last)
-    for tile in range(wvalue_s.shape[1] // TILE):
-        block = pl.ds(tile * TILE, TILE)
-        new = product(wvalue_s, block).astype(jnp.bfloat16)
+
+    def raw_body(tile, carry):
+        block = span(tile, TILE)
+        raw_s[:, block] = product(wboth_s, block)
+        return carry
+
+    maps_conv(tiles - 1)
+    lax.fori_loop(0, 2 * inner // TILE, raw_body, 0)
+
+    def value_body(tile, carry):
+        block = span(tile, TILE)
+        new = raw_s[:, block].astype(jnp.bfloat16)
         newv_s[:, block] = new
         value_s[:, block] = conv(pastv_s, new, conv_v, block)
-        gate_s[:, block] = silu(product(wgate_s, block))
-    for copy in tails[2:]:
-        copy.start()
+        gate_s[:, block] = silu(raw_s[:, span(tile + inner // TILE, TILE)])
+        return carry
+
+    lax.fori_loop(0, inner // TILE, value_body, 0)
+    tails[3].start()
 
     row_of = lax.broadcasted_iota(jnp.int32, (rows, STATE), 0)
     part_of = lax.broadcasted_iota(jnp.int32, (rows, GROUP * HEAD_DIM), 1) // HEAD_DIM
     low = lax.broadcasted_iota(jnp.int32, (rows, LANES), 1) < HEAD_DIM
     step_lane = lax.broadcasted_iota(jnp.int32, step_pre.shape, 1)
+    head_lane = lax.broadcasted_iota(jnp.int32, (1, heads), 1)
+
+    def of_head(ref, head):
+        return jnp.sum(jnp.where(head_lane == head, ref[...], 0.0), axis=1, keepdims=True)
 
     def carried_sums(group, outs):
         total = None
@@ -303,9 +319,9 @@
             column = jnp.sum(
                 jnp.where(step_lane == me * heads + head, step_pre, 0.0), axis=1, keepdims=True
             )
-            pre = jnp.broadcast_to(column, (rows, LANES)) + bias_ref[head]
+            pre = jnp.broadcast_to(column, (rows, LANES)) + of_head(bias_ref, head)
             size_h = jnp.maximum(pre, 0.0) + jnp.log1p(jnp.exp(-jnp.abs(pre)))
-            rate = jnp.exp(jnp.full((rows, LANES), dlog_ref[head]))
+            rate = jnp.exp(of_head(dlog_ref, head))
             decay = jnp.exp(-size_h * rate)
             dec_o[:, wide] = decay
             outs.append(out_s[:, wide])
@@ -321,7 +337,7 @@
             u_o[:, block] = written
             read = jnp.where(low, decays[one], decays[two]) * carried[:, which * LANES : (which + 1) * LANES]
             read = read + jnp.where(low, meets[one], meets[two]) * written
-            skip = jnp.where(low, skip_ref[group * GROUP + one], skip_ref[group * GROUP + two])
+            skip = jnp.where(low, of_head(skip_ref, group * GROUP + one), of_head(skip_ref, group * GROUP + two))
             gated = (read + skip * value) * gate_s[:, block]
             square = gated * gated
             first = jnp.sum(jnp.where(low, square, 0.0), axis=1, keepdims=True)
@@ -332,72 +348,91 @@
 
     lax.fori_loop(0, heads // GROUP, group_body, 0)
 
-    for copy in load_out:
-        copy.wait()
-
-    def out_body(tile, carry):
+    half = inner // 2
+    load_out[0].wait()
+
+    def first_body(tile, carry):
         block = span(tile, TILE)
-        part_o[:, block] = jnp.dot(heads_s[...], wout_s[:, block], preferred_element_type=jnp.float32).astype(
-            jnp.bfloat16
-        )
-        return carry
-
-    lax.fori_loop(0, wout_s.shape[1] // TILE, out_body, 0)
+        raw_s[:, block] = jnp.dot(heads_s[:, :half], wout_s[:half, block], preferred_element_type=jnp.float32)
+        return carry
+
+    def second_body(tile, carry):
+        block = span(tile, TILE)
+        rest = jnp.dot(heads_s[:, half:], wout_s[half:, block], preferred_element_type=jnp.float32)
+        part_o[:, block] = (raw_s[:, block] + rest).astype(jnp.bfloat16)
+        return carry
+
+    lax.fori_loop(0, wout_s.shape[1] // TILE, first_body, 0)
+    load_out[1].wait()
+    lax.fori_loop(0, wout_s.shape[1] // TILE, second_body, 0)
     for copy in tails:
         copy.wait()
 
 
-def write_kernel(parts, state_ref, dec_ref, in_ref, u_ref, wup, next_ref, wup_o, buffers, sems, wsems):
-    rows, heads = state_ref.shape[:2]
+def write_pairs(first, last, state_ref, dec_ref, in_ref, u_ref, next_ref, buffers, sems):
+    rows = state_ref.shape[0]
     slots = buffers.shape[0]
-    loads = row_copies(wup, wup_o, wsems, 0, parts)
-    for copy in loads:
-        copy.start()
-
-    def store(pair):
+
+    def store(pair, which):
         slot = lax.rem(pair, slots)
-        return pltpu.make_async_copy(buffers.at[slot], next_ref.at[:, pl.ds(2 * pair, 2)], sems.at[slot])
+        return pltpu.make_async_copy(
+            buffers.at[slot, which], next_ref.at[:, 2 * pair + which], sems.at[slot, which]
+        )
 
     def pair_body(pair, carry):
-        @pl.when(pair >= slots)
-        def _():
-            store(pair - slots).wait()
-
         slot = lax.rem(pair, slots)
         turned = jnp.transpose(u_ref[:, pl.ds(pl.multiple_of(pair * LANES, LANES), LANES)])
         for which in range(2):
+
+            @pl.when(pair >= first + slots)
+            def _():
+                store(pair - slots, which).wait()
+
             head = 2 * pair + which
             wide = pl.ds(pl.multiple_of(head * STATE, STATE), STATE)
             column = turned[which * HEAD_DIM : (which + 1) * HEAD_DIM]
             decay, in_map = dec_ref[:, wide], in_ref[:, wide]
             for row in range(rows):
-                buffers[slot, row, which] = (
+                buffers[slot, which, row] = (
                     state_ref[row, head] * decay[row : row + 1]
                     + column[:, row : row + 1] * in_map[row : row + 1]
                 )
-        store(pair).start()
-        return carry
-
-    pairs = heads // 2
-    lax.fori_loop(0, pairs, pair_body, 0)
-    for pair in range(max(pairs - slots, 0), pairs):
-        store(pair).wait()
+            store(pair, which).start()
+        return carry
+
+    lax.fori_loop(first, last, pair_body, 0)
+    for pair in range(max(last - slots, first), last):
+        for which in range(2):
+            store(pair, which).wait()
+
+
+def early_kernel(first, last, parts, *refs):
+    wup, next_ref, wup_o, buffers, sems, wsems = refs[4:]
+    loads = row_copies(wup, wup_o, wsems, 0, parts)
+    for copy in loads:
+        copy.start()
+    write_pairs(first, last, *refs[:4], next_ref, buffers, sems)
     for copy in loads:
         copy.wait()
 
 
+def late_kernel(first, last, *refs):
+    next_ref, buffers, sems = refs[5:]
+    write_pairs(first, last, *refs[:4], next_ref, buffers, sems)
+
+
 def mlp_kernel(size, *refs):
-    me_ref, x_ref = refs[:2]
-    parts = refs[2 : 2 + size]
-    gain, wup, wdown = refs[2 + size : 5 + size]
-    base_o = refs[5 + size]
-    pieces = refs[6 + size : 5 + 2 * size]
-    hidden_s, total_s, normed_s, squared_s, wdown_s, sems = refs[5 + 2 * size :]
+    x_ref = refs[0]
+    parts = refs[1 : 1 + size]
+    gain, wup, wdown = refs[1 + size : 4 + size]
+    base_o = refs[4 + size]
+    pieces = refs[5 + size : 4 + 2 * size]
+    hidden_s, total_s, normed_s, squared_s, wdown_s, sems = refs[4 + 2 * size :]
     loads = row_copies(wdown, wdown_s, sems, 0, sems.shape[0])
     for copy in loads:
         copy.start()
     width = base_o.shape[1]
-    me = me_ref[0]
+    me = lax.axis_index("kv")
     total = x_ref[...].astype(jnp.float32)
     for part in parts:
         total = total + part[...].astype(jnp.float32)
@@ -415,14 +450,16 @@
         return carry
 
     lax.fori_loop(0, wup.shape[1] // TILE, up_body, 0)
-    out = None
-    depth = wdown.shape[0] // len(loads)
-    for part, copy in enumerate(loads):
-        copy.wait()
-        block = pl.ds(part * depth, depth)
-        down = jnp.dot(squared_s[:, block], wdown_s[block, :], preferred_element_type=jnp.float32)
-        out = down if out is None else out + down
-    total_s[...] = out
+    depth = wdown.shape[0] // sems.shape[0]
+    total_s[...] = jnp.zeros(total_s.shape, jnp.float32)
+
+    def down_body(part, carry):
+        block = pl.ds(pl.multiple_of(part * depth, depth), depth)
+        pltpu.make_async_copy(wdown.at[block], wdown_s.at[block], sems.at[part]).wait()
+        total_s[...] += jnp.dot(squared_s[:, block], wdown_s[block, :], preferred_element_type=jnp.float32)
+        return carry
+
+    lax.fori_loop(0, sems.shape[0], down_body, 0)
     own = pl.ds(pl.multiple_of(me * width, width), width)
     base_o[...] = hidden_s[:, own] + total_s[:, own]
     for step in range(1, size):
@@ -458,9 +495,8 @@
     model = width * size
     heads = state.shape[1]
     inner, maps = w_value.shape[1], w_maps.shape[1]
-    me = lax.axis_index("kv").astype(jnp.int32).reshape(1)
-
-    chunks = [tokens] + [shifted(tokens, size, step) for step in range(1, size)]
+
+    chunks = [tokens] + [swapped(tokens, size, step) for step in range(1, size)]
     past_value, past_maps = past_value.transpose(1, 0, 2), past_maps.transpose(1, 0, 2)
     maps_near, value_near, past_near = fetch([w_maps, past_value, past_maps], (8, 1, 1), "fetch_maps")
     part, whole, held, decay, in_map, written, value_tail, maps_tail = pl.pallas_call(
@@ -475,12 +511,12 @@
             jax.ShapeDtypeStruct((3, rows, inner), bf16),
             jax.ShapeDtypeStruct((3, rows, maps), bf16),
         ],
-        in_specs=[SMEM] * 4 + [VMEM] * (size + 8) + [HBM] * 4,
+        in_specs=[VMEM] * (size + 11) + [HBM] * 4,
         out_specs=[VMEM] * 6 + [HBM] * 2,
         scratch_shapes=[
             pltpu.VMEM((rows, model), bf16),
-            pltpu.VMEM(w_value.shape, bf16),
-            pltpu.VMEM(w_gate.shape, bf16),
+            pltpu.VMEM((model, 2 * inner), bf16),
+            pltpu.VMEM((rows, max(2 * inner, model)), f32),
             pltpu.VMEM(w_out.shape, bf16),
             pltpu.VMEM((rows, inner), bf16),
             pltpu.VMEM((rows, maps), bf16),
@@ -495,10 +531,9 @@
         cost_estimate=cost(2 * rows * model * (2 * inner + maps), 40e6),
         name="mixer",
     )(
-        me,
-        step_bias,
-        decay_log,
-        skip_gain,
+        step_bias.reshape(1, -1),
+        decay_log.reshape(1, -1),
+        skip_gain.reshape(1, -1),
         *chunks,
         mix_gain.reshape(1, -1),
         w_step.T,
@@ -512,24 +547,26 @@
     )
 
     parts = [part] + [shifted(part, size, step) for step in range(1, size)]
-    state_next, up_near = pl.pallas_call(
-        functools.partial(write_kernel, 4),
+    pairs = heads // 2
+    middle = pairs - pairs * LATE // 8
+    state_first, up_near = pl.pallas_call(
+        functools.partial(early_kernel, 0, middle, 4),
         out_shape=[jax.ShapeDtypeStruct(state.shape, f32), pltpu.VMEM(w_up.shape, bf16)],
         in_specs=[VMEM] * 4 + [HBM],
         out_specs=[HBM, VMEM],
         scratch_shapes=[
-            pltpu.VMEM((SLOTS, rows, 2, HEAD_DIM, STATE), f32),
-            pltpu.SemaphoreType.DMA((SLOTS,)),
+            pltpu.VMEM((SLOTS, 2, rows, HEAD_DIM, STATE), f32),
+            pltpu.SemaphoreType.DMA((SLOTS, 2)),
             pltpu.SemaphoreType.DMA((4,)),
         ],
         compiler_params=pltpu.CompilerParams(vmem_limit_bytes=8 << 20),
         cost_estimate=cost(1e6, 33e6),
-        name="write_state",
+        name="write_early",
     )(held, decay, in_map, written, in_hbm(w_up))
     base, *pieces = pl.pallas_call(
         functools.partial(mlp_kernel, size),
         out_shape=[pltpu.VMEM((rows, width), f32)] + [pltpu.VMEM((rows, width), bf16)] * (size - 1),
-        in_specs=[SMEM] + [VMEM] * (size + 3) + [HBM],
+        in_specs=[VMEM] * (size + 3) + [HBM],
         out_specs=[VMEM] * size,
         scratch_shapes=[
             pltpu.VMEM((rows, model), f32),
@@ -542,9 +579,24 @@
         compiler_params=pltpu.CompilerParams(vmem_limit_bytes=12 << 20),
         cost_estimate=cost(4 * rows * model * w_up.shape[1], 17e6),
         name="mlp",
-    )(me, whole, *parts, mlp_gain.reshape(1, -1), up_near, in_hbm(w_down))
-
-    arrived = [shifted(pieces[step - 1], size, step) for step in range(1, size)]
+    )(whole, *parts, mlp_gain.reshape(1, -1), up_near, in_hbm(w_down))
+
+    arrived = [shifted(pieces[step - 1], size, step) for step in range(size - 1, 0, -1)]
+    held, decay, in_map, written, _ = lax.optimization_barrier((held, decay, in_map, written, base))
+    state_next = pl.pallas_call(
+        functools.partial(late_kernel, middle, pairs),
+        out_shape=jax.ShapeDtypeStruct(state.shape, f32),
+        in_specs=[VMEM] * 4 + [HBM],
+        out_specs=HBM,
+        scratch_shapes=[
+            pltpu.VMEM((SLOTS, 2, rows, HEAD_DIM, STATE), f32),
+            pltpu.SemaphoreType.DMA((SLOTS, 2)),
+        ],
+        input_output_aliases={4: 0},
+        compiler_params=pltpu.CompilerParams(vmem_limit_bytes=8 << 20),
+        cost_estimate=cost(1e6, 1e7),
+        name="write_late",
+    )(held, decay, in_map, written, in_hbm(state_first))
     total = base
     for piece in arrived:
         total = total + piece.astype(f32)
@@ -560,11 +612,11 @@
     tokens, w_value, w_maps, state, w_up = (arrays[i] for i in (0, 3, 4, 14, 17))
     heads = state.shape[1]
     fits = (
-        size <= 8
+        size in (2, 4, 8)
         and heads % GROUP == 0
         and state.shape[2:] == (HEAD_DIM, STATE)
         and w_maps.shape[1] == heads * 2 * STATE
-        and all(extent % TILE == 0 for extent in (w_value.shape[1], w_maps.shape[1], w_up.shape[1]))
+        and all(extent % TILE == 0 for extent in (w_value.shape[1], w_maps.shape[1], w_up.shape[1], tokens.shape[1] * size))
         and tokens.shape[1] % LANES == 0
         and tokens.shape[0] % 8 == 0
     )

time: 47.6 us -> 45.8 us (0.962)
  waiting for transfers between devices: 1.54 us -> 0.02 us
  starting transfers between devices: 15.9 us -> 14.7 us
  Pallas kernels: 28.4 us -> 29.4 us
    ppermute x9 -> x6, starting transfers between devices: 15.9 us -> 8.96 us  [shifted(): lax.ppermute(block, 'kv', [(i, (i + step) % size) for i in range(size)])]
    ppermute x0 -> x3, starting transfers between devices: none -> 5.71 us  [swapped(): return lax.ppermute(block, 'kv', [(i, i ^ step) for i in range(size)])]
    pallas_call x1 -> x2, Pallas kernels: 7.85 us -> 9.39 us  [the longest x1 6.3 us: local_few(): pl.pallas_call(functools.partial(early_kernel, 0, middle, 4), out_shape=[...]
    ppermute x9 -> x6, waiting for transfers between devices: 1.54 us -> 0.02 us  [shifted(): lax.ppermute(block, 'kv', [(i, (i + step) % size) for i in range(size)])]
    pallas_call x1, Pallas kernels: 10.4 us -> 9.91 us  [local_few(): pl.pallas_call(functools.partial(mixer_kernel, size), out_shape=[pltpu.VM...]
  transfers between devices with their start and end apart: 9 -> 9, of which waited for: 2 -> 0; matrix products, arithmetic and copies ran while one was open for 0% -> 0% of each run, Pallas kernels for 29% -> 34%
where the time goes in v4:
time: 45.8 us; the launch traced here: 45.7 us
  Pallas kernels  29.4 us (64%)
  starting transfers between devices  14.7 us (32%)
  between operations  0.91 us (2%)
  other arithmetic  0.63 us (1%)
    pallas_call x1, Pallas kernels, local_few(): pl.pallas_call(functools.partial(mixer_kernel, size), out_shape=[pltpu.VM...  9.91 us
    ppermute x6, starting transfers between devices, shifted(): lax.ppermute(block, 'kv', [(i, (i + step) % size) for i in range(size)])  8.96 us
    pallas_call x1, Pallas kernels, local_few(): pl.pallas_call(functools.partial(early_kernel, 0, middle, 4), out_shape=[...  6.3 us
    pallas_call x1, Pallas kernels, fetch(): pl.pallas_call(functools.partial(fetch_kernel, parts), out_shape=[pltpu.V...  6.04 us
    ppermute x3, starting transfers between devices, swapped(): return lax.ppermute(block, 'kv', [(i, i ^ step) for i in range(size)])  5.71 us
    pallas_call x1, Pallas kernels, local_few(): pl.pallas_call(functools.partial(mlp_kernel, size), out_shape=[pltpu.VMEM...  4.06 us
    pallas_call x1, Pallas kernels, local_few(): pl.pallas_call(functools.partial(late_kernel, middle, pairs), out_shape=j...  3.08 us
  transfers between devices with their start and end apart: 9, of which 0 were waited for; matrix products, arithmetic and copies ran while one was open for 0% of the time, Pallas kernels for 34%

profile of v4, /device:TPU:0, one launch (start us, length us, event | category | flops | bytes accessed | tf_op | source)
XLA Modules:
  0.0 45.7 jit_solution(9259559354269230579)
XLA Ops:
  0.7 3.1 %collective-permute-start = (bf16[24,512]{1,0:T(8,128)(2,1)}, bf16[24,512]{1,0:T(8,128)(2,1)S(1)}, u32[]{:S(2)}, u32[]{:S(2)}) collective-permute-start(bf16[24,512]{1,0:T(8,128)(2,1)} %refs_3_.1), channel_id=1, source_target_pairs={{0,2},{2,0},{4,6},{6,4},{1,3},{3,1},{5,7},{7,5},{8,10},{10,8},{12,... | collective-permute-start | bytes 73736 | tf_op jit(solution)/shard_map/ppermute | solution.py:104
  3.8 2.6 %collective-permute-start.1 = (bf16[24,512]{1,0:T(8,128)(2,1)}, bf16[24,512]{1,0:T(8,128)(2,1)S(1)}, u32[]{:S(2)}, u32[]{:S(2)}) collective-permute-start(bf16[24,512]{1,0:T(8,128)(2,1)} %refs_3_.1), channel_id=1, source_target_pairs={{0,4},{2,6},{4,0},{6,2},{1,5},{3,7},{5,1},{7,3},{8,12},{10,14},{12... | collective-permute-start | bytes 73736 | tf_op jit(solution)/shard_map/ppermute | solution.py:104
  6.4 0.0 collective-permute-start.2
  6.4 6.0 %fetch_maps.1 = (bf16[2048,4096]{1,0:T(8,128)(2,1)S(1)}, bf16[3,24,1024]{2,1,0:T(8,128)(2,1)S(1)}, bf16[3,24,4096]{2,1,0:T(8,128)(2,1)S(1)}) custom-call(bf16[2048,4096]{1,0:T(8,128)(2,1)} %refs_0_.1, bf16[3,24,1024]{2,1,0:T(8,128)(2,1)} %bitcast.19, bf16[3,24,4096]{2,1,0:T(8,128)(2,1)} %bitcast.18), custom_call_target="tpu_custom_call" | custom-call | flops 1000000 | bytes 35028992 | tf_op jit(solution)/shard_map/fetch_maps/pallas_call | solution.py:146
  12.5 0.0 collective-permute-done.refs_4_
  12.5 0.0 collective-permute-done.1.refs_5_
  12.5 0.0 collective-permute-done.2.refs_6_
  12.6 9.9 %mixer.1 = (bf16[24,2048]{1,0:T(8,128)(2,1)S(1)}, bf16[24,2048]{1,0:T(8,128)(2,1)S(1)}, f32[24,16,64,128]{3,2,1,0:T(8,128)S(1)}, f32[24,2048]{1,0:T(8,128)S(1)},...) custom-call(f32[1,16]{1,0:T(1,128)S(1)} %bitcast.15, ...), custom_call_target="tpu_custom_call" | custom-call | flops 603979776 | bytes 40000000 | tf_op jit(solution)/shard_map/mixer/pallas_call | solution.py:502
  22.5 0.0 copy-start.5
  22.5 1.0 %collective-permute-start.3 = (bf16[24,2048]{1,0:T(8,128)(2,1)S(1)}, bf16[24,2048]{1,0:T(8,128)(2,1)S(1)}, u32[]{:S(2)}, u32[]{:S(2)}) collective-permute-start(bf16[24,2048]{1,0:T(8,128)(2,1)S(1)} %get-tuple-element.29.refs_1_), channel_id=1, source_target_pairs={{0,2},{2,4},{4,6},{6,0},{1,3},{3,5},{5,7},{7,1},{8,10},{10,12},{12... | collective-permute-start | bytes 294920 | tf_op jit(solution)/shard_map/ppermute | solution.py:108
  23.5 3.5 %collective-permute-start.4 = (bf16[24,2048]{1,0:T(8,128)(2,1)S(1)}, bf16[24,2048]{1,0:T(8,128)(2,1)S(1)}, u32[]{:S(2)}, u32[]{:S(2)}) collective-permute-start(bf16[24,2048]{1,0:T(8,128)(2,1)S(1)} %get-tuple-element.29.refs_1_), channel_id=1, source_target_pairs={{0,4},{2,6},{4,0},{6,2},{1,5},{3,7},{5,1},{7,3},{8,12},{10,14},{12... | collective-permute-start | bytes 294920 | tf_op jit(solution)/shard_map/ppermute | solution.py:108
  27.0 0.4 collective-permute-start.5
  27.4 6.3 %write_early.1 = (f32[24,16,64,128]{3,2,1,0:T(8,128)}, bf16[2048,2048]{1,0:T(8,128)(2,1)S(1)}) custom-call(f32[24,16,64,128]{3,2,1,0:T(8,128)S(1)} %get-tuple-element.39.refs_0_, f32[24,2048]{1,0:T(8,128)S(1)} %get-tuple-element.40.refs_1_, f32[24,2048]{1,0:T(8,128)S(1)} %get-tuple-element.41.refs_2_, f32[24,1024]{1,0:T(8,128)S(1)} %get-tuple-element.42.refs_3_, ...), custom_call_target="tpu_custom_call" | custom-call | flops 1000000 | bytes 33000000 | tf_op jit(solution)/shard_map/write_early/pallas_call | solution.py:552
  33.7 0.0 collective-permute-done.3.refs_2_
  33.7 0.0 collective-permute-done.4.refs_3_
  33.8 0.0 collective-permute-done.5.refs_4_
  33.8 4.1 %mlp.1 = (f32[24,512]{1,0:T(8,128)S(1)}, bf16[24,512]{1,0:T(8,128)(2,1)S(1)}, bf16[24,512]{1,0:T(8,128)(2,1)S(1)}, bf16[24,512]{1,0:T(8,128)(2,1)S(1)}) custom-call(bf16[24,2048]{1,0:T(8,128)(2,1)S(1)} %get-tuple-element.28.refs_0_, bf16[24,2048]{1,0:T(8,128)(2,1)S(1)} %get-tuple-element.29.refs_1_, bf16[24,2048]{1,0:T(8,128)(2,1)S(1)} %collective-permute-done.3.refs_2_, ...), custom_call_target="tpu_custom_call" | custom-call | flops 402653184 | bytes 17000000 | tf_op jit(solution)/shard_map/mlp/pallas_call | solution.py:566
  37.8 1.6 %collective-permute-start.8 = (bf16[24,512]{1,0:T(8,128)(2,1)S(1)}, bf16[24,512]{1,0:T(8,128)(2,1)S(1)}, u32[]{:S(2)}, u32[]{:S(2)}) collective-permute-start(bf16[24,512]{1,0:T(8,128)(2,1)S(1)} %get-tuple-element.38), channel_id=1, source_target_pairs={{0,2},{2,4},{4,6},{6,0},{1,3},{3,5},{5,7},{7,1},{8,10},{10,12},{12... | collective-permute-start | bytes 73736 | tf_op jit(solution)/shard_map/ppermute | solution.py:108
  39.5 1.5 %collective-permute-start.7 = (bf16[24,512]{1,0:T(8,128)(2,1)S(1)}, bf16[24,512]{1,0:T(8,128)(2,1)S(1)}, u32[]{:S(2)}, u32[]{:S(2)}) collective-permute-start(bf16[24,512]{1,0:T(8,128)(2,1)S(1)} %get-tuple-element.37), channel_id=1, source_target_pairs={{0,4},{2,6},{4,0},{6,2},{1,5},{3,7},{5,1},{7,3},{8,12},{10,14},{12... | collective-permute-start | bytes 73736 | tf_op jit(solution)/shard_map/ppermute | solution.py:108
  41.0 0.9 %collective-permute-start.6 = (bf16[24,512]{1,0:T(8,128)(2,1)S(1)}, bf16[24,512]{1,0:T(8,128)(2,1)S(1)}, u32[]{:S(2)}, u32[]{:S(2)}) collective-permute-start(bf16[24,512]{1,0:T(8,128)(2,1)S(1)} %get-tuple-element.36), channel_id=1, source_target_pairs={{0,6},{2,0},{4,2},{6,4},{1,7},{3,1},{5,3},{7,5},{8,14},{10,8},{12,... | collective-permute-start | bytes 73736 | tf_op jit(solution)/shard_map/ppermute | solution.py:108
  41.9 3.1 %write_late.1 = f32[24,16,64,128]{3,2,1,0:T(8,128)} custom-call(f32[24,16,64,128]{3,2,1,0:T(8,128)S(1)} %get-tuple-element.39.refs_0_, f32[24,2048]{1,0:T(8,128)S(1)} %get-tuple-element.40.refs_1_, f32[24,2048]{1,0:T(8,128)S(1)} %get-tuple-element.41.refs_2_, f32[24,1024]{1,0:T(8,128)S(1)} %get-tuple-element.42.refs_3_, ...), custom_call_target="tpu_custom_call", output_to_operand_aliasing={{}: (4, {})} | custom-call | flops 1000000 | bytes 10000000 | tf_op jit(solution)/shard_map/write_late/pallas_call | solution.py:586
  45.0 0.0 collective-permute-done.7
  45.0 0.0 collective-permute-done.6
  45.0 0.6 %add_convert_fusion = bf16[24,512]{1,0:T(8,128)(2,1)} fusion(bf16[24,512]{1,0:T(8,128)(2,1)S(1)} %collective-permute-done.8, bf16[24,512]{1,0:T(8,128)(2,1)S(1)} %collective-permute-done.7, f32[24,512]{1,0:T(8,128)S(1)} %get-tuple-element.35, bf16[24,512]{1,0:T(8,128)(2,1)S(1)} %collective-permute-done.6), kind=kLoop, calls=%fused_computation | loop fusion | flops 86016 | bytes 147456 | tf_op jit(solution)/shard_map/convert_element_type | solution.py:604
  (20 shorter events, 0.0 us)
Async XLA Ops:
  0.6 11.9 %copy-start.2 = (bf16[24,512]{1,0:T(8,128)(2,1)S(1)}, bf16[24,512]{1,0:T(8,128)(2,1)}, u32[]{:S(2)}) copy-start(bf16[24,512]{1,0:T(8,128)(2,1)} %refs_3_.1) | copy-start | bytes 73732
  0.6 11.9 %copy-start.7 = (f32[16]{0:T(128)S(1)}, f32[16]{0:T(128)}, u32[]{:S(2)}) copy-start(f32[16]{0:T(128)} %param.29) | copy-start | bytes 196
  0.7 11.9 %copy-start.8 = (f32[16]{0:T(128)S(1)}, f32[16]{0:T(128)}, u32[]{:S(2)}) copy-start(f32[16]{0:T(128)} %param.30) | copy-start | bytes 196
  0.7 11.9 %copy-start.9 = (f32[16]{0:T(128)S(1)}, f32[16]{0:T(128)}, u32[]{:S(2)}) copy-start(f32[16]{0:T(128)} %param.31) | copy-start | bytes 196
  0.7 11.9 %copy-start.4 = (f32[2048]{0:T(1024)S(1)}, f32[2048]{0:T(1024)}, u32[]{:S(2)}) copy-start(f32[2048]{0:T(1024)} %param.20) | copy-start | bytes 24580
  0.7 11.9 %copy-start = (bf16[2048,64]{0,1:T(8,128)(2,1)S(1)}, bf16[2048,64]{0,1:T(8,128)(2,1)}, u32[]{:S(2)}) copy-start(bf16[2048,64]{0,1:T(8,128)(2,1)} %param.24) | copy-start | bytes 786436
  0.7 11.9 %copy-start.3 = (f32[4,1024]{1,0:T(4,128)S(1)}, f32[4,1024]{1,0:T(4,128)}, u32[]{:S(2)}) copy-start(f32[4,1024]{1,0:T(4,128)} %refs_9_.1) | copy-start | bytes 49156
  0.7 11.9 %copy-start.1 = (f32[4,4096]{1,0:T(4,128)S(1)}, f32[4,4096]{1,0:T(4,128)}, u32[]{:S(2)}) copy-start(f32[4,4096]{1,0:T(4,128)} %refs_10_.1) | copy-start | bytes 196612
  0.7 11.9 %copy-start.6 = (f32[1024]{0:T(1024)S(1)}, f32[1024]{0:T(1024)}, u32[]{:S(2)}) copy-start(f32[1024]{0:T(1024)} %param.32) | copy-start | bytes 12292
  0.7 11.8 %collective-permute-start = (bf16[24,512]{1,0:T(8,128)(2,1)}, bf16[24,512]{1,0:T(8,128)(2,1)S(1)}, u32[]{:S(2)}, u32[]{:S(2)}) collective-permute-start(bf16[24,512]{1,0:T(8,128)(2,1)} %refs_3_.1), channel_id=1, source_target_pairs={{0,2},{2,0},{4,6},{6,4},{1,3},{3,1},{5,7},{7,5},{8,10},{10,8},{12,... | collective-permute-start | bytes 73736 | tf_op jit(solution)/shard_map/ppermute | solution.py:104
  3.8 8.7 %collective-permute-start.1 = (bf16[24,512]{1,0:T(8,128)(2,1)}, bf16[24,512]{1,0:T(8,128)(2,1)S(1)}, u32[]{:S(2)}, u32[]{:S(2)}) collective-permute-start(bf16[24,512]{1,0:T(8,128)(2,1)} %refs_3_.1), channel_id=1, source_target_pairs={{0,4},{2,6},{4,0},{6,2},{1,5},{3,7},{5,1},{7,3},{8,12},{10,14},{12... | collective-permute-start | bytes 73736 | tf_op jit(solution)/shard_map/ppermute | solution.py:104
  6.4 6.1 %collective-permute-start.2 = (bf16[24,512]{1,0:T(8,128)(2,1)}, bf16[24,512]{1,0:T(8,128)(2,1)S(1)}, u32[]{:S(2)}, u32[]{:S(2)}) collective-permute-start(bf16[24,512]{1,0:T(8,128)(2,1)} %refs_3_.1), channel_id=1, source_target_pairs={{0,6},{2,4},{4,2},{6,0},{1,7},{3,5},{5,3},{7,1},{8,14},{10,12},{12... | collective-permute-start | bytes 73736 | tf_op jit(solution)/shard_map/ppermute | solution.py:104
  22.5 11.2 %copy-start.5 = (f32[2048]{0:T(1024)S(1)}, f32[2048]{0:T(1024)}, u32[]{:S(2)}) copy-start(f32[2048]{0:T(1024)} %param.35) | copy-start | bytes 24580
  22.5 11.2 %collective-permute-start.3 = (bf16[24,2048]{1,0:T(8,128)(2,1)S(1)}, bf16[24,2048]{1,0:T(8,128)(2,1)S(1)}, u32[]{:S(2)}, u32[]{:S(2)}) collective-permute-start(bf16[24,2048]{1,0:T(8,128)(2,1)S(1)} %get-tuple-element.29.refs_1_), channel_id=1, source_target_pairs={{0,2},{2,4},{4,6},{6,0},{1,3},{3,5},{5,7},{7,1},{8,10},{10,12},{12... | collective-permute-start | bytes 294920 | tf_op jit(solution)/shard_map/ppermute | solution.py:108
  23.5 10.3 %collective-permute-start.4 = (bf16[24,2048]{1,0:T(8,128)(2,1)S(1)}, bf16[24,2048]{1,0:T(8,128)(2,1)S(1)}, u32[]{:S(2)}, u32[]{:S(2)}) collective-permute-start(bf16[24,2048]{1,0:T(8,128)(2,1)S(1)} %get-tuple-element.29.refs_1_), channel_id=1, source_target_pairs={{0,4},{2,6},{4,0},{6,2},{1,5},{3,7},{5,1},{7,3},{8,12},{10,14},{12... | collective-permute-start | bytes 294920 | tf_op jit(solution)/shard_map/ppermute | solution.py:108
  27.0 6.8 %collective-permute-start.5 = (bf16[24,2048]{1,0:T(8,128)(2,1)S(1)}, bf16[24,2048]{1,0:T(8,128)(2,1)S(1)}, u32[]{:S(2)}, u32[]{:S(2)}) collective-permute-start(bf16[24,2048]{1,0:T(8,128)(2,1)S(1)} %get-tuple-element.29.refs_1_), channel_id=1, source_target_pairs={{0,6},{2,0},{4,2},{6,4},{1,7},{3,1},{5,3},{7,5},{8,14},{10,8},{12,... | collective-permute-start | bytes 294920 | tf_op jit(solution)/shard_map/ppermute | solution.py:108
  37.8 7.2 %collective-permute-start.8 = (bf16[24,512]{1,0:T(8,128)(2,1)S(1)}, bf16[24,512]{1,0:T(8,128)(2,1)S(1)}, u32[]{:S(2)}, u32[]{:S(2)}) collective-permute-start(bf16[24,512]{1,0:T(8,128)(2,1)S(1)} %get-tuple-element.38), channel_id=1, source_target_pairs={{0,2},{2,4},{4,6},{6,0},{1,3},{3,5},{5,7},{7,1},{8,10},{10,12},{12... | collective-permute-start | bytes 73736 | tf_op jit(solution)/shard_map/ppermute | solution.py:108
  39.5 5.5 %collective-permute-start.7 = (bf16[24,512]{1,0:T(8,128)(2,1)S(1)}, bf16[24,512]{1,0:T(8,128)(2,1)S(1)}, u32[]{:S(2)}, u32[]{:S(2)}) collective-permute-start(bf16[24,512]{1,0:T(8,128)(2,1)S(1)} %get-tuple-element.37), channel_id=1, source_target_pairs={{0,4},{2,6},{4,0},{6,2},{1,5},{3,7},{5,1},{7,3},{8,12},{10,14},{12... | collective-permute-start | bytes 73736 | tf_op jit(solution)/shard_map/ppermute | solution.py:108
  41.0 4.0 %collective-permute-start.6 = (bf16[24,512]{1,0:T(8,128)(2,1)S(1)}, bf16[24,512]{1,0:T(8,128)(2,1)S(1)}, u32[]{:S(2)}, u32[]{:S(2)}) collective-permute-start(bf16[24,512]{1,0:T(8,128)(2,1)S(1)} %get-tuple-element.36), channel_id=1, source_target_pairs={{0,6},{2,0},{4,2},{6,4},{1,7},{3,1},{5,3},{7,5},{8,14},{10,8},{12,... | collective-permute-start | bytes 73736 | tf_op jit(solution)/shard_map/ppermute | solution.py:108

commit v5 on v4

--- a/solution.py
+++ b/solution.py
@@ -208,8 +208,6 @@
             total = total + past[t, :, block].astype(jnp.float32) * taps[t : t + 1, block]
         return silu(total)
 
-    for copy in tails[:2]:
-        copy.start()
     def span(index, extent):
         return pl.ds(pl.multiple_of(index * extent, extent), extent)
 
@@ -241,7 +239,6 @@
     lax.fori_loop(0, tiles, maps_body, 0)
     for pair in range(tiles, later):
         state_copy(pair).start()
-    tails[2].start()
     for copy in load_value + load_gate:
         copy.wait()
 
@@ -262,7 +259,8 @@
         return carry
 
     lax.fori_loop(0, inner // TILE, value_body, 0)
-    tails[3].start()
+    for copy in tails:
+        copy.start()
 
     row_of = lax.broadcasted_iota(jnp.int32, (rows, STATE), 0)
     part_of = lax.broadcasted_iota(jnp.int32, (rows, GROUP * HEAD_DIM), 1) // HEAD_DIM

time: 45.8 us -> 45.7 us (level)
  no operation moved by 1% of the time
where the time goes in v5:
time: 45.7 us; the launch traced here: 45.6 us
  Pallas kernels  29.3 us (64%)
  starting transfers between devices  14.7 us (32%)
  between operations  0.91 us (2%)
  other arithmetic  0.63 us (1%)
    pallas_call x1, Pallas kernels, local_few(): pl.pallas_call(functools.partial(mixer_kernel, size), out_shape=[pltpu.VM...  9.8 us
    ppermute x6, starting transfers between devices, shifted(): lax.ppermute(block, 'kv', [(i, (i + step) % size) for i in range(size)])  8.96 us
    pallas_call x1, Pallas kernels, local_few(): pl.pallas_call(functools.partial(early_kernel, 0, middle, 4), out_shape=[...  6.3 us
    pallas_call x1, Pallas kernels, fetch(): pl.pallas_call(functools.partial(fetch_kernel, parts), out_shape=[pltpu.V...  6.04 us
    ppermute x3, starting transfers between devices, swapped(): return lax.ppermute(block, 'kv', [(i, i ^ step) for i in range(size)])  5.71 us
    pallas_call x1, Pallas kernels, local_few(): pl.pallas_call(functools.partial(mlp_kernel, size), out_shape=[pltpu.VMEM...  4.06 us
    pallas_call x1, Pallas kernels, local_few(): pl.pallas_call(functools.partial(late_kernel, middle, pairs), out_shape=j...  3.08 us
  transfers between devices with their start and end apart: 9, of which 0 were waited for; matrix products, arithmetic and copies ran while one was open for 0% of the time, Pallas kernels for 34%

profile of v5, /device:TPU:0, one launch (start us, length us, event | category | flops | bytes accessed | tf_op | source)
XLA Modules:
  0.0 45.6 jit_solution(14398687326479708715)
XLA Ops:
  0.7 3.1 %collective-permute-start = (bf16[24,512]{1,0:T(8,128)(2,1)}, bf16[24,512]{1,0:T(8,128)(2,1)S(1)}, u32[]{:S(2)}, u32[]{:S(2)}) collective-permute-start(bf16[24,512]{1,0:T(8,128)(2,1)} %refs_3_.1), channel_id=1, source_target_pairs={{0,2},{2,0},{4,6},{6,4},{1,3},{3,1},{5,7},{7,5},{8,10},{10,8},{12,... | collective-permute-start | bytes 73736 | tf_op jit(solution)/shard_map/ppermute | solution.py:104
  3.8 2.6 %collective-permute-start.1 = (bf16[24,512]{1,0:T(8,128)(2,1)}, bf16[24,512]{1,0:T(8,128)(2,1)S(1)}, u32[]{:S(2)}, u32[]{:S(2)}) collective-permute-start(bf16[24,512]{1,0:T(8,128)(2,1)} %refs_3_.1), channel_id=1, source_target_pairs={{0,4},{2,6},{4,0},{6,2},{1,5},{3,7},{5,1},{7,3},{8,12},{10,14},{12... | collective-permute-start | bytes 73736 | tf_op jit(solution)/shard_map/ppermute | solution.py:104
  6.4 0.0 collective-permute-start.2
  6.4 6.0 %fetch_maps.1 = (bf16[2048,4096]{1,0:T(8,128)(2,1)S(1)}, bf16[3,24,1024]{2,1,0:T(8,128)(2,1)S(1)}, bf16[3,24,4096]{2,1,0:T(8,128)(2,1)S(1)}) custom-call(bf16[2048,4096]{1,0:T(8,128)(2,1)} %refs_0_.1, bf16[3,24,1024]{2,1,0:T(8,128)(2,1)} %bitcast.19, bf16[3,24,4096]{2,1,0:T(8,128)(2,1)} %bitcast.18), custom_call_target="tpu_custom_call" | custom-call | flops 1000000 | bytes 35028992 | tf_op jit(solution)/shard_map/fetch_maps/pallas_call | solution.py:146
  12.5 0.0 collective-permute-done.refs_4_
  12.5 0.0 collective-permute-done.1.refs_5_
  12.5 0.0 collective-permute-done.2.refs_6_
  12.6 9.8 %mixer.1 = (bf16[24,2048]{1,0:T(8,128)(2,1)S(1)}, bf16[24,2048]{1,0:T(8,128)(2,1)S(1)}, f32[24,16,64,128]{3,2,1,0:T(8,128)S(1)}, f32[24,2048]{1,0:T(8,128)S(1)},...) custom-call(f32[1,16]{1,0:T(1,128)S(1)} %bitcast.15, ...), custom_call_target="tpu_custom_call" | custom-call | flops 603979776 | bytes 40000000 | tf_op jit(solution)/shard_map/mixer/pallas_call | solution.py:500
  22.4 0.0 copy-start.5
  22.4 0.9 %collective-permute-start.3 = (bf16[24,2048]{1,0:T(8,128)(2,1)S(1)}, bf16[24,2048]{1,0:T(8,128)(2,1)S(1)}, u32[]{:S(2)}, u32[]{:S(2)}) collective-permute-start(bf16[24,2048]{1,0:T(8,128)(2,1)S(1)} %get-tuple-element.29.refs_1_), channel_id=1, source_target_pairs={{0,2},{2,4},{4,6},{6,0},{1,3},{3,5},{5,7},{7,1},{8,10},{10,12},{12... | collective-permute-start | bytes 294920 | tf_op jit(solution)/shard_map/ppermute | solution.py:108
  23.4 3.5 %collective-permute-start.4 = (bf16[24,2048]{1,0:T(8,128)(2,1)S(1)}, bf16[24,2048]{1,0:T(8,128)(2,1)S(1)}, u32[]{:S(2)}, u32[]{:S(2)}) collective-permute-start(bf16[24,2048]{1,0:T(8,128)(2,1)S(1)} %get-tuple-element.29.refs_1_), channel_id=1, source_target_pairs={{0,4},{2,6},{4,0},{6,2},{1,5},{3,7},{5,1},{7,3},{8,12},{10,14},{12... | collective-permute-start | bytes 294920 | tf_op jit(solution)/shard_map/ppermute | solution.py:108
  26.9 0.5 collective-permute-start.5
  27.3 6.3 %write_early.1 = (f32[24,16,64,128]{3,2,1,0:T(8,128)}, bf16[2048,2048]{1,0:T(8,128)(2,1)S(1)}) custom-call(f32[24,16,64,128]{3,2,1,0:T(8,128)S(1)} %get-tuple-element.39.refs_0_, f32[24,2048]{1,0:T(8,128)S(1)} %get-tuple-element.40.refs_1_, f32[24,2048]{1,0:T(8,128)S(1)} %get-tuple-element.41.refs_2_, f32[24,1024]{1,0:T(8,128)S(1)} %get-tuple-element.42.refs_3_, ...), custom_call_target="tpu_custom_call" | custom-call | flops 1000000 | bytes 33000000 | tf_op jit(solution)/shard_map/write_early/pallas_call | solution.py:550
  33.6 0.0 collective-permute-done.3.refs_2_
  33.6 0.0 collective-permute-done.4.refs_3_
  33.7 0.0 collective-permute-done.5.refs_4_
  33.7 4.1 %mlp.1 = (f32[24,512]{1,0:T(8,128)S(1)}, bf16[24,512]{1,0:T(8,128)(2,1)S(1)}, bf16[24,512]{1,0:T(8,128)(2,1)S(1)}, bf16[24,512]{1,0:T(8,128)(2,1)S(1)}) custom-call(bf16[24,2048]{1,0:T(8,128)(2,1)S(1)} %get-tuple-element.28.refs_0_, bf16[24,2048]{1,0:T(8,128)(2,1)S(1)} %get-tuple-element.29.refs_1_, bf16[24,2048]{1,0:T(8,128)(2,1)S(1)} %collective-permute-done.3.refs_2_, ...), custom_call_target="tpu_custom_call" | custom-call | flops 402653184 | bytes 17000000 | tf_op jit(solution)/shard_map/mlp/pallas_call | solution.py:564
  37.7 1.6 %collective-permute-start.8 = (bf16[24,512]{1,0:T(8,128)(2,1)S(1)}, bf16[24,512]{1,0:T(8,128)(2,1)S(1)}, u32[]{:S(2)}, u32[]{:S(2)}) collective-permute-start(bf16[24,512]{1,0:T(8,128)(2,1)S(1)} %get-tuple-element.38), channel_id=1, source_target_pairs={{0,2},{2,4},{4,6},{6,0},{1,3},{3,5},{5,7},{7,1},{8,10},{10,12},{12... | collective-permute-start | bytes 73736 | tf_op jit(solution)/shard_map/ppermute | solution.py:108
  39.4 1.6 %collective-permute-start.7 = (bf16[24,512]{1,0:T(8,128)(2,1)S(1)}, bf16[24,512]{1,0:T(8,128)(2,1)S(1)}, u32[]{:S(2)}, u32[]{:S(2)}) collective-permute-start(bf16[24,512]{1,0:T(8,128)(2,1)S(1)} %get-tuple-element.37), channel_id=1, source_target_pairs={{0,4},{2,6},{4,0},{6,2},{1,5},{3,7},{5,1},{7,3},{8,12},{10,14},{12... | collective-permute-start | bytes 73736 | tf_op jit(solution)/shard_map/ppermute | solution.py:108
  40.9 0.9 %collective-permute-start.6 = (bf16[24,512]{1,0:T(8,128)(2,1)S(1)}, bf16[24,512]{1,0:T(8,128)(2,1)S(1)}, u32[]{:S(2)}, u32[]{:S(2)}) collective-permute-start(bf16[24,512]{1,0:T(8,128)(2,1)S(1)} %get-tuple-element.36), channel_id=1, source_target_pairs={{0,6},{2,0},{4,2},{6,4},{1,7},{3,1},{5,3},{7,5},{8,14},{10,8},{12,... | collective-permute-start | bytes 73736 | tf_op jit(solution)/shard_map/ppermute | solution.py:108
  41.8 3.1 %write_late.1 = f32[24,16,64,128]{3,2,1,0:T(8,128)} custom-call(f32[24,16,64,128]{3,2,1,0:T(8,128)S(1)} %get-tuple-element.39.refs_0_, f32[24,2048]{1,0:T(8,128)S(1)} %get-tuple-element.40.refs_1_, f32[24,2048]{1,0:T(8,128)S(1)} %get-tuple-element.41.refs_2_, f32[24,1024]{1,0:T(8,128)S(1)} %get-tuple-element.42.refs_3_, ...), custom_call_target="tpu_custom_call", output_to_operand_aliasing={{}: (4, {})} | custom-call | flops 1000000 | bytes 10000000 | tf_op jit(solution)/shard_map/write_late/pallas_call | solution.py:584
  44.9 0.0 collective-permute-done.8
  44.9 0.0 collective-permute-done.6
  44.9 0.6 %add_convert_fusion = bf16[24,512]{1,0:T(8,128)(2,1)} fusion(bf16[24,512]{1,0:T(8,128)(2,1)S(1)} %collective-permute-done.8, bf16[24,512]{1,0:T(8,128)(2,1)S(1)} %collective-permute-done.7, f32[24,512]{1,0:T(8,128)S(1)} %get-tuple-element.35, bf16[24,512]{1,0:T(8,128)(2,1)S(1)} %collective-permute-done.6), kind=kLoop, calls=%fused_computation | loop fusion | flops 86016 | bytes 147456 | tf_op jit(solution)/shard_map/convert_element_type | solution.py:602
  (20 shorter events, 0.0 us)
Async XLA Ops:
  0.6 11.9 %copy-start.2 = (bf16[24,512]{1,0:T(8,128)(2,1)S(1)}, bf16[24,512]{1,0:T(8,128)(2,1)}, u32[]{:S(2)}) copy-start(bf16[24,512]{1,0:T(8,128)(2,1)} %refs_3_.1) | copy-start | bytes 73732
  0.6 11.9 %copy-start.7 = (f32[16]{0:T(128)S(1)}, f32[16]{0:T(128)}, u32[]{:S(2)}) copy-start(f32[16]{0:T(128)} %param.29) | copy-start | bytes 196
  0.7 11.9 %copy-start.8 = (f32[16]{0:T(128)S(1)}, f32[16]{0:T(128)}, u32[]{:S(2)}) copy-start(f32[16]{0:T(128)} %param.30) | copy-start | bytes 196
  0.7 11.9 %copy-start.9 = (f32[16]{0:T(128)S(1)}, f32[16]{0:T(128)}, u32[]{:S(2)}) copy-start(f32[16]{0:T(128)} %param.31) | copy-start | bytes 196
  0.7 11.9 %copy-start.4 = (f32[2048]{0:T(1024)S(1)}, f32[2048]{0:T(1024)}, u32[]{:S(2)}) copy-start(f32[2048]{0:T(1024)} %param.20) | copy-start | bytes 24580
  0.7 11.9 %copy-start = (bf16[2048,64]{0,1:T(8,128)(2,1)S(1)}, bf16[2048,64]{0,1:T(8,128)(2,1)}, u32[]{:S(2)}) copy-start(bf16[2048,64]{0,1:T(8,128)(2,1)} %param.24) | copy-start | bytes 786436
  0.7 11.9 %copy-start.3 = (f32[4,1024]{1,0:T(4,128)S(1)}, f32[4,1024]{1,0:T(4,128)}, u32[]{:S(2)}) copy-start(f32[4,1024]{1,0:T(4,128)} %refs_9_.1) | copy-start | bytes 49156
  0.7 11.9 %copy-start.1 = (f32[4,4096]{1,0:T(4,128)S(1)}, f32[4,4096]{1,0:T(4,128)}, u32[]{:S(2)}) copy-start(f32[4,4096]{1,0:T(4,128)} %refs_10_.1) | copy-start | bytes 196612
  0.7 11.9 %copy-start.6 = (f32[1024]{0:T(1024)S(1)}, f32[1024]{0:T(1024)}, u32[]{:S(2)}) copy-start(f32[1024]{0:T(1024)} %param.32) | copy-start | bytes 12292
  0.7 11.8 %collective-permute-start = (bf16[24,512]{1,0:T(8,128)(2,1)}, bf16[24,512]{1,0:T(8,128)(2,1)S(1)}, u32[]{:S(2)}, u32[]{:S(2)}) collective-permute-start(bf16[24,512]{1,0:T(8,128)(2,1)} %refs_3_.1), channel_id=1, source_target_pairs={{0,2},{2,0},{4,6},{6,4},{1,3},{3,1},{5,7},{7,5},{8,10},{10,8},{12,... | collective-permute-start | bytes 73736 | tf_op jit(solution)/shard_map/ppermute | solution.py:104
  3.8 8.7 %collective-permute-start.1 = (bf16[24,512]{1,0:T(8,128)(2,1)}, bf16[24,512]{1,0:T(8,128)(2,1)S(1)}, u32[]{:S(2)}, u32[]{:S(2)}) collective-permute-start(bf16[24,512]{1,0:T(8,128)(2,1)} %refs_3_.1), channel_id=1, source_target_pairs={{0,4},{2,6},{4,0},{6,2},{1,5},{3,7},{5,1},{7,3},{8,12},{10,14},{12... | collective-permute-start | bytes 73736 | tf_op jit(solution)/shard_map/ppermute | solution.py:104
  6.4 6.1 %collective-permute-start.2 = (bf16[24,512]{1,0:T(8,128)(2,1)}, bf16[24,512]{1,0:T(8,128)(2,1)S(1)}, u32[]{:S(2)}, u32[]{:S(2)}) collective-permute-start(bf16[24,512]{1,0:T(8,128)(2,1)} %refs_3_.1), channel_id=1, source_target_pairs={{0,6},{2,4},{4,2},{6,0},{1,7},{3,5},{5,3},{7,1},{8,14},{10,12},{12... | collective-permute-start | bytes 73736 | tf_op jit(solution)/shard_map/ppermute | solution.py:104
  22.4 11.2 %copy-start.5 = (f32[2048]{0:T(1024)S(1)}, f32[2048]{0:T(1024)}, u32[]{:S(2)}) copy-start(f32[2048]{0:T(1024)} %param.35) | copy-start | bytes 24580
  22.4 11.2 %collective-permute-start.3 = (bf16[24,2048]{1,0:T(8,128)(2,1)S(1)}, bf16[24,2048]{1,0:T(8,128)(2,1)S(1)}, u32[]{:S(2)}, u32[]{:S(2)}) collective-permute-start(bf16[24,2048]{1,0:T(8,128)(2,1)S(1)} %get-tuple-element.29.refs_1_), channel_id=1, source_target_pairs={{0,2},{2,4},{4,6},{6,0},{1,3},{3,5},{5,7},{7,1},{8,10},{10,12},{12... | collective-permute-start | bytes 294920 | tf_op jit(solution)/shard_map/ppermute | solution.py:108
  23.4 10.3 %collective-permute-start.4 = (bf16[24,2048]{1,0:T(8,128)(2,1)S(1)}, bf16[24,2048]{1,0:T(8,128)(2,1)S(1)}, u32[]{:S(2)}, u32[]{:S(2)}) collective-permute-start(bf16[24,2048]{1,0:T(8,128)(2,1)S(1)} %get-tuple-element.29.refs_1_), channel_id=1, source_target_pairs={{0,4},{2,6},{4,0},{6,2},{1,5},{3,7},{5,1},{7,3},{8,12},{10,14},{12... | collective-permute-start | bytes 294920 | tf_op jit(solution)/shard_map/ppermute | solution.py:108
  26.9 6.8 %collective-permute-start.5 = (bf16[24,2048]{1,0:T(8,128)(2,1)S(1)}, bf16[24,2048]{1,0:T(8,128)(2,1)S(1)}, u32[]{:S(2)}, u32[]{:S(2)}) collective-permute-start(bf16[24,2048]{1,0:T(8,128)(2,1)S(1)} %get-tuple-element.29.refs_1_), channel_id=1, source_target_pairs={{0,6},{2,0},{4,2},{6,4},{1,7},{3,1},{5,3},{7,5},{8,14},{10,8},{12,... | collective-permute-start | bytes 294920 | tf_op jit(solution)/shard_map/ppermute | solution.py:108
  37.7 7.2 %collective-permute-start.8 = (bf16[24,512]{1,0:T(8,128)(2,1)S(1)}, bf16[24,512]{1,0:T(8,128)(2,1)S(1)}, u32[]{:S(2)}, u32[]{:S(2)}) collective-permute-start(bf16[24,512]{1,0:T(8,128)(2,1)S(1)} %get-tuple-element.38), channel_id=1, source_target_pairs={{0,2},{2,4},{4,6},{6,0},{1,3},{3,5},{5,7},{7,1},{8,10},{10,12},{12... | collective-permute-start | bytes 73736 | tf_op jit(solution)/shard_map/ppermute | solution.py:108
  39.4 5.5 %collective-permute-start.7 = (bf16[24,512]{1,0:T(8,128)(2,1)S(1)}, bf16[24,512]{1,0:T(8,128)(2,1)S(1)}, u32[]{:S(2)}, u32[]{:S(2)}) collective-permute-start(bf16[24,512]{1,0:T(8,128)(2,1)S(1)} %get-tuple-element.37), channel_id=1, source_target_pairs={{0,4},{2,6},{4,0},{6,2},{1,5},{3,7},{5,1},{7,3},{8,12},{10,14},{12... | collective-permute-start | bytes 73736 | tf_op jit(solution)/shard_map/ppermute | solution.py:108
  40.9 4.0 %collective-permute-start.6 = (bf16[24,512]{1,0:T(8,128)(2,1)S(1)}, bf16[24,512]{1,0:T(8,128)(2,1)S(1)}, u32[]{:S(2)}, u32[]{:S(2)}) collective-permute-start(bf16[24,512]{1,0:T(8,128)(2,1)S(1)} %get-tuple-element.36), channel_id=1, source_target_pairs={{0,6},{2,0},{4,2},{6,4},{1,7},{3,1},{5,3},{7,5},{8,14},{10,8},{12,... | collective-permute-start | bytes 73736 | tf_op jit(solution)/shard_map/ppermute | solution.py:108
